TPU v7x, 32 devices: a whole 2x2x4 slice. The times are simulated.
32 devices in a mesh: sp: 16 (over z, y, x), tp: 2 (over core).
Axes of the slice: x: 2, y: 2, z: 4, core: 2. Of those that a mesh axis runs over, the one named last changes fastest.
Arguments:
- conv_value: bfloat16 [4096, 1024], P('sp', 'tp'), may hold values from -6 to 6
- conv_gate: bfloat16 [4096, 1024], P('sp', 'tp'), may hold values from -6 to 6
- taps: bfloat16 [31, 1024], P(None, 'tp'), may hold values from -1 to 1
- doc_ids: int32 [4096], P('sp'), may hold values from 0 to 3, never falling along the last dimension, each value on 1 to 2048 neighbouring positions
- gn_gain: float32 [1024], P('tp'), may hold values from 0.1 to 1.9
- gn_shift: float32 [1024], P('tp'), may hold values from -3 to 3
- conv_out: bfloat16 [1024, 2048], replicated, may hold values from -0.1875 to 0.1875
- residual: bfloat16 [4096, 2048], P(('sp', 'tp')), may hold values from -6 to 6
- norm_gain: float32 [2048], replicated, may hold values from 0.1 to 1.9
- routes: int32 [4096, 2], P(('sp', 'tp')), may hold values from 0 to 31, as said below
- route_weight: float32 [4096, 2], P(('sp', 'tp')), may hold values from 0.3 to 1.2
- expert_gate: bfloat16 [32, 2048, 512], P(('sp', 'tp')), may hold values from -0.125 to 0.125
- expert_up: bfloat16 [32, 2048, 512], P(('sp', 'tp')), may hold values from -0.125 to 0.125
- expert_down: bfloat16 [32, 512, 2048], P(('sp', 'tp')), may hold values from -0.25 to 0.25
- shared_gate: bfloat16 [2048, 512], replicated, may hold values from -0.125 to 0.125
- shared_up: bfloat16 [2048, 512], replicated, may hold values from -0.125 to 0.125
- shared_down: bfloat16 [512, 2048], replicated, may hold values from -0.25 to 0.25
Outputs:
- layer_out: bfloat16 [4096, 2048], P(('sp', 'tp'))
Inputs may be any that keep to these rules, and one draw needn't show every extreme that they name: `routes`: each row names 2 different experts. The rows of one device name each expert at most 16 times, and one expert, the same for every device, exactly 16 times. `doc_ids`: numbers never fall from one position to the next.
All inputs are finite; a program needn't handle non-finite values.
Results may differ from a plain program's by a relative error of at most 0.014.
Values may be sent and summed in bfloat16 or wider, within the bound.
No kernel may reach another device: no remote copies, remote signals or barrier semaphores. Data moves between devices by JAX's collectives and lax.ppermute only.
A program may use at most 128 MiB of HBM per device.

v0:
```python
import jax
import jax.numpy as jnp
from jax import lax
from jax.sharding import PartitionSpec as P

GROUPS = 8


epsilon = 1e-06


def from_behind(x, axis, by):
    peers = lax.axis_size(axis)
    pairs = [(i, i + by) for i in range(peers) if 0 <= i + by < peers]
    return lax.ppermute(x, axis, pairs)


def per_device(
    conv_value,
    conv_gate,
    taps,
    doc_ids,
    gn_gain,
    gn_shift,
    conv_out,
    residual,
    norm_gain,
    routes,
    route_weight,
    expert_gate,
    expert_up,
    expert_down,
    shared_gate,
    shared_up,
    shared_down,
):
    position_count, channel_count = conv_value.shape
    kernel_width = taps.shape[0]
    model_width = residual.shape[1]
    glu_out = (
        conv_value.astype(jnp.float32) * jax.nn.sigmoid(conv_gate.astype(jnp.float32))
    ).astype(jnp.bfloat16)
    rim_start = position_count - kernel_width + 1
    edge_glu, edge_ids = from_behind((glu_out[rim_start:], doc_ids[rim_start:]), "sp", 1)
    longer_glu = jnp.concatenate([edge_glu, glu_out], axis=0)
    longer_ids = jnp.concatenate([edge_ids, doc_ids], axis=0)
    conv_sum = jnp.zeros((position_count, channel_count), jnp.float32)
    for offset in range(kernel_width):
        same_doc = (longer_ids[offset : offset + position_count] == doc_ids)[:, None]
        tap_term = taps[offset].astype(jnp.float32)[None, :] * longer_glu[
            offset : offset + position_count
        ].astype(jnp.float32)
        conv_sum = conv_sum + jnp.where(same_doc, tap_term, 0.0)
    core_split = lax.axis_size("tp")
    groups_here = GROUPS // core_split
    grouped = conv_sum.reshape(position_count, groups_here, channel_count // groups_here)
    group_mean = jnp.mean(grouped, axis=-1, keepdims=True)
    centered = grouped - group_mean
    group_var = jnp.mean(centered * centered, axis=-1, keepdims=True)
    normalized = (centered * lax.rsqrt(group_var + epsilon)).reshape(position_count, channel_count)
    conv_act = jax.nn.silu(normalized * gn_gain + gn_shift).astype(jnp.bfloat16)
    token_rows = lax.all_to_all(conv_act, "tp", split_axis=0, concat_axis=1, tiled=True)
    projected = jnp.dot(token_rows, conv_out, preferred_element_type=jnp.float32)
    stream = (residual.astype(jnp.float32) + projected).astype(jnp.bfloat16)
    stream_wide = stream.astype(jnp.float32)
    normed = (
        stream_wide
        * lax.rsqrt(jnp.mean(stream_wide * stream_wide, axis=-1, keepdims=True) + epsilon)
        * norm_gain
    ).astype(jnp.bfloat16)
    token_count, top_count = routes.shape
    sequence_split = lax.axis_size("sp")
    device_count = sequence_split * core_split
    local_experts = expert_gate.shape[0]
    experts = local_experts * device_count
    capacity = 2 * token_count * top_count // experts
    flat_routes = routes.reshape(-1)
    onehot = (flat_routes[:, None] == jnp.arange(experts, dtype=jnp.int32)[None, :]).astype(
        jnp.int32
    )
    slot_index = jnp.sum(jnp.cumsum(onehot, axis=0) * onehot, axis=1) - 1
    target = flat_routes * capacity + slot_index
    source = (
        jnp.full((experts * capacity,), token_count, jnp.int32)
        .at[target]
        .set(jnp.arange(token_count * top_count, dtype=jnp.int32) // top_count)
    )
    padded_rows = jnp.concatenate([normed, jnp.zeros((1, model_width), normed.dtype)], axis=0)
    outgoing = padded_rows[source]
    shared_hidden = (
        jax.nn.silu(jnp.dot(normed, shared_gate, preferred_element_type=jnp.float32))
        * jnp.dot(normed, shared_up, preferred_element_type=jnp.float32)
    ).astype(jnp.bfloat16)
    shared_out = jnp.dot(shared_hidden, shared_down, preferred_element_type=jnp.float32)
    parcel = outgoing.reshape(device_count, local_experts, capacity, model_width)
    arrived = lax.all_to_all(parcel, ("sp", "tp"), split_axis=0, concat_axis=0, tiled=True)
    expert_rows = arrived[:, 0].reshape(-1, model_width)
    gate_part = jnp.dot(expert_rows, expert_gate[0], preferred_element_type=jnp.float32)
    up_part = jnp.dot(expert_rows, expert_up[0], preferred_element_type=jnp.float32)
    hidden = (jax.nn.silu(gate_part) * up_part).astype(jnp.bfloat16)
    result = jnp.dot(hidden, expert_down[0], preferred_element_type=jnp.float32).astype(
        jnp.bfloat16
    )
    results = [result.reshape(arrived.shape[0], arrived.shape[2], model_width)]
    returned = lax.all_to_all(
        jnp.stack(results, axis=1), ("sp", "tp"), split_axis=0, concat_axis=0, tiled=True
    )
    picked = returned.reshape(experts * capacity, model_width)[target].reshape(
        token_count, top_count, model_width
    )
    routed = jnp.zeros((token_count, model_width), jnp.float32)
    for route_index in range(top_count):
        routed = routed + route_weight[:, route_index, None] * picked[:, route_index].astype(
            jnp.float32
        )
    return (stream_wide + shared_out + routed).astype(jnp.bfloat16)


def solution(mesh):
    return jax.shard_map(
        per_device,
        mesh=mesh,
        in_specs=(
            P("sp", "tp"),
            P("sp", "tp"),
            P(None, "tp"),
            P("sp"),
            P("tp"),
            P("tp"),
            P(),
            P(("sp", "tp"), None),
            P(),
            P(("sp", "tp"), None),
            P(("sp", "tp"), None),
            P(("sp", "tp"), None, None),
            P(("sp", "tp"), None, None),
            P(("sp", "tp"), None, None),
            P(),
            P(),
            P(),
        ),
        out_specs=P(("sp", "tp"), None),
        check_vma=False,
    )
```

profile of v0, /device:TPU:0, one launch (start us, length us, event | category | flops | bytes accessed | tf_op | source)
XLA Modules:
  0.0 168.0 jit_solution(8082973115691364182)
XLA Ops:
  0.0 0.9 slice.297
  0.9 4.9 %collective-permute-start = (s32[30]{0:T(128)S(1)}, s32[30]{0:T(128)S(1)}, u32[]{:S(2)}, u32[]{:S(2)}) collective-permute-start(s32[30]{0:T(128)S(1)} %slice.297), channel_id=1, source_target_pairs={{0,2},{2,4},{4,6},{6,8},{8,10},{10,12},{12,14},{14,16},{16,18},{18... | collective-permute-start | bytes 368 | tf_op jit(solution)/shard_map/ppermute | solution.py:15
  5.8 1.2 multiply_convert_fusion.2
  7.0 3.4 %collective-permute-start.1 = (bf16[30,512]{1,0:T(8,128)(2,1)S(1)}, bf16[30,512]{1,0:T(8,128)(2,1)S(1)}, u32[]{:S(2)}, u32[]{:S(2)}) collective-permute-start(bf16[30,512]{1,0:T(8,128)(2,1)S(1)} %slice.400), channel_id=1, source_target_pairs={{0,2},{2,4},{4,6},{6,8},{8,10},{10,12},{12,14},{14,16},{16,18},{18... | collective-permute-start | bytes 92168 | tf_op jit(solution)/shard_map/ppermute | solution.py:15
  10.4 1.0 slice_convert_fusion.30
  11.4 1.0 slice_convert_fusion.29
  12.4 0.8 copy.33
  13.2 0.1 eq.149
  13.3 0.1 eq.145
  13.5 0.7 broadcast_multiply_fusion.1
  14.2 0.6 reduce-window.6
  14.8 0.2 slice_reduce_fusion
  15.0 0.1 fusion.58
  15.1 0.1 copy.32
  15.2 0.1 mul.647
  15.4 1.4 scatter_custom_fusion
  16.8 0.0 collective-permute-done
  16.8 0.8 pad_add_fusion
  17.6 0.8 slice_compare_fusion.29
  18.4 0.8 slice_compare_fusion.28
  19.1 4.0 %multiply_add_fusion = f32[256,512]{1,0:T(8,128)S(1)} fusion(bf16[256,512]{1,0:T(8,128)(2,1)S(1)} %multiply_convert_fusion.2, bf16[30,512]{1,0:T(8,128)(2,1)S(1)} %collective-permute-done.1, f32[512]{0:T(512)S(1)} %bitcast.151, f32[512]{0:T(512)S(1)} %bitcast.152, f32[512]{0:T(512)S(1)} %bitcast.123, f32[512]{0:T(512)S(1)} %bitcast.124, ...), kind=kLoop, calls=%fused_computation.62 | loop fusion | flops 27787264 | bytes 888320 | tf_op jit(solution)/shard_map/add | solution.py:53
  23.2 0.0 copy-start.6
  23.2 0.0 copy-start.7
  23.2 0.2 reshape.126
  23.4 0.3 reduce_sum.36
  23.8 0.6 multiply_reduce_fusion.1
  24.4 0.0 copy-start.4
  24.4 0.3 mul.630
  24.8 0.3 sub.25
  25.1 0.2 multiply_convert_fusion.1
  25.3 3.9 %all_to_all.29 = bf16[2,128,512]{2,1,0:T(8,128)(2,1)S(1)} all-to-all(bf16[2,128,512]{2,1,0:T(8,128)(2,1)S(1)} %bitcast.119), channel_id=1, replica_groups=mesh['sp'=16,'tp'=2] {'tp'}, dimensions={0} | all-to-all | bytes 524288 | tf_op jit(solution)/shard_map/all_to_all | solution.py:62
  29.3 0.2 copy.31
  29.5 0.0 copy-start.5
  29.5 3.0 %multiply_reduce_fusion = (f32[128]{0:T(128)S(1)}, f32[128,2048]{1,0:T(8,128)S(1)}) fusion(bf16[128,1024]{0,1:T(8,128)(2,1)S(1)} %bitcast.120, bf16[1024,2048]{1,0:T(8,128)(2,1)} %param.23, bf16[128,2048]{1,0:T(8,128)(2,1)S(1)} %copy-done.4), kind=kOutput, calls=%fused_computation.52 | convolution fusion | flops 538443648 | bytes 6029824 | tf_op jit(solution)/shard_map/dot_general | solution.py:63
  32.5 1.0 copy-done.2
  33.5 0.2 multiply_convert_fusion
  33.7 3.3 %gather_fusion = bf16[512,2048]{1,0:T(8,128)(2,1)} fusion(bf16[129,2048]{1,0:T(8,128)(2,1)S(1)} %concatenate.11, s32[1024]{0:T(1024)S(1)} %pad_clamp_fusion.1), kind=kCustom, calls=%fused_computation | custom fusion | bytes 4196352 | tf_op jit(solution)/shard_map/gather | solution.py:89
  37.1 53.6 %all_to_all.30 = bf16[32,1,16,2048]{3,2,1,0:T(8,128)(2,1)S(1)} all-to-all(bf16[32,1,16,2048]{3,2,1,0:T(8,128)(2,1)} %bitcast.113), channel_id=1, replica_groups=mesh['sp'=16,'tp'=2] {'sp','tp'}, dimensions={0} | all-to-all | bytes 4194304 | tf_op jit(solution)/shard_map/all_to_all | solution.py:96
  90.6 1.3 copy-done.3
  91.9 2.3 %fusion.7 = f32[512,512]{1,0:T(8,128)} fusion(bf16[512,2048]{1,0:T(8,128)(2,1)S(1)} %bitcast.117, bf16[1,2048,512]{2,1,0:T(8,128)(2,1)S(1)} %copy-done.9), kind=kOutput, calls=%fused_computation.42 | convolution fusion | flops 1073741824 | bytes 5242880 | tf_op jit(solution)/shard_map/dot_general | solution.py:98
  94.2 6.3 %convolution_convert_fusion = bf16[512,2048]{1,0:T(8,128)(2,1)} fusion(bf16[1,512,2048]{2,1,0:T(8,128)(2,1)S(1)} %copy-done, bf16[512,2048]{1,0:T(8,128)(2,1)} %bitcast.118, bf16[1,2048,512]{2,1,0:T(8,128)(2,1)} %param.29, f32[512,512]{1,0:T(8,128)} %fusion.7), kind=kOutput, calls=%fused_computation.3 | convolution fusion | flops 2150105088 | bytes 9437184 | tf_op jit(solution)/shard_map/dot_general | solution.py:101
  100.5 4.0 %all-to-all-start.2 = ((bf16[32,1,16,2048]{3,2,1,0:T(8,128)(2,1)}), bf16[32,1,16,2048]{3,2,1,0:T(8,128)(2,1)}, u32[]{:S(2)}, u32[]{:S(2)}) async-start(bf16[32,1,16,2048]{3,2,1,0:T(8,128)(2,1)} %bitcast.116), calls=%async_computation.2 | async-start | bytes 4194304 | tf_op jit(solution)/shard_map/all_to_all | solution.py:105
  104.5 2.0 %fusion.65 = f32[128,512]{1,0:T(8,128)S(1)} fusion(bf16[128,2048]{1,0:T(8,128)(2,1)S(1)} %multiply_convert_fusion, bf16[2048,512]{1,0:T(8,128)(2,1)} %param.31), kind=kOutput, calls=%fused_computation.198 | convolution fusion | flops 268435456 | bytes 2883584 | tf_op jit(solution)/shard_map/dot_general | solution.py:91
  106.5 46.6 %all-to-all-done.2 = bf16[32,1,16,2048]{3,2,1,0:T(8,128)(2,1)} async-done(((bf16[32,1,16,2048]{3,2,1,0:T(8,128)(2,1)}), bf16[32,1,16,2048]{3,2,1,0:T(8,128)(2,1)}, u32[]{:S(2)}, u32[]{:S(2)}) %all-to-all-start.2) | async-done | bytes 2097184 | tf_op jit(solution)/shard_map/all_to_all | solution.py:105
  153.1 5.2 %gather_fusion.1 = bf16[256,2048]{1,0:T(8,128)(2,1)} fusion(bf16[512,2048]{1,0:T(8,128)(2,1)} %bitcast.46, s32[1024]{0:T(1024)S(1)} %pad_clamp_fusion), kind=kCustom, calls=%fused_computation.1 | custom fusion | bytes 2098176 | tf_op jit(solution)/shard_map/gather | solution.py:108
  158.3 1.7 %reshape.130 = bf16[128,2,2048]{2,1,0:T(2,128)(2,1)S(1)} reshape(bf16[256,2048]{1,0:T(8,128)(2,1)} %gather_fusion.1) | data formatting | bytes 2097152 | tf_op jit(solution)/shard_map/reshape | solution.py:108
  160.1 2.5 %fusion.64 = (bf16[128,1,2048]{2,1,0:T(2,128)(2,1)}, bf16[128,1,2048]{2,1,0:T(2,128)(2,1)}) fusion(bf16[128,2,2048]{2,1,0:T(2,128)(2,1)S(1)} %reshape.130), kind=kLoop, calls=%fused_computation.197 | loop fusion | bytes 2097152 | tf_op jit(solution)/shard_map/slice | solution.py:113
  162.6 5.4 %fusion.3 = bf16[128,2048]{1,0:T(8,128)(2,1)} fusion(f32[128,2048]{1,0:T(8,128)} %copy-done.2, bf16[512,2048]{1,0:T(8,128)(2,1)} %param.33, bf16[128,2048]{1,0:T(8,128)(2,1)} %copy-done.1, bf16[2048,512]{1,0:T(8,128)(2,1)} %param.32, bf16[128,1,2048]{2,1,0:T(2,128)(2,1)} %get-tuple-element.6, bf16[128,1,2048]{2,1,0:T(2,128)(2,1)} %get-tuple-element.5, ...), kind=kOutput, calls=%fused_computation.38 | convolution fusion | flops 539361280 | bytes 7603200 | tf_op jit(solution)/shard_map/dot_general | solution.py:94
  (30 shorter events, 0.2 us)
Async XLA Ops:
  0.0 94.2 %copy-start = (bf16[1,512,2048]{2,1,0:T(8,128)(2,1)S(1)}, bf16[1,512,2048]{2,1,0:T(8,128)(2,1)}, u32[]{:S(2)}) copy-start(bf16[1,512,2048]{2,1,0:T(8,128)(2,1)} %param.30) | copy-start | bytes 6291460
  0.9 15.9 %collective-permute-start = (s32[30]{0:T(128)S(1)}, s32[30]{0:T(128)S(1)}, u32[]{:S(2)}, u32[]{:S(2)}) collective-permute-start(s32[30]{0:T(128)S(1)} %slice.297), channel_id=1, source_target_pairs={{0,2},{2,4},{4,6},{6,8},{8,10},{10,12},{12,14},{14,16},{16,18},{18... | collective-permute-start | bytes 368 | tf_op jit(solution)/shard_map/ppermute | solution.py:15
  7.0 12.2 %collective-permute-start.1 = (bf16[30,512]{1,0:T(8,128)(2,1)S(1)}, bf16[30,512]{1,0:T(8,128)(2,1)S(1)}, u32[]{:S(2)}, u32[]{:S(2)}) collective-permute-start(bf16[30,512]{1,0:T(8,128)(2,1)S(1)} %slice.400), channel_id=1, source_target_pairs={{0,2},{2,4},{4,6},{6,8},{8,10},{10,12},{12,14},{14,16},{16,18},{18... | collective-permute-start | bytes 92168 | tf_op jit(solution)/shard_map/ppermute | solution.py:15
  23.2 1.9 %copy-start.6 = (f32[512]{0:T(512)S(1)}, f32[512]{0:T(512)}, u32[]{:S(2)}) copy-start(f32[512]{0:T(512)} %param.22) | copy-start | bytes 6148
  23.2 1.9 %copy-start.7 = (f32[512]{0:T(512)S(1)}, f32[512]{0:T(512)}, u32[]{:S(2)}) copy-start(f32[512]{0:T(512)} %param.21) | copy-start | bytes 6148
  24.4 5.0 %copy-start.4 = (bf16[128,2048]{1,0:T(8,128)(2,1)S(1)}, bf16[128,2048]{1,0:T(8,128)(2,1)}, u32[]{:S(2)}) copy-start(bf16[128,2048]{1,0:T(8,128)(2,1)} %param.24) | copy-start | bytes 1572868
  29.5 4.0 %copy-start.5 = (f32[2048]{0:T(1024)S(1)}, f32[2048]{0:T(1024)}, u32[]{:S(2)}) copy-start(f32[2048]{0:T(1024)} %param.25) | copy-start | bytes 24580
  32.5 1.0 copy-start.2
  33.6 70.8 %copy-start.1 = (bf16[128,2048]{1,0:T(8,128)(2,1)}, bf16[128,2048]{1,0:T(8,128)(2,1)S(1)}, u32[]{:S(2)}) copy-start(bf16[128,2048]{1,0:T(8,128)(2,1)S(1)} %multiply_convert_fusion) | copy-start | bytes 1572868
  37.1 54.9 %copy-start.9 = (bf16[1,2048,512]{2,1,0:T(8,128)(2,1)S(1)}, bf16[1,2048,512]{2,1,0:T(8,128)(2,1)}, u32[]{:S(2)}) copy-start(bf16[1,2048,512]{2,1,0:T(8,128)(2,1)} %param.28) | copy-start | bytes 6291460
  90.6 1.3 copy-start.3
  100.5 4.0 %copy-start.8 = (f32[128,2]{0,1:T(2,128)S(1)}, f32[128,2]{0,1:T(2,128)}, u32[]{:S(2)}) copy-start(f32[128,2]{0,1:T(2,128)} %param.27) | copy-start | bytes 3076
  100.5 52.6 %all-to-all-start.2 = ((bf16[32,1,16,2048]{3,2,1,0:T(8,128)(2,1)}), bf16[32,1,16,2048]{3,2,1,0:T(8,128)(2,1)}, u32[]{:S(2)}, u32[]{:S(2)}) async-start(bf16[32,1,16,2048]{3,2,1,0:T(8,128)(2,1)} %bitcast.116), calls=%async_computation.2 | async-start | bytes 4194304 | tf_op jit(solution)/shard_map/all_to_all | solution.py:105
where the time goes:
time: 169 us; the launch traced here: 168 us
  blocking collectives  57.5 us (34%)
  waiting for transfers between devices  46.6 us (28%)
  local copies, waits for them, and re-layouts  20 us (12%)
  matrix products  19 us (11%)
  other arithmetic  12.3 us (7%)
  starting transfers between devices  12.2 us (7%)
    all_to_all x1, blocking collectives, per_device(): lax.all_to_all(parcel, ('sp', 'tp'), split_axis=0, concat_axis=0, tiled=T...  53.6 us
    all_to_all x1, waiting for transfers between devices, per_device(): lax.all_to_all(jnp.stack(results, axis=1), ('sp', 'tp'), split_axis=0, co...  46.6 us
    ppermute x2, starting transfers between devices, from_behind(): return lax.ppermute(x, axis, pairs)  8.26 us
    dot_general x1, matrix products, per_device(): jnp.dot(hidden, expert_down[0], preferred_element_type=jnp.float32)  6.28 us
    dot_general x1, matrix products, per_device(): jnp.dot(shared_hidden, shared_down, preferred_element_type=jnp.float32)  5.43 us
    gather x1, local copies, waits for them, and re-layouts, per_device(): returned.reshape(experts * capacity, model_width)[target]  5.21 us
    add x1, other arithmetic, per_device(): conv_sum = conv_sum + jnp.where(same_doc, tap_term, 0.0)  4.03 us
    all_to_all x1, starting transfers between devices, per_device(): lax.all_to_all(jnp.stack(results, axis=1), ('sp', 'tp'), split_axis=0, co...  3.96 us
  transfers between devices with their start and end apart: 3, of which 1 were waited for; matrix products, arithmetic and copies ran while one was open for 7% of the time, Pallas kernels for 0%

commit v1 on v0

v1 whole, which is shorter than its diff:
```python
import functools

import jax
import jax.numpy as jnp
from jax import lax
from jax.experimental import pallas as pl
from jax.experimental.pallas import tpu as pltpu
from jax.sharding import Mesh
from jax.sharding import PartitionSpec as P

LANES = 128


epsilon = 1e-06

HALF = ("sp", "tp")
LINE = ("half", "sp")

F32, BF16, I32 = jnp.float32, jnp.bfloat16, jnp.int32


def from_behind(x, axis, by):
    peers = lax.axis_size(axis)
    pairs = [(i, i + by) for i in range(peers) if 0 <= i + by < peers]
    return lax.ppermute(x, axis, pairs)


def to_mirror(x):
    return lax.ppermute(x, "half", [(0, 1), (1, 0)])


def call(body, outs, scratch=(), flops=0, moved=0):
    return pl.pallas_call(
        body,
        out_shape=outs,
        scratch_shapes=list(scratch),
        cost_estimate=pl.CostEstimate(flops=flops, bytes_accessed=moved, transcendentals=0),
    )


def glu_of(value, gate):
    return (value.astype(F32) * jax.nn.sigmoid(gate.astype(F32))).astype(BF16)


def conv_body(
    value_ref, gate_ref, edge_ref, ids_ref, taps_ref, gain_ref, shift_ref, out_ref, glu, ids
):
    positions, channels = value_ref.shape
    width = taps_ref.shape[0]
    rim = edge_ref.shape[0]
    blocks = channels // LANES
    rows = 32
    ids[pl.ds(0, rim), :] = edge_ref[:, pl.ds(channels, LANES)].astype(F32)
    ids[pl.ds(rim, positions), :] = ids_ref[...]
    for c in range(blocks):
        lanes = pl.ds(c * LANES, LANES)
        glu[c, pl.ds(0, rim), :] = edge_ref[:, lanes].astype(F32)
        glu[c, pl.ds(rim, positions), :] = glu_of(value_ref[:, lanes], gate_ref[:, lanes]).astype(
            F32
        )

    def chunk(index, carry):
        row = pl.multiple_of(index * rows, rows)
        here = ids[pl.ds(row + rim, rows), :]
        total = [jnp.zeros((rows, LANES), F32) for _ in range(blocks)]
        for tap in range(width):
            past = row + (rim - width + 1 + tap)
            same = ids[pl.ds(past, rows), :] == here
            for c in range(blocks):
                weight = taps_ref[pl.ds(tap, 1), pl.ds(c * LANES, LANES)]
                term = weight * glu[c, pl.ds(past, rows), :]
                total[c] = total[c] + jnp.where(same, term, 0.0)
        for c in range(blocks):
            lanes = pl.ds(c * LANES, LANES)
            centered = total[c] - jnp.mean(total[c], axis=-1, keepdims=True)
            spread = jnp.mean(centered * centered, axis=-1, keepdims=True)
            scaled = centered * lax.rsqrt(spread + epsilon)
            out_ref[pl.ds(row, rows), lanes] = jax.nn.silu(
                scaled * gain_ref[:, lanes] + shift_ref[:, lanes]
            ).astype(BF16)
        return carry

    lax.fori_loop(0, positions // rows, chunk, 0)


def convolve(value, gate, edge, ids, taps, gain, shift):
    positions, channels = value.shape
    rim = edge.shape[0]
    return call(
        conv_body,
        jax.ShapeDtypeStruct(value.shape, BF16),
        scratch=[
            pltpu.VMEM((channels // LANES, rim + positions, LANES), F32),
            pltpu.VMEM((rim + positions, LANES), F32),
        ],
        flops=6_000_000_000,
        moved=3 * value.size * 2,
    )(value, gate, edge, ids, taps, gain, shift)


def selection(routes, first, experts, capacity, rows):
    top, tokens = routes.shape
    routes = routes.astype(I32)
    names = lax.broadcasted_iota(I32, (experts, tokens), 0)
    earlier = lax.broadcasted_iota(I32, (tokens, tokens), 0) < lax.broadcasted_iota(
        I32, (tokens, tokens), 1
    )
    earlier = earlier.astype(F32).astype(BF16)
    index = lax.broadcasted_iota(I32, (rows, tokens), 0)
    used = jnp.zeros((experts, 1), F32)
    picks = []
    for k in range(top):
        route = routes[k : k + 1, :]
        chosen = (names == route).astype(F32)
        before = jnp.dot(chosen.astype(BF16), earlier, preferred_element_type=F32) + used
        slot = jnp.sum(chosen * before, axis=0, keepdims=True).astype(I32)
        picks.append(index == (route - first) * capacity + slot)
        used = used + jnp.sum(chosen, axis=1, keepdims=True)
    return picks


def project_body(
    shape_of, keep, first_ref, act_ref, weight_ref, residual_ref, gain_ref, routes_ref, *outs
):
    experts, capacity = shape_of
    parcel_ref = outs[0]
    parts, _, depth = act_ref.shape
    projected = jnp.dot(act_ref[0], weight_ref[pl.ds(0, depth), :], preferred_element_type=F32)
    for part in range(1, parts):
        projected = projected + jnp.dot(
            act_ref[part], weight_ref[pl.ds(part * depth, depth), :], preferred_element_type=F32
        )
    stream = (residual_ref[...].astype(F32) + projected).astype(BF16)
    wide = stream.astype(F32)
    normed = (
        wide * lax.rsqrt(jnp.mean(wide * wide, axis=-1, keepdims=True) + epsilon) * gain_ref[...]
    ).astype(BF16)
    if keep:
        outs[1][...] = stream
        outs[2][...] = normed
    picks = selection(routes_ref[...], first_ref[0], experts, capacity, parcel_ref.shape[0])
    chosen = functools.reduce(jnp.logical_or, picks).astype(F32).astype(BF16)
    parcel_ref[...] = jnp.dot(chosen, normed, preferred_element_type=F32).astype(BF16)


def project(act, weight, residual, gain, routes, first, experts, capacity, rows, keep):
    tokens, width = residual.shape
    out = jax.ShapeDtypeStruct((tokens, width), BF16)
    outs = [jax.ShapeDtypeStruct((rows, width), BF16)] + [out, out] * keep
    smem = pl.BlockSpec(memory_space=pltpu.SMEM)
    vmem = pl.BlockSpec(memory_space=pltpu.VMEM)
    return pl.pallas_call(
        functools.partial(project_body, (experts, capacity), keep),
        out_shape=outs,
        in_specs=[smem] + [vmem] * 5,
        out_specs=[vmem] * len(outs),
        cost_estimate=pl.CostEstimate(
            flops=2 * tokens * weight.size, bytes_accessed=2 * weight.size, transcendentals=0
        ),
        name="project_keep" if keep else "project",
    )(first, act, weight, residual, gain, routes)


def mlp_body(rows_ref, gate_ref, up_ref, down_ref, out_ref, hidden):
    inner = gate_ref.shape[-1]
    width = out_ref.shape[-1]
    rows = rows_ref[...]
    tile = min(inner, 256)
    for n in range(inner // tile):
        cols = pl.ds(n * tile, tile)
        gate = jnp.dot(rows, gate_ref[:, cols], preferred_element_type=F32)
        up = jnp.dot(rows, up_ref[:, cols], preferred_element_type=F32)
        hidden[:, cols] = (jax.nn.silu(gate) * up).astype(BF16)
    tile = min(width, 512)
    for n in range(width // tile):
        cols = pl.ds(n * tile, tile)
        out_ref[:, cols] = jnp.dot(
            hidden[...], down_ref[:, cols], preferred_element_type=F32
        ).astype(out_ref.dtype)


def gated_mlp(rows, gate, up, down, dtype):
    count, width = rows.shape
    inner = gate.shape[-1]
    return call(
        mlp_body,
        jax.ShapeDtypeStruct((count, width), dtype),
        scratch=[pltpu.VMEM((count, inner), BF16)],
        flops=6 * count * width * inner,
        moved=6 * width * inner,
    )(rows, gate, up, down)


def combine_body(shape_of, first_ref, routes_ref, weight_ref, back_ref, *rest):
    experts, capacity = shape_of
    out_ref = rest[-1]
    rows = back_ref.shape[0]
    picks = selection(routes_ref[...], first_ref[0], experts, capacity, rows)
    table = jnp.zeros((rows, routes_ref.shape[1]), F32)
    for k, pick in enumerate(picks):
        table = table + jnp.where(pick, weight_ref[k : k + 1, :], 0.0)
    high = table.astype(BF16)
    low = (table - high.astype(F32)).astype(BF16)
    back = back_ref[...]
    over = (((0,), (0,)), ((), ()))
    total = lax.dot_general(high, back, over, preferred_element_type=F32)
    total = total + lax.dot_general(low, back, over, preferred_element_type=F32)
    for ref in rest[:-1]:
        total = total + ref[...].astype(F32)
    out_ref[...] = total.astype(out_ref.dtype)


def combine(routes, weights, back, first, experts, capacity, dtype, extra):
    rows, width = back.shape
    tokens = routes.shape[1]
    smem = pl.BlockSpec(memory_space=pltpu.SMEM)
    vmem = pl.BlockSpec(memory_space=pltpu.VMEM)
    return pl.pallas_call(
        functools.partial(combine_body, (experts, capacity)),
        out_shape=jax.ShapeDtypeStruct((tokens, width), dtype),
        in_specs=[smem] + [vmem] * (3 + len(extra)),
        out_specs=vmem,
        cost_estimate=pl.CostEstimate(
            flops=4 * tokens * rows * width, bytes_accessed=2 * rows * width, transcendentals=0
        ),
    )(first, routes, weights, back, *extra)


def per_device(
    conv_value,
    conv_gate,
    taps,
    doc_ids,
    gn_gain,
    gn_shift,
    conv_out,
    residual,
    norm_gain,
    routes,
    route_weight,
    expert_gate,
    expert_up,
    expert_down,
    shared_gate,
    shared_up,
    shared_down,
):
    position_count, channel_count = conv_value.shape
    kernel_width = taps.shape[0]
    model_width = residual.shape[1]
    token_count, top_count = routes.shape
    core_split = lax.axis_size("tp")
    half_devices = lax.axis_size("sp") * core_split
    local_experts = expert_gate.shape[0]
    half_experts = local_experts * half_devices
    experts = half_experts * lax.axis_size("half")
    capacity = 2 * token_count * top_count // experts
    half_rows = half_experts * capacity
    first = (lax.axis_index("half").astype(I32) * half_experts).reshape(1)

    mirror_residual = to_mirror(residual)

    rim = -(-(kernel_width - 1) // 8) * 8
    rim_glu = glu_of(conv_value[-rim:], conv_gate[-rim:])
    rim_ids = jnp.broadcast_to(doc_ids[-rim:, None].astype(BF16), (rim, LANES))
    edge = from_behind(jnp.concatenate([rim_glu, rim_ids], axis=1), LINE, 1)
    own_meta = jnp.concatenate([routes.astype(F32), route_weight], axis=1).T
    mirror_meta = to_mirror(own_meta)
    own_routes, own_weight = own_meta[:top_count], own_meta[top_count:]
    mirror_routes, mirror_weight = mirror_meta[:top_count], mirror_meta[top_count:]

    wide_ids = jnp.broadcast_to(doc_ids[:, None].astype(F32), (position_count, LANES))
    conv_act = convolve(
        conv_value,
        conv_gate,
        edge,
        wide_ids,
        taps.astype(F32),
        gn_gain[None, :],
        gn_shift[None, :],
    )
    by_core = conv_act.reshape(core_split, token_count, channel_count)
    act = lax.all_to_all(by_core, "tp", split_axis=0, concat_axis=0, tiled=True)
    mirror_act = to_mirror(act)

    def exchange(rows):
        parcel = rows.reshape(half_devices, local_experts * capacity, model_width)
        arrived = lax.all_to_all(parcel, HALF, split_axis=0, concat_axis=0, tiled=True)
        return arrived.reshape(half_rows, model_width)

    def experts_on(rows):
        split = rows.reshape(half_devices, local_experts, capacity, model_width)
        results = []
        for e in range(local_experts):
            mine = split[:, e].reshape(half_devices * capacity, model_width)
            result = gated_mlp(mine, expert_gate[e], expert_up[e], expert_down[e], BF16)
            results.append(result.reshape(half_devices, capacity, model_width))
        return jnp.stack(results, axis=1)

    sizes = (experts, capacity)
    gain = norm_gain[None, :]
    parcel, stream, normed = project(
        act, conv_out, residual, gain, own_routes, first, *sizes, half_rows, True
    )
    own_arrived = exchange(parcel)
    (mirror_parcel,) = project(
        mirror_act, conv_out, mirror_residual, gain, mirror_routes, first, *sizes, half_rows, False
    )
    mirror_arrived = exchange(mirror_parcel)
    shared_out = gated_mlp(normed, shared_gate, shared_up, shared_down, F32)
    own_result = experts_on(own_arrived)
    mirror_result = experts_on(mirror_arrived)
    mirror_back = exchange(mirror_result)
    partial = combine(mirror_routes, mirror_weight, mirror_back, first, *sizes, BF16, ())
    other_part = to_mirror(partial)
    own_back = exchange(own_result)
    own_part = combine(own_routes, own_weight, own_back, first, *sizes, F32, (stream, shared_out))
    return (own_part + other_part.astype(F32)).astype(BF16)


def solution(mesh):
    sequence_split, core_split = mesh.devices.shape
    folded = Mesh(
        mesh.devices.reshape(2, sequence_split // 2, core_split), ("half", "sp", "tp")
    )
    line, everyone = LINE, LINE + ("tp",)
    return jax.shard_map(
        per_device,
        mesh=folded,
        in_specs=(
            P(line, "tp"),
            P(line, "tp"),
            P(None, "tp"),
            P(line),
            P("tp"),
            P("tp"),
            P(),
            P(everyone, None),
            P(),
            P(everyone, None),
            P(everyone, None),
            P(everyone, None, None),
            P(everyone, None, None),
            P(everyone, None, None),
            P(),
            P(),
            P(),
        ),
        out_specs=P(everyone, None),
        check_vma=False,
    )
```

time: 169 us -> 146 us (0.86)
  blocking collectives: 57.5 us -> 4.98 us
  Pallas kernels: 0 us -> 38 us
  matrix products: 19 us -> 0 us
  waiting for transfers between devices: 46.6 us -> 64.5 us
  local copies, waits for them, and re-layouts: 20 us -> 3.94 us
  starting transfers between devices: 12.2 us -> 27.9 us
  other arithmetic: 12.3 us -> 5.76 us
    all_to_all x2 -> x1, blocking collectives: 57.5 us -> 4.98 us  [per_device(): act = lax.all_to_all(by_core, 'tp', split_axis=0, concat_axis=0, tiled=True)]
    pallas_call x0 -> x8, Pallas kernels: none -> 38 us  [the longest x3 17 us: gated_mlp(): call(mlp_body, jax.ShapeDtypeStruct((count, width), dtype), scratch=[pltp...]
    dot_general x5 -> x0, matrix products: 19 us -> none  [the longest x1 6.28 us: per_device(): jnp.dot(hidden, expert_down[0], preferred_element_type=jnp.float32)]
    ppermute x0 -> x4, waiting for transfers between devices: none -> 18.1 us  [to_mirror(): return lax.ppermute(x, 'half', [(0, 1), (1, 0)])]
    all_to_all x1 -> x4, starting transfers between devices: 3.96 us -> 14.8 us  [exchange(): lax.all_to_all(parcel, HALF, split_axis=0, concat_axis=0, tiled=True)]
    gather x2 -> x0, local copies, waits for them, and re-layouts: 8.56 us -> none  [the longest x1 5.21 us: per_device(): returned.reshape(experts * capacity, model_width)[target]]
    ppermute x0 -> x4, starting transfers between devices: none -> 8.2 us  [to_mirror(): return lax.ppermute(x, 'half', [(0, 1), (1, 0)])]
    convert_element_type x4 -> x5, other arithmetic: 1.55 us -> 5.75 us  [the longest x1 2.13 us: per_device(): return (own_part + other_part.astype(F32)).astype(BF16)]
  transfers between devices with their start and end apart: 3 -> 9, of which waited for: 1 -> 5; matrix products, arithmetic and copies ran while one was open for 7% -> 3% of each run, Pallas kernels for 0% -> 23%
where the time goes in v1:
time: 146 us; the launch traced here: 145 us
  waiting for transfers between devices  64.5 us (44%)
  Pallas kernels  38 us (26%)
  starting transfers between devices  27.9 us (19%)
  other arithmetic  5.76 us (4%)
  blocking collectives  4.98 us (3%)
  local copies, waits for them, and re-layouts  3.94 us (3%)
    all_to_all x4, waiting for transfers between devices, exchange(): lax.all_to_all(parcel, HALF, split_axis=0, concat_axis=0, tiled=True)  46.4 us
    ppermute x4, waiting for transfers between devices, to_mirror(): return lax.ppermute(x, 'half', [(0, 1), (1, 0)])  18.1 us
    pallas_call x3, Pallas kernels, gated_mlp(): call(mlp_body, jax.ShapeDtypeStruct((count, width), dtype), scratch=[pltp...  17 us
    all_to_all x4, starting transfers between devices, exchange(): lax.all_to_all(parcel, HALF, split_axis=0, concat_axis=0, tiled=True)  14.8 us
    pallas_call x2, Pallas kernels, project(): pl.pallas_call(functools.partial(project_body, (experts, capacity), keep)...  9.33 us
    ppermute x4, starting transfers between devices, to_mirror(): return lax.ppermute(x, 'half', [(0, 1), (1, 0)])  8.2 us
    pallas_call x2, Pallas kernels, combine(): pl.pallas_call(functools.partial(combine_body, (experts, capacity)), out_...  6.04 us
    pallas_call x1, Pallas kernels, convolve(): call(conv_body, jax.ShapeDtypeStruct(value.shape, BF16), scratch=[pltpu.V...  5.61 us
  transfers between devices with their start and end apart: 9, of which 5 were waited for; matrix products, arithmetic and copies ran while one was open for 3% of the time, Pallas kernels for 23%

profile of v1, /device:TPU:0, one launch (start us, length us, event | category | flops | bytes accessed | tf_op | source)
XLA Modules:
  0.0 145.1 jit_solution(16073379713897328492)
XLA Ops:
  0.0 0.8 fusion.2
  0.8 0.1 slice.26
  0.8 0.8 multiply_convert_fusion
  1.6 0.1 broadcast_in_dim.10
  1.7 4.9 %collective-permute-start = (bf16[32,640]{1,0:T(8,128)(2,1)S(1)}, bf16[32,640]{1,0:T(8,128)(2,1)S(1)}, u32[]{:S(2)}, u32[]{:S(2)}) collective-permute-start(bf16[32,640]{1,0:T(8,128)(2,1)S(1)} %pad_maximum_fusion), channel_id=1, source_target_pairs={{0,2},{2,4},{4,6},{6,8},{8,10},{10,12},{12,14},{14,16},{16,18},{18... | collective-permute-start | bytes 122888 | tf_op jit(solution)/shard_map/ppermute | solution.py:25
  6.6 2.7 %collective-permute-start.3 = (bf16[128,2048]{1,0:T(8,128)(2,1)}, bf16[128,2048]{1,0:T(8,128)(2,1)S(1)}, u32[]{:S(2)}, u32[]{:S(2)}) collective-permute-start(bf16[128,2048]{1,0:T(8,128)(2,1)} %residual_ref.1), channel_id=1, source_target_pairs={{0,16},{16,0},{1,17},{17,1},{2,18},{18,2},{3,19},{19,3},{4,20},{20... | collective-permute-start | bytes 1572872 | tf_op jit(solution)/shard_map/ppermute | solution.py:29
  9.3 1.4 convert_element_type.32.taps_ref
  10.6 0.7 convert_element_type.27
  11.3 0.0 collective-permute-done.edge_ref
  11.3 0.0 copy-start.8
  11.3 0.7 broadcast_in_dim.22.ids_ref
  12.1 0.0 copy-done.8
  12.1 5.6 %shard_map.163 = bf16[256,512]{1,0:T(8,128)(2,1)} custom-call(bf16[256,512]{1,0:T(8,128)(2,1)} %value_ref.1, bf16[256,512]{1,0:T(8,128)(2,1)} %gate_ref.2, bf16[32,640]{1,0:T(8,128)(2,1)} %copy-done.8, f32[256,128]{1,0:T(8,128)} %broadcast_in_dim.22.ids_ref, f32[31,512]{1,0:T(8,128)} %convert_element_type.32.taps_ref, f32[1,512]{1,0:T(1,128)} %bitcast.35, ...), custom_call_target="tpu_custom_call" | custom-call | flops 6000000000 | bytes 786432 | tf_op jit(solution)/shard_map/pallas_call | solution.py:89
  17.7 5.0 %all_to_all.25.act_ref = bf16[2,128,512]{2,1,0:T(8,128)(2,1)S(1)} all-to-all(bf16[2,128,512]{2,1,0:T(8,128)(2,1)} %bitcast.32), channel_id=1, replica_groups=mesh['half'=2,'sp'=8,'tp'=2] {'tp'}, dimensions={0} | all-to-all | bytes 524288 | tf_op jit(solution)/shard_map/all_to_all | solution.py:283
  22.7 2.6 %collective-permute-start.2 = (bf16[2,128,512]{2,1,0:T(8,128)(2,1)S(1)}, bf16[2,128,512]{2,1,0:T(8,128)(2,1)S(1)}, u32[]{:S(2)}, u32[]{:S(2)}) collective-permute-start(bf16[2,128,512]{2,1,0:T(8,128)(2,1)S(1)} %all_to_all.25.act_ref), channel_id=1, source_target_pairs={{0,16},{16,0},{1,17},{17,1},{2,18},{18,2},{3,19},{19,3},{4,20},{20... | collective-permute-start | bytes 786440 | tf_op jit(solution)/shard_map/ppermute | solution.py:29
  25.2 0.0 copy-done.7
  25.3 0.4 collective-permute-start.1
  25.7 18.0 %collective-permute-done.1 = f32[4,128]{1,0:T(4,128)S(1)} collective-permute-done((f32[4,128]{1,0:T(4,128)S(1)}, f32[4,128]{1,0:T(4,128)S(1)}, u32[]{:S(2)}, u32[]{:S(2)}) %collective-permute-start.1) | collective-permute-done | bytes 2080 | tf_op jit(solution)/shard_map/ppermute | solution.py:29
  43.7 0.6 fusion
  44.3 0.0 collective-permute-done.2.act_ref
  44.3 0.0 collective-permute-done.3.residual_ref
  44.3 0.0 copy-start.5
  44.3 0.7 copy-done.6
  45.0 0.2 copy-done.5
  45.2 4.6 %project.1 = bf16[256,2048]{1,0:T(8,128)(2,1)} custom-call(s32[1]{0:T(128)} %bitcast.first_ref, bf16[2,128,512]{2,1,0:T(8,128)(2,1)} %copy-done.6, bf16[1024,2048]{1,0:T(8,128)(2,1)} %weight_ref.3, bf16[128,2048]{1,0:T(8,128)(2,1)} %copy-done.5, f32[1,2048]{1,0:T(1,128)} %bitcast.33, f32[2,128]{1,0:T(2,128)} %get-tuple-element.12.routes_ref), custom_call_target="tpu_custom_call" | custom-call | flops 536870912 | bytes 4194304 | tf_op jit(solution)/shard_map/project/pallas_call | solution.py:152
  49.8 0.0 copy-done.4
  49.8 3.8 %all-to-all-start.3 = ((bf16[16,16,2048]{2,1,0:T(8,128)(2,1)}), bf16[16,16,2048]{2,1,0:T(8,128)(2,1)S(1)}, u32[]{:S(2)}, u32[]{:S(2)}) async-start(bf16[16,16,2048]{2,1,0:T(8,128)(2,1)} %bitcast.26), calls=%async_computation.3 | async-start | bytes 2097152 | tf_op jit(solution)/shard_map/all_to_all | solution.py:288
  53.7 0.6 fusion.1
  54.3 4.7 %project_keep.1 = (bf16[256,2048]{1,0:T(8,128)(2,1)}, bf16[128,2048]{1,0:T(8,128)(2,1)}, bf16[128,2048]{1,0:T(8,128)(2,1)}) custom-call(s32[1]{0:T(128)} %bitcast.first_ref, bf16[2,128,512]{2,1,0:T(8,128)(2,1)} %copy-done.4, bf16[1024,2048]{1,0:T(8,128)(2,1)} %weight_ref.3, bf16[128,2048]{1,0:T(8,128)(2,1)} %residual_ref.1, f32[1,2048]{1,0:T(1,128)} %bitcast.34, ...), custom_call_target="tpu_custom_call" | custom-call | flops 536870912 | bytes 4194304 | tf_op jit(solution)/shard_map/project_keep/pallas_call | solution.py:152
  58.9 10.9 %all-to-all-done.3 = bf16[16,16,2048]{2,1,0:T(8,128)(2,1)S(1)} async-done(((bf16[16,16,2048]{2,1,0:T(8,128)(2,1)}), bf16[16,16,2048]{2,1,0:T(8,128)(2,1)S(1)}, u32[]{:S(2)}, u32[]{:S(2)}) %all-to-all-start.3) | async-done | bytes 1048608 | tf_op jit(solution)/shard_map/all_to_all | solution.py:288
  69.8 3.7 %all-to-all-start.1 = ((bf16[16,16,2048]{2,1,0:T(8,128)(2,1)}), bf16[16,16,2048]{2,1,0:T(8,128)(2,1)S(1)}, u32[]{:S(2)}, u32[]{:S(2)}) async-start(bf16[16,16,2048]{2,1,0:T(8,128)(2,1)} %bitcast.31), calls=%async_computation.1 | async-start | bytes 2097152 | tf_op jit(solution)/shard_map/all_to_all | solution.py:288
  73.5 0.0 copy-done.2
  73.5 5.9 %shard_map.167 = bf16[256,2048]{1,0:T(8,128)(2,1)} custom-call(bf16[256,2048]{1,0:T(8,128)(2,1)} %bitcast.27, bf16[2048,512]{1,0:T(8,128)(2,1)} %bitcast.18, bf16[2048,512]{1,0:T(8,128)(2,1)} %bitcast.20, bf16[512,2048]{1,0:T(8,128)(2,1)} %bitcast.22), custom_call_target="tpu_custom_call" | custom-call | flops 1610612736 | bytes 6291456 | tf_op jit(solution)/shard_map/pallas_call | solution.py:185
  79.4 10.2 %all-to-all-done.1 = bf16[16,16,2048]{2,1,0:T(8,128)(2,1)S(1)} async-done(((bf16[16,16,2048]{2,1,0:T(8,128)(2,1)}), bf16[16,16,2048]{2,1,0:T(8,128)(2,1)S(1)}, u32[]{:S(2)}, u32[]{:S(2)}) %all-to-all-start.1) | async-done | bytes 1048608 | tf_op jit(solution)/shard_map/all_to_all | solution.py:288
  89.6 3.7 %all-to-all-start.4 = ((bf16[16,16,2048]{2,1,0:T(8,128)(2,1)}), bf16[16,16,2048]{2,1,0:T(8,128)(2,1)S(1)}, u32[]{:S(2)}, u32[]{:S(2)}) async-start(bf16[16,16,2048]{2,1,0:T(8,128)(2,1)} %bitcast.30), calls=%async_computation.4 | async-start | bytes 2097152 | tf_op jit(solution)/shard_map/all_to_all | solution.py:288
  93.2 0.0 copy-done.3
  93.2 6.0 %shard_map.164 = bf16[256,2048]{1,0:T(8,128)(2,1)} custom-call(bf16[256,2048]{1,0:T(8,128)(2,1)} %bitcast.29, bf16[2048,512]{1,0:T(8,128)(2,1)} %bitcast.19, bf16[2048,512]{1,0:T(8,128)(2,1)} %bitcast.21, bf16[512,2048]{1,0:T(8,128)(2,1)} %bitcast.23), custom_call_target="tpu_custom_call" | custom-call | flops 1610612736 | bytes 6291456 | tf_op jit(solution)/shard_map/pallas_call | solution.py:185
  99.2 10.1 %all-to-all-done.4 = bf16[16,16,2048]{2,1,0:T(8,128)(2,1)S(1)} async-done(((bf16[16,16,2048]{2,1,0:T(8,128)(2,1)}), bf16[16,16,2048]{2,1,0:T(8,128)(2,1)S(1)}, u32[]{:S(2)}, u32[]{:S(2)}) %all-to-all-start.4) | async-done | bytes 1048608 | tf_op jit(solution)/shard_map/all_to_all | solution.py:288
  109.3 3.7 %all-to-all-start.2 = ((bf16[16,16,2048]{2,1,0:T(8,128)(2,1)}), bf16[16,16,2048]{2,1,0:T(8,128)(2,1)S(1)}, u32[]{:S(2)}, u32[]{:S(2)}) async-start(bf16[16,16,2048]{2,1,0:T(8,128)(2,1)} %bitcast.28), calls=%async_computation.2 | async-start | bytes 2097152 | tf_op jit(solution)/shard_map/all_to_all | solution.py:288
  113.0 0.0 copy-done.1
  113.0 2.7 %shard_map.168 = bf16[128,2048]{1,0:T(8,128)(2,1)} custom-call(s32[1]{0:T(128)} %bitcast.first_ref, f32[2,128]{1,0:T(2,128)} %get-tuple-element.12.routes_ref, f32[2,128]{1,0:T(2,128)} %get-tuple-element.11.weight_ref, bf16[256,2048]{1,0:T(8,128)(2,1)} %bitcast.25), custom_call_target="tpu_custom_call" | custom-call | flops 268435456 | bytes 1048576 | tf_op jit(solution)/shard_map/pallas_call | solution.py:218
  115.7 2.6 %collective-permute-start.4 = (bf16[128,2048]{1,0:T(8,128)(2,1)}, bf16[128,2048]{1,0:T(8,128)(2,1)S(1)}, u32[]{:S(2)}, u32[]{:S(2)}) collective-permute-start(bf16[128,2048]{1,0:T(8,128)(2,1)} %shard_map.168), channel_id=1, source_target_pairs={{0,16},{16,0},{1,17},{17,1},{2,18},{18,2},{3,19},{19,3},{4,20},{20... | collective-permute-start | bytes 1572872 | tf_op jit(solution)/shard_map/ppermute | solution.py:29
  118.2 5.1 %shard_map.165.rest_1_ = f32[128,2048]{1,0:T(8,128)} custom-call(bf16[128,2048]{1,0:T(8,128)(2,1)} %get-tuple-element.10.rows_ref, bf16[2048,512]{1,0:T(8,128)(2,1)} %gate_ref.3, bf16[2048,512]{1,0:T(8,128)(2,1)} %up_ref.1, bf16[512,2048]{1,0:T(8,128)(2,1)} %down_ref.1), custom_call_target="tpu_custom_call" | custom-call | flops 805306368 | bytes 6291456 | tf_op jit(solution)/shard_map/pallas_call | solution.py:185
  123.3 15.3 %all-to-all-done.2 = bf16[16,16,2048]{2,1,0:T(8,128)(2,1)S(1)} async-done(((bf16[16,16,2048]{2,1,0:T(8,128)(2,1)}), bf16[16,16,2048]{2,1,0:T(8,128)(2,1)S(1)}, u32[]{:S(2)}, u32[]{:S(2)}) %all-to-all-start.2) | async-done | bytes 1048608 | tf_op jit(solution)/shard_map/all_to_all | solution.py:288
  138.6 1.0 copy-done
  139.6 3.4 %shard_map.166 = f32[128,2048]{1,0:T(8,128)} custom-call(s32[1]{0:T(128)} %bitcast.first_ref, f32[2,128]{1,0:T(2,128)} %get-tuple-element.14.routes_ref, f32[2,128]{1,0:T(2,128)} %get-tuple-element.13.weight_ref, bf16[256,2048]{1,0:T(8,128)(2,1)} %bitcast.24, bf16[128,2048]{1,0:T(8,128)(2,1)} %get-tuple-element.9.rest_0_, f32[128,2048]{1,0:T(8,128)} %shard_map.165.rest_1_), custom_call_target="tpu_custom_call" | custom-call | flops 268435456 | bytes 1048576 | tf_op jit(solution)/shard_map/pallas_call | solution.py:218
  142.9 0.0 collective-permute-done.4
  142.9 2.1 %add_convert_fusion = bf16[128,2048]{1,0:T(8,128)(2,1)} fusion(f32[128,2048]{1,0:T(8,128)} %shard_map.166, bf16[128,2048]{1,0:T(8,128)(2,1)S(1)} %collective-permute-done.4), kind=kLoop, calls=%fused_computation | loop fusion | flops 786432 | bytes 2097152 | tf_op jit(solution)/shard_map/convert_element_type | solution.py:318
  (9 shorter events, 0.0 us)
Async XLA Ops:
  1.7 9.6 %collective-permute-start = (bf16[32,640]{1,0:T(8,128)(2,1)S(1)}, bf16[32,640]{1,0:T(8,128)(2,1)S(1)}, u32[]{:S(2)}, u32[]{:S(2)}) collective-permute-start(bf16[32,640]{1,0:T(8,128)(2,1)S(1)} %pad_maximum_fusion), channel_id=1, source_target_pairs={{0,2},{2,4},{4,6},{6,8},{8,10},{10,12},{12,14},{14,16},{16,18},{18... | collective-permute-start | bytes 122888 | tf_op jit(solution)/shard_map/ppermute | solution.py:25
  6.6 37.7 %collective-permute-start.3 = (bf16[128,2048]{1,0:T(8,128)(2,1)}, bf16[128,2048]{1,0:T(8,128)(2,1)S(1)}, u32[]{:S(2)}, u32[]{:S(2)}) collective-permute-start(bf16[128,2048]{1,0:T(8,128)(2,1)} %residual_ref.1), channel_id=1, source_target_pairs={{0,16},{16,0},{1,17},{17,1},{2,18},{18,2},{3,19},{19,3},{4,20},{20... | collective-permute-start | bytes 1572872 | tf_op jit(solution)/shard_map/ppermute | solution.py:29
  11.3 0.7 copy-start.8
  12.1 13.2 %copy-start.7 = (f32[128,2]{0,1:T(2,128)S(1)}, f32[128,2]{0,1:T(2,128)}, u32[]{:S(2)}) copy-start(f32[128,2]{0,1:T(2,128)} %param.27) | copy-start | bytes 3076
  22.7 27.2 %copy-start.4 = (bf16[2,128,512]{2,1,0:T(8,128)(2,1)}, bf16[2,128,512]{2,1,0:T(8,128)(2,1)S(1)}, u32[]{:S(2)}) copy-start(bf16[2,128,512]{2,1,0:T(8,128)(2,1)S(1)} %all_to_all.25.act_ref) | copy-start | bytes 786436
  22.7 21.6 %collective-permute-start.2 = (bf16[2,128,512]{2,1,0:T(8,128)(2,1)S(1)}, bf16[2,128,512]{2,1,0:T(8,128)(2,1)S(1)}, u32[]{:S(2)}, u32[]{:S(2)}) collective-permute-start(bf16[2,128,512]{2,1,0:T(8,128)(2,1)S(1)} %all_to_all.25.act_ref), channel_id=1, source_target_pairs={{0,16},{16,0},{1,17},{17,1},{2,18},{18,2},{3,19},{19,3},{4,20},{20... | collective-permute-start | bytes 786440 | tf_op jit(solution)/shard_map/ppermute | solution.py:29
  25.3 18.4 %collective-permute-start.1 = (f32[4,128]{1,0:T(4,128)S(1)}, f32[4,128]{1,0:T(4,128)S(1)}, u32[]{:S(2)}, u32[]{:S(2)}) collective-permute-start(f32[4,128]{1,0:T(4,128)S(1)} %maximum_bitcast_fusion), channel_id=1, source_target_pairs={{0,16},{16,0},{1,17},{17,1},{2,18},{18,2},{3,19},{19,3},{4,20},{20... | collective-permute-start | bytes 6152 | tf_op jit(solution)/shard_map/ppermute | solution.py:29
  44.3 0.7 copy-start.6
  44.3 0.9 copy-start.5
  49.8 20.0 %all-to-all-start.3 = ((bf16[16,16,2048]{2,1,0:T(8,128)(2,1)}), bf16[16,16,2048]{2,1,0:T(8,128)(2,1)S(1)}, u32[]{:S(2)}, u32[]{:S(2)}) async-start(bf16[16,16,2048]{2,1,0:T(8,128)(2,1)} %bitcast.26), calls=%async_computation.3 | async-start | bytes 2097152 | tf_op jit(solution)/shard_map/all_to_all | solution.py:288
  69.8 3.7 %copy-start.2 = (bf16[16,16,2048]{2,1,0:T(8,128)(2,1)}, bf16[16,16,2048]{2,1,0:T(8,128)(2,1)S(1)}, u32[]{:S(2)}) copy-start(bf16[16,16,2048]{2,1,0:T(8,128)(2,1)S(1)} %all-to-all-done.3) | copy-start | bytes 3145732
  69.8 19.8 %all-to-all-start.1 = ((bf16[16,16,2048]{2,1,0:T(8,128)(2,1)}), bf16[16,16,2048]{2,1,0:T(8,128)(2,1)S(1)}, u32[]{:S(2)}, u32[]{:S(2)}) async-start(bf16[16,16,2048]{2,1,0:T(8,128)(2,1)} %bitcast.31), calls=%async_computation.1 | async-start | bytes 2097152 | tf_op jit(solution)/shard_map/all_to_all | solution.py:288
  89.6 3.7 %copy-start.3 = (bf16[16,16,2048]{2,1,0:T(8,128)(2,1)}, bf16[16,16,2048]{2,1,0:T(8,128)(2,1)S(1)}, u32[]{:S(2)}) copy-start(bf16[16,16,2048]{2,1,0:T(8,128)(2,1)S(1)} %all-to-all-done.1) | copy-start | bytes 3145732
  89.6 19.8 %all-to-all-start.4 = ((bf16[16,16,2048]{2,1,0:T(8,128)(2,1)}), bf16[16,16,2048]{2,1,0:T(8,128)(2,1)S(1)}, u32[]{:S(2)}, u32[]{:S(2)}) async-start(bf16[16,16,2048]{2,1,0:T(8,128)(2,1)} %bitcast.30), calls=%async_computation.4 | async-start | bytes 2097152 | tf_op jit(solution)/shard_map/all_to_all | solution.py:288
  109.3 3.7 %copy-start.1 = (bf16[16,16,2048]{2,1,0:T(8,128)(2,1)}, bf16[16,16,2048]{2,1,0:T(8,128)(2,1)S(1)}, u32[]{:S(2)}) copy-start(bf16[16,16,2048]{2,1,0:T(8,128)(2,1)S(1)} %all-to-all-done.4) | copy-start | bytes 3145732
  109.3 29.2 %all-to-all-start.2 = ((bf16[16,16,2048]{2,1,0:T(8,128)(2,1)}), bf16[16,16,2048]{2,1,0:T(8,128)(2,1)S(1)}, u32[]{:S(2)}, u32[]{:S(2)}) async-start(bf16[16,16,2048]{2,1,0:T(8,128)(2,1)} %bitcast.28), calls=%async_computation.2 | async-start | bytes 2097152 | tf_op jit(solution)/shard_map/all_to_all | solution.py:288
  115.7 27.2 %collective-permute-start.4 = (bf16[128,2048]{1,0:T(8,128)(2,1)}, bf16[128,2048]{1,0:T(8,128)(2,1)S(1)}, u32[]{:S(2)}, u32[]{:S(2)}) collective-permute-start(bf16[128,2048]{1,0:T(8,128)(2,1)} %shard_map.168), channel_id=1, source_target_pairs={{0,16},{16,0},{1,17},{17,1},{2,18},{18,2},{3,19},{19,3},{4,20},{20... | collective-permute-start | bytes 1572872 | tf_op jit(solution)/shard_map/ppermute | solution.py:29
  138.6 1.0 copy-start

commit v2 on v1

v2 whole, which is shorter than its diff:
```python
import functools

import jax
import jax.numpy as jnp
from jax import lax
from jax.experimental import pallas as pl
from jax.experimental.pallas import tpu as pltpu
from jax.sharding import Mesh
from jax.sharding import PartitionSpec as P

LANES = 128


epsilon = 1e-06

HALF = ("sp", "tp")
LINE = ("half", "sp")

F32, BF16, I32 = jnp.float32, jnp.bfloat16, jnp.int32


def from_behind(x, axis, by):
    peers = lax.axis_size(axis)
    pairs = [(i, i + by) for i in range(peers) if 0 <= i + by < peers]
    return lax.ppermute(x, axis, pairs)


def to_mirror(x):
    return lax.ppermute(x, "half", [(0, 1), (1, 0)])


def glu_of(value, gate):
    return (value.astype(F32) * jax.nn.sigmoid(gate.astype(F32))).astype(BF16)


def cost(flops, moved):
    return pl.CostEstimate(
        flops=int(flops), bytes_accessed=int(moved), transcendentals=0
    )


def column_of(row, count, start):
    across = lax.broadcasted_iota(I32, (count, LANES), 1)
    down = lax.broadcasted_iota(I32, (count, LANES), 0)
    picked = jnp.where(across == down + start, row, 0.0)
    return jnp.broadcast_to(jnp.sum(picked, axis=1, keepdims=True), (count, LANES))


def edge_body(value_ref, gate_ref, ids_ref, routes_ref, weight_ref, edge_ref, meta_ref):
    rim, channels = value_ref.shape
    top = routes_ref.shape[0]
    edge_ref[:, pl.ds(0, channels)] = glu_of(value_ref[...], gate_ref[...])
    edge_ref[:, pl.ds(channels, LANES)] = column_of(
        ids_ref[...].astype(F32), rim, LANES - rim
    ).astype(BF16)
    meta_ref[pl.ds(0, top), :] = routes_ref[...].astype(F32)
    meta_ref[pl.ds(top, top), :] = weight_ref[...]


def edge_of(value, gate, ids, routes, weight, rim):
    positions, channels = value.shape
    top, tokens = routes.shape
    tail = pl.BlockSpec((rim, channels), lambda i: (positions // rim - 1, 0))
    whole = pl.BlockSpec((top, tokens), lambda i: (0, 0))
    return pl.pallas_call(
        edge_body,
        grid=(1,),
        out_shape=(
            jax.ShapeDtypeStruct((rim, channels + LANES), BF16),
            jax.ShapeDtypeStruct((2 * top, tokens), F32),
        ),
        in_specs=[
            tail,
            tail,
            pl.BlockSpec((1, LANES), lambda i: (0, positions // LANES - 1)),
            whole,
            whole,
        ],
        out_specs=(
            pl.BlockSpec((rim, channels + LANES), lambda i: (0, 0)),
            pl.BlockSpec((2 * top, tokens), lambda i: (0, 0)),
        ),
        cost_estimate=cost(1e6, 1e5),
        name="edge",
    )(value, gate, ids, routes, weight)


def conv_body(
    core_ref,
    value_ref,
    gate_ref,
    edge_ref,
    ids_ref,
    taps_ref,
    gain_ref,
    shift_ref,
    keep_ref,
    send_ref,
    glu,
    ids,
    weights,
):
    positions, channels = value_ref.shape
    width = taps_ref.shape[0]
    rim = edge_ref.shape[0]
    blocks = channels // LANES
    rows = 32
    tokens = keep_ref.shape[0]
    weights[pl.ds(0, width), :] = taps_ref[...].astype(F32)
    ids[pl.ds(0, rim), :] = edge_ref[:, pl.ds(channels, LANES)].astype(F32)
    for start in range(0, positions, LANES):
        row = ids_ref[:, pl.ds(start, LANES)].astype(F32)
        ids[pl.ds(rim + start, LANES), :] = column_of(row, LANES, 0)
    for c in range(blocks):
        lanes = pl.ds(c * LANES, LANES)
        glu[c, pl.ds(0, rim), :] = edge_ref[:, lanes].astype(F32)
        glu[c, pl.ds(rim, positions), :] = glu_of(value_ref[:, lanes], gate_ref[:, lanes]).astype(
            F32
        )

    def chunk(out_ref, base, index):
        inside = pl.multiple_of(index * rows, rows)
        row = pl.multiple_of(base + inside, rows)
        here = ids[pl.ds(row + rim, rows), :]
        total = [jnp.zeros((rows, LANES), F32) for _ in range(blocks)]
        for tap in range(width):
            past = row + (rim - width + 1 + tap)
            same = ids[pl.ds(past, rows), :] == here
            for c in range(blocks):
                weight = weights[pl.ds(tap, 1), pl.ds(c * LANES, LANES)]
                term = weight * glu[c, pl.ds(past, rows), :]
                total[c] = total[c] + jnp.where(same, term, 0.0)
        for c in range(blocks):
            lanes = pl.ds(c * LANES, LANES)
            centered = total[c] - jnp.mean(total[c], axis=-1, keepdims=True)
            spread = jnp.mean(centered * centered, axis=-1, keepdims=True)
            scaled = centered * lax.rsqrt(spread + epsilon)
            out_ref[pl.ds(inside, rows), lanes] = jax.nn.silu(
                scaled * gain_ref[:, lanes] + shift_ref[:, lanes]
            ).astype(BF16)

    core = core_ref[0]
    parts = positions // tokens
    for out_ref, part in ((send_ref, parts - 1 - core), (keep_ref, core)):
        base = pl.multiple_of(part * tokens, tokens)

        def step(index, carry, out_ref=out_ref, base=base):
            chunk(out_ref, base, index)
            return carry

        lax.fori_loop(0, tokens // rows, step, 0)


def convolve(core, value, gate, edge, ids, taps, gain, shift, tokens):
    positions, channels = value.shape
    rim = edge.shape[0]
    half = jax.ShapeDtypeStruct((tokens, channels), BF16)
    return pl.pallas_call(
        conv_body,
        out_shape=(half, half),
        in_specs=[pl.BlockSpec(memory_space=pltpu.SMEM)]
        + [pl.BlockSpec(memory_space=pltpu.VMEM)] * 7,
        scratch_shapes=[
            pltpu.VMEM((channels // LANES, rim + positions, LANES), F32),
            pltpu.VMEM((rim + positions, LANES), F32),
            pltpu.VMEM((-(-taps.shape[0] // 8) * 8, channels), F32),
        ],
        cost_estimate=cost(6e9, 6 * value.size),
        name="conv",
    )(core, value, gate, edge, ids, taps, gain, shift)


def selection(routes, first, experts, capacity, rows):
    top, tokens = routes.shape
    routes = routes.astype(I32)
    names = lax.broadcasted_iota(I32, (experts, tokens), 0)
    earlier = lax.broadcasted_iota(I32, (tokens, tokens), 0) < lax.broadcasted_iota(
        I32, (tokens, tokens), 1
    )
    earlier = earlier.astype(F32).astype(BF16)
    index = lax.broadcasted_iota(I32, (rows, tokens), 0)
    used = jnp.zeros((experts, 1), F32)
    picks = []
    for k in range(top):
        route = routes[k : k + 1, :]
        chosen = (names == route).astype(F32)
        before = jnp.dot(chosen.astype(BF16), earlier, preferred_element_type=F32) + used
        slot = jnp.sum(chosen * before, axis=0, keepdims=True).astype(I32)
        picks.append(index == (route - first) * capacity + slot)
        used = used + jnp.sum(chosen, axis=1, keepdims=True)
    return picks


def chosen_of(picks):
    return functools.reduce(jnp.logical_or, picks).astype(F32).astype(BF16)


def project_body(
    shape_of,
    first_ref,
    core_ref,
    keep_ref,
    got_ref,
    weight_hbm,
    residual_ref,
    gain_ref,
    meta_ref,
    parcel_ref,
    stream_ref,
    normed_ref,
    weight,
    total,
    sems,
):
    experts, capacity, top = shape_of
    depth = keep_ref.shape[1]
    chunks = weight.shape[0]
    step = weight.shape[1]
    core = core_ref[0]
    copies = []
    for index in range(chunks):
        part, inside = divmod(index * step, depth)
        owner = core if part == 0 else 1 - core
        start = pl.multiple_of(owner * depth + inside, step)
        copy = pltpu.make_async_copy(
            weight_hbm.at[pl.ds(start, step), :], weight.at[index], sems.at[index]
        )
        copy.start()
        copies.append(copy)
    picks = selection(
        meta_ref[pl.ds(0, top), :], first_ref[0], experts, capacity, parcel_ref.shape[0]
    )
    chosen = chosen_of(picks)
    total[...] = residual_ref[...].astype(F32)
    for index, copy in enumerate(copies):
        part, inside = divmod(index * step, depth)
        act = (keep_ref if part == 0 else got_ref)[:, pl.ds(inside, step)]
        copy.wait()
        total[...] += jnp.dot(act, weight[index], preferred_element_type=F32)
    stream = total[...].astype(BF16)
    wide = stream.astype(F32)
    normed = (
        wide * lax.rsqrt(jnp.mean(wide * wide, axis=-1, keepdims=True) + epsilon) * gain_ref[...]
    ).astype(BF16)
    stream_ref[...] = stream
    normed_ref[...] = normed
    parcel_ref[...] = jnp.dot(chosen, normed, preferred_element_type=F32).astype(BF16)


def project(first, core, keep, got, weight, residual, gain, meta, sizes, rows):
    tokens, width = residual.shape
    depth = keep.shape[1]
    step = depth // 2
    chunks = 2 * depth // step
    out = jax.ShapeDtypeStruct((tokens, width), BF16)
    smem = pl.BlockSpec(memory_space=pltpu.SMEM)
    vmem = pl.BlockSpec(memory_space=pltpu.VMEM)
    return pl.pallas_call(
        functools.partial(project_body, sizes),
        out_shape=(jax.ShapeDtypeStruct((rows, width), BF16), out, out),
        in_specs=[smem, smem, vmem, vmem, pl.BlockSpec(memory_space=pl.ANY), vmem, vmem, vmem],
        out_specs=[vmem] * 3,
        scratch_shapes=[
            pltpu.VMEM((chunks, step, width), BF16),
            pltpu.VMEM((tokens, width), F32),
            pltpu.SemaphoreType.DMA((chunks,)),
        ],
        cost_estimate=cost(2 * tokens * weight.size, 2 * weight.size),
        name="project",
    )(first, core, keep, got, weight, residual, gain, meta)


def gather_body(shape_of, first_ref, meta_ref, rows_ref, parcel_ref, chosen):
    experts, capacity, top = shape_of

    @pl.when(pl.program_id(0) == 0)
    def _():
        picks = selection(
            meta_ref[pl.ds(0, top), :], first_ref[0], experts, capacity, parcel_ref.shape[0]
        )
        chosen[...] = chosen_of(picks)

    parcel_ref[...] = jnp.dot(chosen[...], rows_ref[...], preferred_element_type=F32).astype(BF16)


def gather(first, meta, rows, sizes, count):
    tokens, width = rows.shape
    tile = width // 2
    return pl.pallas_call(
        functools.partial(gather_body, sizes),
        grid=(width // tile,),
        out_shape=jax.ShapeDtypeStruct((count, width), BF16),
        in_specs=[
            pl.BlockSpec(memory_space=pltpu.SMEM),
            pl.BlockSpec(meta.shape, lambda n: (0, 0)),
            pl.BlockSpec((tokens, tile), lambda n: (0, n)),
        ],
        out_specs=pl.BlockSpec((count, tile), lambda n: (0, n)),
        scratch_shapes=[pltpu.VMEM((count, tokens), BF16)],
        cost_estimate=cost(2 * count * tokens * width, 2 * (count + tokens) * width),
        name="gather",
    )(first, meta, rows)


def mlp_body(
    steps,
    rows_hbm,
    gate_hbm,
    up_hbm,
    down_hbm,
    *rest,
):
    extra = rest[:-11]
    (out_hbm, rows, gate, up, down, total_gate, total_up, hidden, out, in_sems, out_sems) = rest[
        -11:
    ]
    depth = gate.shape[0] // steps
    tile = down.shape[1] // steps
    rows_copy = pltpu.make_async_copy(rows_hbm, rows, in_sems.at[0])
    rows_copy.start()
    wide, narrow = [], []
    for n in range(steps):
        part = pl.ds(n * depth, depth)
        pair = (
            pltpu.make_async_copy(gate_hbm.at[part, :], gate.at[part, :], in_sems.at[1 + 3 * n]),
            pltpu.make_async_copy(up_hbm.at[part, :], up.at[part, :], in_sems.at[2 + 3 * n]),
        )
        for copy in pair:
            copy.start()
        wide.append(pair)
    for n in range(steps):
        cols = pl.ds(n * tile, tile)
        copy = pltpu.make_async_copy(down_hbm.at[:, cols], down.at[:, cols], in_sems.at[3 + 3 * n])
        copy.start()
        narrow.append(copy)
    rows_copy.wait()
    for n, pair in enumerate(wide):
        part = pl.ds(n * depth, depth)
        for copy, weight, total in zip(pair, (gate, up), (total_gate, total_up)):
            copy.wait()
            product = jnp.dot(rows[:, part], weight[part, :], preferred_element_type=F32)
            total[...] = product if n == 0 else total[...] + product
    hidden[...] = (jax.nn.silu(total_gate[...]) * total_up[...]).astype(BF16)
    back = []
    for n, copy in enumerate(narrow):
        cols = pl.ds(n * tile, tile)
        copy.wait()
        result = jnp.dot(hidden[...], down[:, cols], preferred_element_type=F32)
        for ref in extra:
            result = result + ref[:, cols].astype(F32)
        out[:, cols] = result.astype(out.dtype)
        copy = pltpu.make_async_copy(out.at[:, cols], out_hbm.at[:, cols], out_sems.at[n])
        copy.start()
        back.append(copy)
    for copy in back:
        copy.wait()


def gated_mlp(rows, gate, up, down, extra, dtype):
    count, width = rows.shape
    inner = gate.shape[-1]
    steps = 4
    anywhere = pl.BlockSpec(memory_space=pl.ANY)
    return pl.pallas_call(
        functools.partial(mlp_body, steps),
        out_shape=jax.ShapeDtypeStruct((count, width), dtype),
        in_specs=[anywhere] * 4 + [pl.BlockSpec(memory_space=pltpu.VMEM)] * len(extra),
        out_specs=anywhere,
        scratch_shapes=[
            pltpu.VMEM((count, width), rows.dtype),
            pltpu.VMEM((width, inner), gate.dtype),
            pltpu.VMEM((width, inner), up.dtype),
            pltpu.VMEM((inner, width), down.dtype),
            pltpu.VMEM((count, inner), F32),
            pltpu.VMEM((count, inner), F32),
            pltpu.VMEM((count, inner), BF16),
            pltpu.VMEM((count, width), dtype),
            pltpu.SemaphoreType.DMA((1 + 3 * steps,)),
            pltpu.SemaphoreType.DMA((steps,)),
        ],
        cost_estimate=cost(6 * count * width * inner, 6 * width * inner),
    )(rows, gate, up, down, *extra)


def combine_body(shape_of, first_ref, meta_ref, back_ref, *rest):
    experts, capacity, top = shape_of
    out_ref, high, low = rest[-3:]

    @pl.when(pl.program_id(0) == 0)
    def _():
        rows = back_ref.shape[0]
        picks = selection(meta_ref[pl.ds(0, top), :], first_ref[0], experts, capacity, rows)
        table = jnp.zeros((rows, meta_ref.shape[1]), F32)
        for k, pick in enumerate(picks):
            table = table + jnp.where(pick, meta_ref[pl.ds(top + k, 1), :], 0.0)
        table = table.T
        high[...] = table.astype(BF16)
        low[...] = (table - table.astype(BF16).astype(F32)).astype(BF16)

    back = back_ref[...]
    total = jnp.dot(high[...], back, preferred_element_type=F32)
    total = total + jnp.dot(low[...], back, preferred_element_type=F32)
    for ref in rest[:-3]:
        total = total + ref[...].astype(F32)
    out_ref[...] = total.astype(out_ref.dtype)


def combine(first, meta, back, sizes, extra):
    rows, width = back.shape
    tokens = meta.shape[1]
    tile = width // 2
    row = pl.BlockSpec((tokens, tile), lambda n: (0, n))
    return pl.pallas_call(
        functools.partial(combine_body, sizes),
        grid=(width // tile,),
        out_shape=jax.ShapeDtypeStruct((tokens, width), BF16),
        in_specs=[
            pl.BlockSpec(memory_space=pltpu.SMEM),
            pl.BlockSpec(meta.shape, lambda n: (0, 0)),
            pl.BlockSpec((rows, tile), lambda n: (0, n)),
        ]
        + [row] * len(extra),
        out_specs=row,
        scratch_shapes=[pltpu.VMEM((tokens, rows), BF16)] * 2,
        cost_estimate=cost(4 * tokens * rows * width, 2 * rows * width),
    )(first, meta, back, *extra)


def per_device(
    conv_value,
    conv_gate,
    taps,
    doc_ids,
    gn_gain,
    gn_shift,
    conv_out,
    residual,
    norm_gain,
    routes,
    route_weight,
    expert_gate,
    expert_up,
    expert_down,
    shared_gate,
    shared_up,
    shared_down,
):
    kernel_width = taps.shape[0]
    model_width = residual.shape[1]
    token_count, top_count = routes.shape
    half_devices = lax.axis_size("sp") * lax.axis_size("tp")
    local_experts = expert_gate.shape[0]
    half_experts = local_experts * half_devices
    experts = half_experts * lax.axis_size("half")
    capacity = 2 * token_count * top_count // experts
    half_rows = half_experts * capacity
    first = (lax.axis_index("half").astype(I32) * half_experts).reshape(1)
    core = lax.axis_index("tp").astype(I32).reshape(1)
    sizes = (experts, capacity, top_count)

    rim = -(-(kernel_width - 1) // 16) * 16
    ids = doc_ids[None, :]
    own_edge, own_meta = edge_of(conv_value, conv_gate, ids, routes.T, route_weight.T, rim)
    edge = from_behind(own_edge, LINE, 1)
    mirror_meta = to_mirror(own_meta)
    keep, send = convolve(
        core,
        conv_value,
        conv_gate,
        edge,
        ids,
        taps,
        gn_gain[None, :],
        gn_shift[None, :],
        token_count,
    )
    got = lax.ppermute(send, "tp", [(0, 1), (1, 0)])
    parcel, stream, normed = project(
        first, core, keep, got, conv_out, residual, norm_gain[None, :], own_meta, sizes, half_rows
    )
    mirror_normed = to_mirror(normed)

    def exchange(rows):
        parcel = rows.reshape(half_devices, local_experts * capacity, model_width)
        arrived = lax.all_to_all(parcel, HALF, split_axis=0, concat_axis=0, tiled=True)
        return arrived.reshape(half_rows, model_width)

    def experts_on(rows):
        split = rows.reshape(half_devices, local_experts, capacity, model_width)
        results = []
        for e in range(local_experts):
            mine = split[:, e].reshape(half_devices * capacity, model_width)
            result = gated_mlp(mine, expert_gate[e], expert_up[e], expert_down[e], (), BF16)
            results.append(result.reshape(half_devices, capacity, model_width))
        return jnp.stack(results, axis=1)

    own_arrived = exchange(parcel)
    mirror_parcel = gather(first, mirror_meta, mirror_normed, sizes, half_rows)
    mirror_arrived = exchange(mirror_parcel)
    base = gated_mlp(normed, shared_gate, shared_up, shared_down, (stream,), F32)
    own_result = experts_on(own_arrived)
    mirror_result = experts_on(mirror_arrived)
    mirror_back = exchange(mirror_result)
    partial = combine(first, mirror_meta, mirror_back, sizes, ())
    other_part = to_mirror(partial)
    own_back = exchange(own_result)
    return combine(first, own_meta, own_back, sizes, (base, other_part))


def solution(mesh):
    sequence_split, core_split = mesh.devices.shape
    folded = Mesh(
        mesh.devices.reshape(2, sequence_split // 2, core_split), ("half", "sp", "tp")
    )
    line, everyone = LINE, LINE + ("tp",)
    return jax.shard_map(
        per_device,
        mesh=folded,
        in_specs=(
            P(line, "tp"),
            P(line, "tp"),
            P(None, "tp"),
            P(line),
            P("tp"),
            P("tp"),
            P(),
            P(everyone, None),
            P(),
            P(everyone, None),
            P(everyone, None),
            P(everyone, None, None),
            P(everyone, None, None),
            P(everyone, None, None),
            P(),
            P(),
            P(),
        ),
        out_specs=P(everyone, None),
        check_vma=False,
    )
```

time: 146 us -> 152 us (1.041)
  blocking collectives: 4.98 us -> 20.5 us
  other arithmetic: 5.76 us -> 0 us
  starting transfers between devices: 27.9 us -> 22.4 us
  waiting for transfers between devices: 64.5 us -> 68.7 us
  Pallas kernels: 38 us -> 36.4 us
    all_to_all x1, blocking collectives: 4.98 us -> 20.5 us  [exchange(): lax.all_to_all(parcel, HALF, split_axis=0, concat_axis=0, tiled=True)]
    ppermute x4 -> x3, waiting for transfers between devices: 18.1 us -> 28.5 us  [to_mirror(): return lax.ppermute(x, 'half', [(0, 1), (1, 0)])]
    all_to_all x4 -> x3, waiting for transfers between devices: 46.4 us -> 36.6 us  [exchange(): lax.all_to_all(parcel, HALF, split_axis=0, concat_axis=0, tiled=True)]
    convert_element_type x5 -> x0, other arithmetic: 5.75 us -> none  [the longest x1 2.13 us: per_device(): return (own_part + other_part.astype(F32)).astype(BF16)]
    all_to_all x4 -> x3, starting transfers between devices: 14.8 us -> 11 us  [exchange(): lax.all_to_all(parcel, HALF, split_axis=0, concat_axis=0, tiled=True)]
    ppermute x1, waiting for transfers between devices: 0.01 us -> 1.97 us  [from_behind(): return lax.ppermute(x, axis, pairs)]
    ppermute x4 -> x3, starting transfers between devices: 8.2 us -> 6.6 us  [to_mirror(): return lax.ppermute(x, 'half', [(0, 1), (1, 0)])]
    pallas_call x8 -> x9, Pallas kernels: 38 us -> 36.4 us  [the longest x3 15.9 us: gated_mlp(): pl.pallas_call(functools.partial(mlp_body, steps), out_shape=jax.ShapeDty...]
  transfers between devices with their start and end apart: 9 -> 8, of which waited for: 5 -> 7; matrix products, arithmetic and copies ran while one was open for 3% -> 0% of each run, Pallas kernels for 23% -> 12%
where the time goes in v2:
time: 152 us; the launch traced here: 151 us
  waiting for transfers between devices  68.7 us (45%)
  Pallas kernels  36.4 us (24%)
  starting transfers between devices  22.4 us (15%)
  blocking collectives  20.5 us (13%)
  local copies, waits for them, and re-layouts  3.43 us (2%)
    all_to_all x3, waiting for transfers between devices, exchange(): lax.all_to_all(parcel, HALF, split_axis=0, concat_axis=0, tiled=True)  36.6 us
    ppermute x3, waiting for transfers between devices, to_mirror(): return lax.ppermute(x, 'half', [(0, 1), (1, 0)])  28.5 us
    all_to_all x1, blocking collectives, exchange(): lax.all_to_all(parcel, HALF, split_axis=0, concat_axis=0, tiled=True)  20.5 us
    pallas_call x3, Pallas kernels, gated_mlp(): pl.pallas_call(functools.partial(mlp_body, steps), out_shape=jax.ShapeDty...  15.9 us
    all_to_all x3, starting transfers between devices, exchange(): lax.all_to_all(parcel, HALF, split_axis=0, concat_axis=0, tiled=True)  11 us
    ppermute x3, starting transfers between devices, to_mirror(): return lax.ppermute(x, 'half', [(0, 1), (1, 0)])  6.6 us
    pallas_call x1, Pallas kernels, convolve(): pl.pallas_call(conv_body, out_shape=(half, half), in_specs=[pl.BlockSpec(...  5.63 us
    pallas_call x2, Pallas kernels, combine(): pl.pallas_call(functools.partial(combine_body, sizes), grid=(width // til...  5.59 us
  transfers between devices with their start and end apart: 8, of which 7 were waited for; matrix products, arithmetic and copies ran while one was open for 0% of the time, Pallas kernels for 12%

profile of v2, /device:TPU:0, one launch (start us, length us, event | category | flops | bytes accessed | tf_op | source)
XLA Modules:
  0.0 151.4 jit_solution(6741745586929049628)
XLA Ops:
  0.0 1.5 edge.1
  1.5 4.9 %collective-permute-start = (bf16[32,640]{1,0:T(8,128)(2,1)}, bf16[32,640]{1,0:T(8,128)(2,1)S(1)}, u32[]{:S(2)}, u32[]{:S(2)}) collective-permute-start(bf16[32,640]{1,0:T(8,128)(2,1)} %get-tuple-element.13), channel_id=1, source_target_pairs={{0,2},{2,4},{4,6},{6,8},{8,10},{10,12},{12,14},{14,16},{16,18},{18... | collective-permute-start | bytes 122888 | tf_op jit(solution)/shard_map/ppermute | solution.py:25
  6.4 2.0 %collective-permute-done.edge_ref = bf16[32,640]{1,0:T(8,128)(2,1)S(1)} collective-permute-done((bf16[32,640]{1,0:T(8,128)(2,1)}, bf16[32,640]{1,0:T(8,128)(2,1)S(1)}, u32[]{:S(2)}, u32[]{:S(2)}) %collective-permute-start) | collective-permute-done | bytes 40992 | tf_op jit(solution)/shard_map/ppermute | solution.py:25
  8.3 0.0 copy-start.8
  8.3 0.6 copy-done.8
  8.9 5.6 %conv.1 = (bf16[128,512]{1,0:T(8,128)(2,1)}, bf16[128,512]{1,0:T(8,128)(2,1)}) custom-call(s32[1]{0:T(128)} %bitcast.4.core_ref, bf16[256,512]{1,0:T(8,128)(2,1)} %value_ref.3, bf16[256,512]{1,0:T(8,128)(2,1)} %gate_ref.3, bf16[32,640]{1,0:T(8,128)(2,1)} %copy-done.8, s32[1,256]{1,0:T(1,128)} %bitcast.36, bf16[31,512]{1,0:T(8,128)(2,1)} %taps_ref.1, ...), custom_call_target="tpu_custom_call" | custom-call | flops 6000000000 | bytes 786432 | tf_op jit(solution)/shard_map/conv/pallas_call | solution.py:158
  14.6 0.0 collective-permute-start.1
  14.6 1.6 %collective-permute-done.1.got_ref = bf16[128,512]{1,0:T(8,128)(2,1)S(1)} collective-permute-done((bf16[128,512]{1,0:T(8,128)(2,1)}, bf16[128,512]{1,0:T(8,128)(2,1)S(1)}, u32[]{:S(2)}, u32[]{:S(2)}) %collective-permute-start.1) | collective-permute-done | bytes 131104 | tf_op jit(solution)/shard_map/ppermute | solution.py:477
  16.1 0.0 copy-start.5
  16.1 0.6 copy-done.5
  16.8 0.0 copy-start.6
  16.8 5.3 %project.1 = (bf16[256,2048]{1,0:T(8,128)(2,1)}, bf16[128,2048]{1,0:T(8,128)(2,1)}, bf16[128,2048]{1,0:T(8,128)(2,1)}) custom-call(s32[1]{0:T(128)} %bitcast.first_ref, s32[1]{0:T(128)} %bitcast.4.core_ref, bf16[128,512]{1,0:T(8,128)(2,1)} %get-tuple-element.14.keep_ref, bf16[128,512]{1,0:T(8,128)(2,1)} %copy-done.5, bf16[1024,2048]{1,0:T(8,128)(2,1)} %weight_hbm.1, ...), custom_call_target="tpu_custom_call" | custom-call | flops 536870912 | bytes 4194304 | tf_op jit(solution)/shard_map/project/pallas_call | solution.py:258
  22.1 5.2 %collective-permute-start.3 = (bf16[128,2048]{1,0:T(8,128)(2,1)}, bf16[128,2048]{1,0:T(8,128)(2,1)S(1)}, u32[]{:S(2)}, u32[]{:S(2)}) collective-permute-start(bf16[128,2048]{1,0:T(8,128)(2,1)} %get-tuple-element.17.rows_hbm), channel_id=1, source_target_pairs={{0,16},{16,0},{1,17},{17,1},{2,18},{18,2},{3,19},{19,3},{4,20},{20... | collective-permute-start | bytes 1572872 | tf_op jit(solution)/shard_map/ppermute | solution.py:29
  27.3 0.0 copy-done.6
  27.3 0.1 collective-permute-start.2
  27.3 23.7 %collective-permute-done.2.meta_ref = f32[4,128]{1,0:T(4,128)S(1)} collective-permute-done((f32[4,128]{1,0:T(4,128)S(1)}, f32[4,128]{1,0:T(4,128)S(1)}, u32[]{:S(2)}, u32[]{:S(2)}) %collective-permute-start.2) | collective-permute-done | bytes 2080 | tf_op jit(solution)/shard_map/ppermute | solution.py:29
  51.0 0.0 copy-start.7
  51.0 0.0 collective-permute-done.3.rows_ref
  51.0 0.6 copy-done.7
  51.6 0.0 copy-start.3
  51.6 0.8 copy-done.3
  52.4 2.5 %gather.1 = bf16[256,2048]{1,0:T(8,128)(2,1)} custom-call(s32[1]{0:T(128)} %bitcast.first_ref, f32[4,128]{1,0:T(4,128)} %copy-done.7, bf16[128,2048]{1,0:T(8,128)(2,1)} %copy-done.3), custom_call_target="tpu_custom_call" | custom-call | flops 134217728 | bytes 1572864 | tf_op jit(solution)/shard_map/gather/pallas_call | solution.py:289
  54.9 20.5 %all_to_all.20 = bf16[16,16,2048]{2,1,0:T(8,128)(2,1)} all-to-all(bf16[16,16,2048]{2,1,0:T(8,128)(2,1)} %bitcast.27), channel_id=1, replica_groups=mesh['half'=2,'sp'=8,'tp'=2] {'sp','tp'}, dimensions={0} | all-to-all | bytes 2097152 | tf_op jit(solution)/shard_map/all_to_all | solution.py:485
  75.4 3.7 %all-to-all-start = ((bf16[16,16,2048]{2,1,0:T(8,128)(2,1)}), bf16[16,16,2048]{2,1,0:T(8,128)(2,1)S(1)}, u32[]{:S(2)}, u32[]{:S(2)}) async-start(bf16[16,16,2048]{2,1,0:T(8,128)(2,1)} %bitcast.8), calls=%async_computation | async-start | bytes 2097152 | tf_op jit(solution)/shard_map/all_to_all | solution.py:485
  79.0 5.2 %shard_map.165 = bf16[256,2048]{1,0:T(8,128)(2,1)} custom-call(bf16[256,2048]{1,0:T(8,128)(2,1)} %bitcast.31, bf16[2048,512]{1,0:T(8,128)(2,1)} %bitcast.19, bf16[2048,512]{1,0:T(8,128)(2,1)} %bitcast.21, bf16[512,2048]{1,0:T(8,128)(2,1)} %bitcast.23), custom_call_target="tpu_custom_call" | custom-call | flops 1610612736 | bytes 6291456 | tf_op jit(solution)/shard_map/pallas_call | solution.py:364
  84.3 10.9 %all-to-all-done = bf16[16,16,2048]{2,1,0:T(8,128)(2,1)S(1)} async-done(((bf16[16,16,2048]{2,1,0:T(8,128)(2,1)}), bf16[16,16,2048]{2,1,0:T(8,128)(2,1)S(1)}, u32[]{:S(2)}, u32[]{:S(2)}) %all-to-all-start) | async-done | bytes 1048608 | tf_op jit(solution)/shard_map/all_to_all | solution.py:485
  95.1 0.0 copy-start.2
  95.1 3.7 %all-to-all-start.3 = ((bf16[16,16,2048]{2,1,0:T(8,128)(2,1)}), bf16[16,16,2048]{2,1,0:T(8,128)(2,1)S(1)}, u32[]{:S(2)}, u32[]{:S(2)}) async-start(bf16[16,16,2048]{2,1,0:T(8,128)(2,1)} %bitcast.30), calls=%async_computation.3 | async-start | bytes 2097152 | tf_op jit(solution)/shard_map/all_to_all | solution.py:485
  98.8 0.0 copy-done.2
  98.8 5.2 %shard_map.163 = bf16[256,2048]{1,0:T(8,128)(2,1)} custom-call(bf16[256,2048]{1,0:T(8,128)(2,1)} %bitcast.29, bf16[2048,512]{1,0:T(8,128)(2,1)} %bitcast.20, bf16[2048,512]{1,0:T(8,128)(2,1)} %bitcast.22, bf16[512,2048]{1,0:T(8,128)(2,1)} %bitcast.24), custom_call_target="tpu_custom_call" | custom-call | flops 1610612736 | bytes 6291456 | tf_op jit(solution)/shard_map/pallas_call | solution.py:364
  104.0 10.9 %all-to-all-done.3 = bf16[16,16,2048]{2,1,0:T(8,128)(2,1)S(1)} async-done(((bf16[16,16,2048]{2,1,0:T(8,128)(2,1)}), bf16[16,16,2048]{2,1,0:T(8,128)(2,1)S(1)}, u32[]{:S(2)}, u32[]{:S(2)}) %all-to-all-start.3) | async-done | bytes 1048608 | tf_op jit(solution)/shard_map/all_to_all | solution.py:485
  114.9 0.0 copy-start.1
  114.9 3.7 %all-to-all-start.1 = ((bf16[16,16,2048]{2,1,0:T(8,128)(2,1)}), bf16[16,16,2048]{2,1,0:T(8,128)(2,1)S(1)}, u32[]{:S(2)}, u32[]{:S(2)}) async-start(bf16[16,16,2048]{2,1,0:T(8,128)(2,1)} %bitcast.28), calls=%async_computation.1 | async-start | bytes 2097152 | tf_op jit(solution)/shard_map/all_to_all | solution.py:485
  118.6 0.0 copy-done.1
  118.6 2.7 %shard_map.166 = bf16[128,2048]{1,0:T(8,128)(2,1)} custom-call(s32[1]{0:T(128)} %bitcast.first_ref, f32[4,128]{1,0:T(4,128)} %copy-done.7, bf16[256,2048]{1,0:T(8,128)(2,1)} %bitcast.26), custom_call_target="tpu_custom_call" | custom-call | flops 268435456 | bytes 1048576 | tf_op jit(solution)/shard_map/pallas_call | solution.py:413
  121.3 1.3 collective-permute-start.4
  122.6 5.5 %shard_map.164.rest_0_ = f32[128,2048]{1,0:T(8,128)} custom-call(bf16[128,2048]{1,0:T(8,128)(2,1)} %get-tuple-element.17.rows_hbm, bf16[2048,512]{1,0:T(8,128)(2,1)} %gate_hbm.1, bf16[2048,512]{1,0:T(8,128)(2,1)} %up_hbm.1, bf16[512,2048]{1,0:T(8,128)(2,1)} %down_hbm.1, bf16[128,2048]{1,0:T(8,128)(2,1)} %get-tuple-element.18.rest_0_), custom_call_target="tpu_custom_call" | custom-call | flops 805306368 | bytes 6291456 | tf_op jit(solution)/shard_map/pallas_call | solution.py:364
  128.1 14.8 %all-to-all-done.1 = bf16[16,16,2048]{2,1,0:T(8,128)(2,1)S(1)} async-done(((bf16[16,16,2048]{2,1,0:T(8,128)(2,1)}), bf16[16,16,2048]{2,1,0:T(8,128)(2,1)S(1)}, u32[]{:S(2)}, u32[]{:S(2)}) %all-to-all-start.1) | async-done | bytes 1048608 | tf_op jit(solution)/shard_map/all_to_all | solution.py:485
  142.9 0.0 copy-start
  142.9 4.9 %collective-permute-done.4.rest_1_ = bf16[128,2048]{1,0:T(8,128)(2,1)S(1)} collective-permute-done((bf16[128,2048]{1,0:T(8,128)(2,1)}, bf16[128,2048]{1,0:T(8,128)(2,1)S(1)}, u32[]{:S(2)}, u32[]{:S(2)}) %collective-permute-start.4) | collective-permute-done | bytes 524320 | tf_op jit(solution)/shard_map/ppermute | solution.py:29
  147.8 0.0 copy-start.4
  147.8 0.0 copy-done
  147.8 0.8 copy-done.4
  148.6 2.9 %shard_map.167 = bf16[128,2048]{1,0:T(8,128)(2,1)} custom-call(s32[1]{0:T(128)} %bitcast.first_ref, f32[4,128]{1,0:T(4,128)} %get-tuple-element.12.meta_ref, bf16[256,2048]{1,0:T(8,128)(2,1)} %bitcast.25, f32[128,2048]{1,0:T(8,128)} %shard_map.164.rest_0_, bf16[128,2048]{1,0:T(8,128)(2,1)} %copy-done.4), custom_call_target="tpu_custom_call" | custom-call | flops 268435456 | bytes 1048576 | tf_op jit(solution)/shard_map/pallas_call | solution.py:413
Async XLA Ops:
  1.5 6.8 %collective-permute-start = (bf16[32,640]{1,0:T(8,128)(2,1)}, bf16[32,640]{1,0:T(8,128)(2,1)S(1)}, u32[]{:S(2)}, u32[]{:S(2)}) collective-permute-start(bf16[32,640]{1,0:T(8,128)(2,1)} %get-tuple-element.13), channel_id=1, source_target_pairs={{0,2},{2,4},{4,6},{6,8},{8,10},{10,12},{12,14},{14,16},{16,18},{18... | collective-permute-start | bytes 122888 | tf_op jit(solution)/shard_map/ppermute | solution.py:25
  8.3 0.6 copy-start.8
  14.6 1.6 %collective-permute-start.1 = (bf16[128,512]{1,0:T(8,128)(2,1)}, bf16[128,512]{1,0:T(8,128)(2,1)S(1)}, u32[]{:S(2)}, u32[]{:S(2)}) collective-permute-start(bf16[128,512]{1,0:T(8,128)(2,1)} %get-tuple-element.15), channel_id=1, source_target_pairs={{0,1},{1,0},{2,3},{3,2},{4,5},{5,4},{6,7},{7,6},{8,9},{9,8},{10,11... | collective-permute-start | bytes 393224 | tf_op jit(solution)/shard_map/ppermute | solution.py:477
  16.1 0.7 copy-start.5
  16.8 10.5 %copy-start.6 = (f32[4,128]{1,0:T(4,128)S(1)}, f32[4,128]{1,0:T(4,128)}, u32[]{:S(2)}) copy-start(f32[4,128]{1,0:T(4,128)} %get-tuple-element.12.meta_ref) | copy-start | bytes 6148
  22.1 29.0 %collective-permute-start.3 = (bf16[128,2048]{1,0:T(8,128)(2,1)}, bf16[128,2048]{1,0:T(8,128)(2,1)S(1)}, u32[]{:S(2)}, u32[]{:S(2)}) collective-permute-start(bf16[128,2048]{1,0:T(8,128)(2,1)} %get-tuple-element.17.rows_hbm), channel_id=1, source_target_pairs={{0,16},{16,0},{1,17},{17,1},{2,18},{18,2},{3,19},{19,3},{4,20},{20... | collective-permute-start | bytes 1572872 | tf_op jit(solution)/shard_map/ppermute | solution.py:29
  27.3 23.8 %collective-permute-start.2 = (f32[4,128]{1,0:T(4,128)S(1)}, f32[4,128]{1,0:T(4,128)S(1)}, u32[]{:S(2)}, u32[]{:S(2)}) collective-permute-start(f32[4,128]{1,0:T(4,128)S(1)} %copy-done.6), channel_id=1, source_target_pairs={{0,16},{16,0},{1,17},{17,1},{2,18},{18,2},{3,19},{19,3},{4,20},{20... | collective-permute-start | bytes 6152 | tf_op jit(solution)/shard_map/ppermute | solution.py:29
  51.0 0.6 copy-start.7
  51.6 0.8 copy-start.3
  75.4 19.8 %all-to-all-start = ((bf16[16,16,2048]{2,1,0:T(8,128)(2,1)}), bf16[16,16,2048]{2,1,0:T(8,128)(2,1)S(1)}, u32[]{:S(2)}, u32[]{:S(2)}) async-start(bf16[16,16,2048]{2,1,0:T(8,128)(2,1)} %bitcast.8), calls=%async_computation | async-start | bytes 2097152 | tf_op jit(solution)/shard_map/all_to_all | solution.py:485
  95.1 3.7 %copy-start.2 = (bf16[16,16,2048]{2,1,0:T(8,128)(2,1)}, bf16[16,16,2048]{2,1,0:T(8,128)(2,1)S(1)}, u32[]{:S(2)}) copy-start(bf16[16,16,2048]{2,1,0:T(8,128)(2,1)S(1)} %all-to-all-done) | copy-start | bytes 3145732
  95.1 19.8 %all-to-all-start.3 = ((bf16[16,16,2048]{2,1,0:T(8,128)(2,1)}), bf16[16,16,2048]{2,1,0:T(8,128)(2,1)S(1)}, u32[]{:S(2)}, u32[]{:S(2)}) async-start(bf16[16,16,2048]{2,1,0:T(8,128)(2,1)} %bitcast.30), calls=%async_computation.3 | async-start | bytes 2097152 | tf_op jit(solution)/shard_map/all_to_all | solution.py:485
  114.9 3.7 %copy-start.1 = (bf16[16,16,2048]{2,1,0:T(8,128)(2,1)}, bf16[16,16,2048]{2,1,0:T(8,128)(2,1)S(1)}, u32[]{:S(2)}) copy-start(bf16[16,16,2048]{2,1,0:T(8,128)(2,1)S(1)} %all-to-all-done.3) | copy-start | bytes 3145732
  114.9 28.0 %all-to-all-start.1 = ((bf16[16,16,2048]{2,1,0:T(8,128)(2,1)}), bf16[16,16,2048]{2,1,0:T(8,128)(2,1)S(1)}, u32[]{:S(2)}, u32[]{:S(2)}) async-start(bf16[16,16,2048]{2,1,0:T(8,128)(2,1)} %bitcast.28), calls=%async_computation.1 | async-start | bytes 2097152 | tf_op jit(solution)/shard_map/all_to_all | solution.py:485
  121.3 26.5 %collective-permute-start.4 = (bf16[128,2048]{1,0:T(8,128)(2,1)}, bf16[128,2048]{1,0:T(8,128)(2,1)S(1)}, u32[]{:S(2)}, u32[]{:S(2)}) collective-permute-start(bf16[128,2048]{1,0:T(8,128)(2,1)} %shard_map.166), channel_id=1, source_target_pairs={{0,16},{16,0},{1,17},{17,1},{2,18},{18,2},{3,19},{19,3},{4,20},{20... | collective-permute-start | bytes 1572872 | tf_op jit(solution)/shard_map/ppermute | solution.py:29
  142.9 4.9 %copy-start = (bf16[16,16,2048]{2,1,0:T(8,128)(2,1)}, bf16[16,16,2048]{2,1,0:T(8,128)(2,1)S(1)}, u32[]{:S(2)}) copy-start(bf16[16,16,2048]{2,1,0:T(8,128)(2,1)S(1)} %all-to-all-done.1) | copy-start | bytes 3145732
  147.8 0.8 copy-start.4

commit v3 on v2

--- a/solution.py
+++ b/solution.py
@@ -17,6 +17,14 @@
 LINE = ("half", "sp")
 
 F32, BF16, I32 = jnp.float32, jnp.bfloat16, jnp.int32
+
+ROWS = 32
+STEPS = 4
+
+SMEM = pl.BlockSpec(memory_space=pltpu.SMEM)
+VMEM = pl.BlockSpec(memory_space=pltpu.VMEM)
+ANY = pl.BlockSpec(memory_space=pl.ANY)
+PARAMS = pltpu.CompilerParams(vmem_limit_bytes=24 * 2**20)
 
 
 def from_behind(x, axis, by):
@@ -81,15 +89,36 @@
             pl.BlockSpec((2 * top, tokens), lambda i: (0, 0)),
         ),
         cost_estimate=cost(1e6, 1e5),
+        compiler_params=PARAMS,
         name="edge",
     )(value, gate, ids, routes, weight)
+
+
+def conv_rows(row, count, rim, width, blocks, glu, ids, weights, gain_ref, shift_ref, store):
+    here = ids[pl.ds(row + rim, count), :]
+    total = [jnp.zeros((count, LANES), F32) for _ in range(blocks)]
+    for tap in range(width):
+        past = row + (rim - width + 1 + tap)
+        same = ids[pl.ds(past, count), :] == here
+        for c in range(blocks):
+            weight = weights[pl.ds(tap, 1), pl.ds(c * LANES, LANES)]
+            term = weight * glu[c, pl.ds(past, count), :]
+            total[c] = total[c] + jnp.where(same, term, 0.0)
+    for c in range(blocks):
+        lanes = pl.ds(c * LANES, LANES)
+        centered = total[c] - jnp.mean(total[c], axis=-1, keepdims=True)
+        spread = jnp.mean(centered * centered, axis=-1, keepdims=True)
+        scaled = centered * lax.rsqrt(spread + epsilon)
+        store(
+            lanes,
+            jax.nn.silu(scaled * gain_ref[:, lanes] + shift_ref[:, lanes]).astype(BF16),
+        )
 
 
 def conv_body(
     core_ref,
     value_ref,
     gate_ref,
-    edge_ref,
     ids_ref,
     taps_ref,
     gain_ref,
@@ -102,72 +131,143 @@
 ):
     positions, channels = value_ref.shape
     width = taps_ref.shape[0]
-    rim = edge_ref.shape[0]
     blocks = channels // LANES
-    rows = 32
+    rows = ROWS
     tokens = keep_ref.shape[0]
     weights[pl.ds(0, width), :] = taps_ref[...].astype(F32)
-    ids[pl.ds(0, rim), :] = edge_ref[:, pl.ds(channels, LANES)].astype(F32)
     for start in range(0, positions, LANES):
         row = ids_ref[:, pl.ds(start, LANES)].astype(F32)
-        ids[pl.ds(rim + start, LANES), :] = column_of(row, LANES, 0)
+        ids[pl.ds(start, LANES), :] = column_of(row, LANES, 0)
     for c in range(blocks):
         lanes = pl.ds(c * LANES, LANES)
-        glu[c, pl.ds(0, rim), :] = edge_ref[:, lanes].astype(F32)
-        glu[c, pl.ds(rim, positions), :] = glu_of(value_ref[:, lanes], gate_ref[:, lanes]).astype(
-            F32
-        )
-
-    def chunk(out_ref, base, index):
-        inside = pl.multiple_of(index * rows, rows)
-        row = pl.multiple_of(base + inside, rows)
-        here = ids[pl.ds(row + rim, rows), :]
-        total = [jnp.zeros((rows, LANES), F32) for _ in range(blocks)]
-        for tap in range(width):
-            past = row + (rim - width + 1 + tap)
-            same = ids[pl.ds(past, rows), :] == here
-            for c in range(blocks):
-                weight = weights[pl.ds(tap, 1), pl.ds(c * LANES, LANES)]
-                term = weight * glu[c, pl.ds(past, rows), :]
-                total[c] = total[c] + jnp.where(same, term, 0.0)
-        for c in range(blocks):
-            lanes = pl.ds(c * LANES, LANES)
-            centered = total[c] - jnp.mean(total[c], axis=-1, keepdims=True)
-            spread = jnp.mean(centered * centered, axis=-1, keepdims=True)
-            scaled = centered * lax.rsqrt(spread + epsilon)
-            out_ref[pl.ds(inside, rows), lanes] = jax.nn.silu(
-                scaled * gain_ref[:, lanes] + shift_ref[:, lanes]
-            ).astype(BF16)
+        glu[c] = glu_of(value_ref[:, lanes], gate_ref[:, lanes]).astype(F32)
 
     core = core_ref[0]
     parts = positions // tokens
     for out_ref, part in ((send_ref, parts - 1 - core), (keep_ref, core)):
-        base = pl.multiple_of(part * tokens, tokens)
-
-        def step(index, carry, out_ref=out_ref, base=base):
-            chunk(out_ref, base, index)
+
+        def step(index, carry, out_ref=out_ref, part=part):
+            inside = pl.multiple_of(index * rows, rows)
+            row = pl.multiple_of(part * tokens + inside - rows, rows)
+
+            def store(lanes, act):
+                out_ref[pl.ds(inside, rows), lanes] = act
+
+            conv_rows(
+                row, rows, rows, width, blocks, glu, ids, weights, gain_ref, shift_ref, store
+            )
             return carry
 
-        lax.fori_loop(0, tokens // rows, step, 0)
-
-
-def convolve(core, value, gate, edge, ids, taps, gain, shift, tokens):
+        lax.fori_loop((part == 0).astype(I32), tokens // rows, step, 0)
+
+
+def convolve(core, value, gate, ids, taps, gain, shift, tokens):
     positions, channels = value.shape
-    rim = edge.shape[0]
     half = jax.ShapeDtypeStruct((tokens, channels), BF16)
     return pl.pallas_call(
         conv_body,
         out_shape=(half, half),
-        in_specs=[pl.BlockSpec(memory_space=pltpu.SMEM)]
-        + [pl.BlockSpec(memory_space=pltpu.VMEM)] * 7,
+        in_specs=[SMEM] + [VMEM] * 6,
         scratch_shapes=[
-            pltpu.VMEM((channels // LANES, rim + positions, LANES), F32),
-            pltpu.VMEM((rim + positions, LANES), F32),
+            pltpu.VMEM((channels // LANES, positions, LANES), F32),
+            pltpu.VMEM((positions, LANES), F32),
             pltpu.VMEM((-(-taps.shape[0] // 8) * 8, channels), F32),
         ],
         cost_estimate=cost(6e9, 6 * value.size),
+        compiler_params=PARAMS,
         name="conv",
-    )(core, value, gate, edge, ids, taps, gain, shift)
+    )(core, value, gate, ids, taps, gain, shift)
+
+
+def rim_body(
+    core_ref,
+    edge_hbm,
+    value_ref,
+    gate_ref,
+    ids_ref,
+    taps_ref,
+    gain_ref,
+    shift_ref,
+    keep_in,
+    send_in,
+    keep_hbm,
+    send_hbm,
+    edge,
+    glu,
+    ids,
+    weights,
+    act,
+    sems,
+):
+    rows, channels = value_ref.shape
+    width = taps_ref.shape[0]
+    blocks = channels // LANES
+    arrival = pltpu.make_async_copy(edge_hbm, edge, sems.at[0])
+    arrival.start()
+    weights[pl.ds(0, width), :] = taps_ref[...].astype(F32)
+    ids[pl.ds(rows, rows), :] = column_of(ids_ref[...].astype(F32), rows, 0)
+    for c in range(blocks):
+        lanes = pl.ds(c * LANES, LANES)
+        glu[c, pl.ds(rows, rows), :] = glu_of(value_ref[:, lanes], gate_ref[:, lanes]).astype(F32)
+    arrival.wait()
+    ids[pl.ds(0, rows), :] = edge[:, pl.ds(channels, LANES)].astype(F32)
+    for c in range(blocks):
+        glu[c, pl.ds(0, rows), :] = edge[:, pl.ds(c * LANES, LANES)].astype(F32)
+
+    def store(lanes, value):
+        act[:, lanes] = value
+
+    conv_rows(0, rows, rows, width, blocks, glu, ids, weights, gain_ref, shift_ref, store)
+
+    for mine, out_hbm in ((core_ref[0] == 0, keep_hbm), (core_ref[0] != 0, send_hbm)):
+
+        @pl.when(mine)
+        def _(out_hbm=out_hbm):
+            copy = pltpu.make_async_copy(act, out_hbm.at[pl.ds(0, rows), :], sems.at[1])
+            copy.start()
+            copy.wait()
+
+
+def convolve_rim(core, edge, value, gate, ids, taps, gain, shift, keep, send):
+    channels = value.shape[1]
+    head = pl.BlockSpec((ROWS, channels), lambda i: (0, 0))
+
+    def whole(x):
+        return pl.BlockSpec(x.shape, lambda i: (0, 0))
+
+    return pl.pallas_call(
+        rim_body,
+        grid=(1,),
+        out_shape=(
+            jax.ShapeDtypeStruct(keep.shape, BF16),
+            jax.ShapeDtypeStruct(send.shape, BF16),
+        ),
+        in_specs=[
+            SMEM,
+            ANY,
+            head,
+            head,
+            pl.BlockSpec((1, LANES), lambda i: (0, 0)),
+            whole(taps),
+            whole(gain),
+            whole(shift),
+            ANY,
+            ANY,
+        ],
+        out_specs=(ANY, ANY),
+        input_output_aliases={8: 0, 9: 1},
+        scratch_shapes=[
+            pltpu.VMEM(edge.shape, BF16),
+            pltpu.VMEM((channels // LANES, 2 * ROWS, LANES), F32),
+            pltpu.VMEM((2 * ROWS, LANES), F32),
+            pltpu.VMEM((-(-taps.shape[0] // 8) * 8, channels), F32),
+            pltpu.VMEM((ROWS, channels), BF16),
+            pltpu.SemaphoreType.DMA((2,)),
+        ],
+        cost_estimate=cost(1e9, 4e5),
+        compiler_params=PARAMS,
+        name="rim",
+    )(core, edge, value, gate, ids, taps, gain, shift, keep, send)
 
 
 def selection(routes, first, experts, capacity, rows):
@@ -199,52 +299,84 @@
     shape_of,
     first_ref,
     core_ref,
-    keep_ref,
-    got_ref,
+    meta_ref,
+    gain_ref,
+    keep_hbm,
+    got_hbm,
     weight_hbm,
-    residual_ref,
-    gain_ref,
-    meta_ref,
-    parcel_ref,
-    stream_ref,
-    normed_ref,
+    residual_hbm,
+    parcel_hbm,
+    stream_hbm,
+    normed_hbm,
+    act,
     weight,
     total,
-    sems,
+    residual,
+    stream,
+    normed,
+    parcel,
+    act_sems,
+    in_sems,
+    out_sems,
 ):
     experts, capacity, top = shape_of
-    depth = keep_ref.shape[1]
-    chunks = weight.shape[0]
-    step = weight.shape[1]
+    depth = keep_hbm.shape[1]
+    chunks, step, width = weight.shape
     core = core_ref[0]
+    arrivals = []
+    for index, source in enumerate((keep_hbm, got_hbm)):
+        copy = pltpu.make_async_copy(source, act.at[index], act_sems.at[index])
+        copy.start()
+        arrivals.append(copy)
     copies = []
     for index in range(chunks):
         part, inside = divmod(index * step, depth)
         owner = core if part == 0 else 1 - core
         start = pl.multiple_of(owner * depth + inside, step)
         copy = pltpu.make_async_copy(
-            weight_hbm.at[pl.ds(start, step), :], weight.at[index], sems.at[index]
+            weight_hbm.at[pl.ds(start, step), :], weight.at[index], in_sems.at[index]
         )
         copy.start()
         copies.append(copy)
+    old = pltpu.make_async_copy(residual_hbm, residual, act_sems.at[2])
+    old.start()
     picks = selection(
-        meta_ref[pl.ds(0, top), :], first_ref[0], experts, capacity, parcel_ref.shape[0]
+        meta_ref[pl.ds(0, top), :], first_ref[0], experts, capacity, parcel.shape[0]
     )
     chosen = chosen_of(picks)
-    total[...] = residual_ref[...].astype(F32)
     for index, copy in enumerate(copies):
         part, inside = divmod(index * step, depth)
-        act = (keep_ref if part == 0 else got_ref)[:, pl.ds(inside, step)]
+        if inside == 0:
+            arrivals[part].wait()
         copy.wait()
-        total[...] += jnp.dot(act, weight[index], preferred_element_type=F32)
-    stream = total[...].astype(BF16)
-    wide = stream.astype(F32)
-    normed = (
+        product = jnp.dot(
+            act[part, :, pl.ds(inside, step)], weight[index], preferred_element_type=F32
+        )
+        if index == 0:
+            total[...] = product
+        else:
+            total[...] += product
+    old.wait()
+    stream[...] = (residual[...].astype(F32) + total[...]).astype(BF16)
+    back = [pltpu.make_async_copy(stream, stream_hbm, out_sems.at[0])]
+    back[0].start()
+    wide = stream[...].astype(F32)
+    normed[...] = (
         wide * lax.rsqrt(jnp.mean(wide * wide, axis=-1, keepdims=True) + epsilon) * gain_ref[...]
     ).astype(BF16)
-    stream_ref[...] = stream
-    normed_ref[...] = normed
-    parcel_ref[...] = jnp.dot(chosen, normed, preferred_element_type=F32).astype(BF16)
+    back.append(pltpu.make_async_copy(normed, normed_hbm, out_sems.at[1]))
+    back[1].start()
+    tile = width // STEPS
+    for n in range(STEPS):
+        cols = pl.ds(n * tile, tile)
+        parcel[:, cols] = jnp.dot(chosen, normed[:, cols], preferred_element_type=F32).astype(BF16)
+        copy = pltpu.make_async_copy(
+            parcel.at[:, cols], parcel_hbm.at[:, cols], out_sems.at[2 + n]
+        )
+        copy.start()
+        back.append(copy)
+    for copy in back:
+        copy.wait()
 
 
 def project(first, core, keep, got, weight, residual, gain, meta, sizes, rows):
@@ -253,51 +385,77 @@
     step = depth // 2
     chunks = 2 * depth // step
     out = jax.ShapeDtypeStruct((tokens, width), BF16)
-    smem = pl.BlockSpec(memory_space=pltpu.SMEM)
-    vmem = pl.BlockSpec(memory_space=pltpu.VMEM)
     return pl.pallas_call(
         functools.partial(project_body, sizes),
         out_shape=(jax.ShapeDtypeStruct((rows, width), BF16), out, out),
-        in_specs=[smem, smem, vmem, vmem, pl.BlockSpec(memory_space=pl.ANY), vmem, vmem, vmem],
-        out_specs=[vmem] * 3,
+        in_specs=[SMEM, SMEM, VMEM, VMEM] + [ANY] * 4,
+        out_specs=[ANY] * 3,
         scratch_shapes=[
+            pltpu.VMEM((2, tokens, depth), BF16),
             pltpu.VMEM((chunks, step, width), BF16),
             pltpu.VMEM((tokens, width), F32),
+            pltpu.VMEM((tokens, width), BF16),
+            pltpu.VMEM((tokens, width), BF16),
+            pltpu.VMEM((tokens, width), BF16),
+            pltpu.VMEM((rows, width), BF16),
+            pltpu.SemaphoreType.DMA((3,)),
             pltpu.SemaphoreType.DMA((chunks,)),
+            pltpu.SemaphoreType.DMA((2 + STEPS,)),
         ],
         cost_estimate=cost(2 * tokens * weight.size, 2 * weight.size),
+        compiler_params=PARAMS,
         name="project",
-    )(first, core, keep, got, weight, residual, gain, meta)
-
-
-def gather_body(shape_of, first_ref, meta_ref, rows_ref, parcel_ref, chosen):
+    )(first, core, meta, gain, keep, got, weight, residual)
+
+
+def stream_in(source, target, sems):
+    tile = target.shape[1] // STEPS
+    copies = []
+    for n in range(STEPS):
+        cols = pl.ds(n * tile, tile)
+        copies.append(pltpu.make_async_copy(source.at[:, cols], target.at[:, cols], sems.at[n]))
+        copies[-1].start()
+    return copies
+
+
+def gather_body(
+    shape_of, first_ref, meta_ref, rows_hbm, parcel_hbm, rows, parcel, in_sems, out_sems
+):
     experts, capacity, top = shape_of
-
-    @pl.when(pl.program_id(0) == 0)
-    def _():
-        picks = selection(
-            meta_ref[pl.ds(0, top), :], first_ref[0], experts, capacity, parcel_ref.shape[0]
+    copies = stream_in(rows_hbm, rows, in_sems)
+    picks = selection(
+        meta_ref[pl.ds(0, top), :], first_ref[0], experts, capacity, parcel.shape[0]
+    )
+    chosen = chosen_of(picks)
+    tile = rows.shape[1] // STEPS
+    back = []
+    for n, copy in enumerate(copies):
+        cols = pl.ds(n * tile, tile)
+        copy.wait()
+        parcel[:, cols] = jnp.dot(chosen, rows[:, cols], preferred_element_type=F32).astype(BF16)
+        back.append(
+            pltpu.make_async_copy(parcel.at[:, cols], parcel_hbm.at[:, cols], out_sems.at[n])
         )
-        chosen[...] = chosen_of(picks)
-
-    parcel_ref[...] = jnp.dot(chosen[...], rows_ref[...], preferred_element_type=F32).astype(BF16)
+        back[-1].start()
+    for copy in back:
+        copy.wait()
 
 
 def gather(first, meta, rows, sizes, count):
     tokens, width = rows.shape
-    tile = width // 2
     return pl.pallas_call(
         functools.partial(gather_body, sizes),
-        grid=(width // tile,),
         out_shape=jax.ShapeDtypeStruct((count, width), BF16),
-        in_specs=[
-            pl.BlockSpec(memory_space=pltpu.SMEM),
-            pl.BlockSpec(meta.shape, lambda n: (0, 0)),
-            pl.BlockSpec((tokens, tile), lambda n: (0, n)),
+        in_specs=[SMEM, VMEM, ANY],
+        out_specs=ANY,
+        scratch_shapes=[
+            pltpu.VMEM((tokens, width), BF16),
+            pltpu.VMEM((count, width), BF16),
+            pltpu.SemaphoreType.DMA((STEPS,)),
+            pltpu.SemaphoreType.DMA((STEPS,)),
         ],
-        out_specs=pl.BlockSpec((count, tile), lambda n: (0, n)),
-        scratch_shapes=[pltpu.VMEM((count, tokens), BF16)],
         cost_estimate=cost(2 * count * tokens * width, 2 * (count + tokens) * width),
+        compiler_params=PARAMS,
         name="gather",
     )(first, meta, rows)
 
@@ -359,13 +517,12 @@
 def gated_mlp(rows, gate, up, down, extra, dtype):
     count, width = rows.shape
     inner = gate.shape[-1]
-    steps = 4
-    anywhere = pl.BlockSpec(memory_space=pl.ANY)
+    steps = STEPS
     return pl.pallas_call(
         functools.partial(mlp_body, steps),
         out_shape=jax.ShapeDtypeStruct((count, width), dtype),
-        in_specs=[anywhere] * 4 + [pl.BlockSpec(memory_space=pltpu.VMEM)] * len(extra),
-        out_specs=anywhere,
+        in_specs=[ANY] * 4 + [VMEM] * len(extra),
+        out_specs=ANY,
         scratch_shapes=[
             pltpu.VMEM((count, width), rows.dtype),
             pltpu.VMEM((width, inner), gate.dtype),
@@ -379,50 +536,61 @@
             pltpu.SemaphoreType.DMA((steps,)),
         ],
         cost_estimate=cost(6 * count * width * inner, 6 * width * inner),
+        compiler_params=PARAMS,
     )(rows, gate, up, down, *extra)
 
 
-def combine_body(shape_of, first_ref, meta_ref, back_ref, *rest):
+def combine_body(shape_of, extras, first_ref, meta_ref, back_hbm, *rest):
     experts, capacity, top = shape_of
-    out_ref, high, low = rest[-3:]
-
-    @pl.when(pl.program_id(0) == 0)
-    def _():
-        rows = back_ref.shape[0]
-        picks = selection(meta_ref[pl.ds(0, top), :], first_ref[0], experts, capacity, rows)
-        table = jnp.zeros((rows, meta_ref.shape[1]), F32)
-        for k, pick in enumerate(picks):
-            table = table + jnp.where(pick, meta_ref[pl.ds(top + k, 1), :], 0.0)
-        table = table.T
-        high[...] = table.astype(BF16)
-        low[...] = (table - table.astype(BF16).astype(F32)).astype(BF16)
-
-    back = back_ref[...]
-    total = jnp.dot(high[...], back, preferred_element_type=F32)
-    total = total + jnp.dot(low[...], back, preferred_element_type=F32)
-    for ref in rest[:-3]:
-        total = total + ref[...].astype(F32)
-    out_ref[...] = total.astype(out_ref.dtype)
+    extra_hbm, rest = rest[:extras], rest[extras:]
+    out_hbm, rest = rest[0], rest[1:]
+    extra, rest = rest[:extras], rest[extras:]
+    back, out, in_sems, out_sems = rest
+    rows = back.shape[0]
+    arrivals = [stream_in(back_hbm, back, in_sems.at[0])]
+    for index in range(extras):
+        arrivals.append(stream_in(extra_hbm[index], extra[index], in_sems.at[1 + index]))
+    picks = selection(meta_ref[pl.ds(0, top), :], first_ref[0], experts, capacity, rows)
+    table = jnp.zeros((rows, meta_ref.shape[1]), F32)
+    for k, pick in enumerate(picks):
+        table = table + jnp.where(pick, meta_ref[pl.ds(top + k, 1), :], 0.0)
+    table = table.T
+    high = table.astype(BF16)
+    low = (table - high.astype(F32)).astype(BF16)
+    tile = back.shape[1] // STEPS
+    done = []
+    for n in range(STEPS):
+        cols = pl.ds(n * tile, tile)
+        for copies in arrivals:
+            copies[n].wait()
+        total = jnp.dot(high, back[:, cols], preferred_element_type=F32)
+        total = total + jnp.dot(low, back[:, cols], preferred_element_type=F32)
+        for ref in extra:
+            total = total + ref[:, cols].astype(F32)
+        out[:, cols] = total.astype(out.dtype)
+        done.append(pltpu.make_async_copy(out.at[:, cols], out_hbm.at[:, cols], out_sems.at[n]))
+        done[-1].start()
+    for copy in done:
+        copy.wait()
 
 
 def combine(first, meta, back, sizes, extra):
     rows, width = back.shape
     tokens = meta.shape[1]
-    tile = width // 2
-    row = pl.BlockSpec((tokens, tile), lambda n: (0, n))
     return pl.pallas_call(
-        functools.partial(combine_body, sizes),
-        grid=(width // tile,),
+        functools.partial(combine_body, sizes, len(extra)),
         out_shape=jax.ShapeDtypeStruct((tokens, width), BF16),
-        in_specs=[
-            pl.BlockSpec(memory_space=pltpu.SMEM),
-            pl.BlockSpec(meta.shape, lambda n: (0, 0)),
-            pl.BlockSpec((rows, tile), lambda n: (0, n)),
-        ]
-        + [row] * len(extra),
-        out_specs=row,
-        scratch_shapes=[pltpu.VMEM((tokens, rows), BF16)] * 2,
+        in_specs=[SMEM, VMEM] + [ANY] * (1 + len(extra)),
+        out_specs=ANY,
+        scratch_shapes=[pltpu.VMEM(x.shape, x.dtype) for x in extra]
+        + [
+            pltpu.VMEM((rows, width), BF16),
+            pltpu.VMEM((tokens, width), BF16),
+            pltpu.SemaphoreType.DMA((1 + len(extra), STEPS)),
+            pltpu.SemaphoreType.DMA((STEPS,)),
+        ],
         cost_estimate=cost(4 * tokens * rows * width, 2 * rows * width),
+        compiler_params=PARAMS,
     )(first, meta, back, *extra)
 
 
@@ -445,7 +613,6 @@
     shared_up,
     shared_down,
 ):
-    kernel_width = taps.shape[0]
     model_width = residual.shape[1]
     token_count, top_count = routes.shape
     half_devices = lax.axis_size("sp") * lax.axis_size("tp")
@@ -458,23 +625,18 @@
     core = lax.axis_index("tp").astype(I32).reshape(1)
     sizes = (experts, capacity, top_count)
 
-    rim = -(-(kernel_width - 1) // 16) * 16
     ids = doc_ids[None, :]
-    own_edge, own_meta = edge_of(conv_value, conv_gate, ids, routes.T, route_weight.T, rim)
+    gain, shift = gn_gain[None, :], gn_shift[None, :]
+    own_edge, own_meta = edge_of(conv_value, conv_gate, ids, routes.T, route_weight.T, ROWS)
     edge = from_behind(own_edge, LINE, 1)
+    keep, send = convolve(
+        core, conv_value, conv_gate, ids, taps, gain, shift, token_count
+    )
+    keep, send = convolve_rim(
+        core, edge, conv_value, conv_gate, ids, taps, gain, shift, keep, send
+    )
+    got = lax.ppermute(send, "tp", [(0, 1), (1, 0)])
     mirror_meta = to_mirror(own_meta)
-    keep, send = convolve(
-        core,
-        conv_value,
-        conv_gate,
-        edge,
-        ids,
-        taps,
-        gn_gain[None, :],
-        gn_shift[None, :],
-        token_count,
-    )
-    got = lax.ppermute(send, "tp", [(0, 1), (1, 0)])
     parcel, stream, normed = project(
         first, core, keep, got, conv_out, residual, norm_gain[None, :], own_meta, sizes, half_rows
     )

time: 152 us -> 149 us (0.980)
  local copies, waits for them, and re-layouts: 3.43 us -> 29.5 us
  waiting for transfers between devices: 68.7 us -> 51.5 us
  Pallas kernels: 36.4 us -> 24.3 us
    unnamed x18 -> x72, local copies, waits for them, and re-layouts: 3.43 us -> 29.5 us
    all_to_all x3, waiting for transfers between devices: 36.6 us -> 24.4 us  [exchange(): lax.all_to_all(parcel, HALF, split_axis=0, concat_axis=0, tiled=True)]
    pallas_call x3, Pallas kernels: 15.9 us -> 11.4 us  [gated_mlp(): pl.pallas_call(functools.partial(mlp_body, steps), out_shape=jax.ShapeDty...]
    pallas_call x4 -> x5, Pallas kernels: 13.7 us -> 9.6 us  [the longest x2 4.28 us: combine(): pl.pallas_call(functools.partial(combine_body, sizes, len(extra)), out_sh...]
    ppermute x3, waiting for transfers between devices: 28.5 us -> 25.7 us  [to_mirror(): return lax.ppermute(x, 'half', [(0, 1), (1, 0)])]
    pallas_call x1, Pallas kernels: 5.29 us -> 3.2 us  [project(): pl.pallas_call(functools.partial(project_body, sizes), out_shape=(jax.Sha...]
    ppermute x1, waiting for transfers between devices: 1.97 us -> 0.01 us  [from_behind(): return lax.ppermute(x, axis, pairs)]
  transfers between devices with their start and end apart: 8 -> 8, of which waited for: 7 -> 6; matrix products, arithmetic and copies ran while one was open for 0% -> 0% of each run, Pallas kernels for 12% -> 11%
where the time goes in v3:
time: 149 us; the launch traced here: 147 us
  waiting for transfers between devices  51.5 us (35%)
  local copies, waits for them, and re-layouts  29.5 us (20%)
  Pallas kernels  24.3 us (16%)
  starting transfers between devices  21.7 us (15%)
  blocking collectives  20 us (13%)
    unnamed x72, local copies, waits for them, and re-layouts  29.5 us
    ppermute x3, waiting for transfers between devices, to_mirror(): return lax.ppermute(x, 'half', [(0, 1), (1, 0)])  25.7 us
    all_to_all x3, waiting for transfers between devices, exchange(): lax.all_to_all(parcel, HALF, split_axis=0, concat_axis=0, tiled=True)  24.4 us
    all_to_all x1, blocking collectives, exchange(): lax.all_to_all(parcel, HALF, split_axis=0, concat_axis=0, tiled=True)  20 us
    pallas_call x3, Pallas kernels, gated_mlp(): pl.pallas_call(functools.partial(mlp_body, steps), out_shape=jax.ShapeDty...  11.4 us
    all_to_all x3, starting transfers between devices, exchange(): lax.all_to_all(parcel, HALF, split_axis=0, concat_axis=0, tiled=True)  11.2 us
    ppermute x3, starting transfers between devices, to_mirror(): return lax.ppermute(x, 'half', [(0, 1), (1, 0)])  5.6 us
    ppermute x1, starting transfers between devices, from_behind(): return lax.ppermute(x, axis, pairs)  4.86 us
  transfers between devices with their start and end apart: 8, of which 6 were waited for; matrix products, arithmetic and copies ran while one was open for 0% of the time, Pallas kernels for 11%

profile of v3, /device:TPU:0, one launch (start us, length us, event | category | flops | bytes accessed | tf_op | source)
XLA Modules:
  0.0 147.4 jit_solution(1663323177108862980)
XLA Ops:
  0.0 0.9 copy-done.20
  1.0 0.9 copy-done.22
  1.9 0.7 copy-done.25
  2.6 0.7 copy-done.26
  3.3 0.7 copy-done.27
  4.0 4.9 %collective-permute-start = (bf16[32,640]{1,0:T(8,128)(2,1)S(1)}, bf16[32,640]{1,0:T(8,128)(2,1)S(1)}, u32[]{:S(2)}, u32[]{:S(2)}) collective-permute-start(bf16[32,640]{1,0:T(8,128)(2,1)S(1)} %get-tuple-element.15), channel_id=1, source_target_pairs={{0,2},{2,4},{4,6},{6,8},{8,10},{10,12},{12,14},{14,16},{16,18},{18... | collective-permute-start | bytes 122888 | tf_op jit(solution)/shard_map/ppermute | solution.py:33
  8.9 0.9 copy-done.21
  9.9 0.9 copy-done.23
  10.8 0.7 copy-done.28
  11.5 0.8 copy-done.30
  12.2 0.7 copy-done.32
  12.9 0.7 copy-done.34
  13.6 3.3 %conv.1 = (bf16[128,512]{1,0:T(8,128)(2,1)S(1)}, bf16[128,512]{1,0:T(8,128)(2,1)S(1)}) custom-call(s32[1]{0:T(128)} %bitcast.4.core_ref, bf16[256,512]{1,0:T(8,128)(2,1)S(1)} %copy-done.21, bf16[256,512]{1,0:T(8,128)(2,1)S(1)} %copy-done.23, s32[1,256]{1,0:T(1,128)S(1)} %bitcast.37, bf16[31,512]{1,0:T(8,128)(2,1)S(1)} %copy-done.30, f32[1,512]{1,0:T(1,128)S(1)} %bitcast.39, ...), custom_call_target="tpu_custom_call" | custom-call | flops 6000000000 | bytes 786432 | tf_op jit(solution)/shard_map/conv/pallas_call | solution.py:167
  17.0 0.7 rim.1
  17.8 1.3 collective-permute-done.1.got_hbm
  19.1 2.2 %copy-done.5 = bf16[1024,2048]{1,0:T(8,128)(2,1)S(1)} copy-done((bf16[1024,2048]{1,0:T(8,128)(2,1)S(1)}, bf16[1024,2048]{1,0:T(8,128)(2,1)}, u32[]{:S(2)}) %copy-start.5) | copy-done | bytes 4194328
  21.3 3.2 %project.1 = (bf16[256,2048]{1,0:T(8,128)(2,1)S(1)}, bf16[128,2048]{1,0:T(8,128)(2,1)S(1)}, bf16[128,2048]{1,0:T(8,128)(2,1)S(1)}) custom-call(s32[1]{0:T(128)} %bitcast.first_ref, s32[1]{0:T(128)} %bitcast.4.core_ref, f32[4,128]{1,0:T(4,128)S(1)} %get-tuple-element.14.meta_ref, f32[1,2048]{1,0:T(1,128)S(1)} %bitcast.33, ...), custom_call_target="tpu_custom_call" | custom-call | flops 536870912 | bytes 4194304 | tf_op jit(solution)/shard_map/project/pallas_call | solution.py:388
  24.6 2.7 %collective-permute-start.3 = (bf16[128,2048]{1,0:T(8,128)(2,1)S(1)}, bf16[128,2048]{1,0:T(8,128)(2,1)S(1)}, u32[]{:S(2)}, u32[]{:S(2)}) collective-permute-start(bf16[128,2048]{1,0:T(8,128)(2,1)S(1)} %get-tuple-element.21.rows_hbm), channel_id=1, source_target_pairs={{0,16},{16,0},{1,17},{17,1},{2,18},{18,2},{3,19},{19,3},{4,20},{20... | collective-permute-start | bytes 1572872 | tf_op jit(solution)/shard_map/ppermute | solution.py:37
  27.6 23.3 %collective-permute-done.2.meta_ref = f32[4,128]{1,0:T(4,128)S(1)} collective-permute-done((f32[4,128]{1,0:T(4,128)S(1)}, f32[4,128]{1,0:T(4,128)S(1)}, u32[]{:S(2)}, u32[]{:S(2)}) %collective-permute-start.2) | collective-permute-done | bytes 2080 | tf_op jit(solution)/shard_map/ppermute | solution.py:37
  50.8 1.3 gather.1
  52.2 20.0 %all_to_all.20 = bf16[16,16,2048]{2,1,0:T(8,128)(2,1)} all-to-all(bf16[16,16,2048]{2,1,0:T(8,128)(2,1)S(1)} %bitcast.27), channel_id=1, replica_groups=mesh['half'=2,'sp'=8,'tp'=2] {'sp','tp'}, dimensions={0} | all-to-all | bytes 2097152 | tf_op jit(solution)/shard_map/all_to_all | solution.py:647
  72.2 3.7 %all-to-all-start = ((bf16[16,16,2048]{2,1,0:T(8,128)(2,1)}), bf16[16,16,2048]{2,1,0:T(8,128)(2,1)S(1)}, u32[]{:S(2)}, u32[]{:S(2)}) async-start(bf16[16,16,2048]{2,1,0:T(8,128)(2,1)} %bitcast.32), calls=%async_computation | async-start | bytes 2097152 | tf_op jit(solution)/shard_map/all_to_all | solution.py:647
  75.9 1.6 %copy-done.1 = bf16[1,2048,512]{2,1,0:T(8,128)(2,1)S(1)} copy-done((bf16[1,2048,512]{2,1,0:T(8,128)(2,1)S(1)}, bf16[1,2048,512]{2,1,0:T(8,128)(2,1)}, u32[]{:S(2)}) %copy-start.1) | copy-done | bytes 2097176
  77.5 1.6 %copy-done.3 = bf16[1,512,2048]{2,1,0:T(8,128)(2,1)S(1)} copy-done((bf16[1,512,2048]{2,1,0:T(8,128)(2,1)S(1)}, bf16[1,512,2048]{2,1,0:T(8,128)(2,1)}, u32[]{:S(2)}) %copy-start.3) | copy-done | bytes 2097176
  79.1 1.2 copy-done.10
  80.3 4.1 %shard_map.165 = bf16[256,2048]{1,0:T(8,128)(2,1)S(1)} custom-call(bf16[256,2048]{1,0:T(8,128)(2,1)S(1)} %bitcast.31, bf16[2048,512]{1,0:T(8,128)(2,1)S(1)} %bitcast.19, bf16[2048,512]{1,0:T(8,128)(2,1)S(1)} %bitcast.21, bf16[512,2048]{1,0:T(8,128)(2,1)S(1)} %bitcast.23), custom_call_target="tpu_custom_call" | custom-call | flops 1610612736 | bytes 6291456 | tf_op jit(solution)/shard_map/pallas_call | solution.py:521
  84.4 1.0 copy-done.9
  85.4 6.6 %all-to-all-done = bf16[16,16,2048]{2,1,0:T(8,128)(2,1)S(1)} async-done(((bf16[16,16,2048]{2,1,0:T(8,128)(2,1)}), bf16[16,16,2048]{2,1,0:T(8,128)(2,1)S(1)}, u32[]{:S(2)}, u32[]{:S(2)}) %all-to-all-start) | async-done | bytes 1048608 | tf_op jit(solution)/shard_map/all_to_all | solution.py:647
  92.0 1.0 copy-done.7
  93.0 3.7 %all-to-all-start.3 = ((bf16[16,16,2048]{2,1,0:T(8,128)(2,1)}), bf16[16,16,2048]{2,1,0:T(8,128)(2,1)S(1)}, u32[]{:S(2)}, u32[]{:S(2)}) async-start(bf16[16,16,2048]{2,1,0:T(8,128)(2,1)} %bitcast.30), calls=%async_computation.3 | async-start | bytes 2097152 | tf_op jit(solution)/shard_map/all_to_all | solution.py:647
  96.6 1.6 %copy-done.2 = bf16[1,2048,512]{2,1,0:T(8,128)(2,1)S(1)} copy-done((bf16[1,2048,512]{2,1,0:T(8,128)(2,1)S(1)}, bf16[1,2048,512]{2,1,0:T(8,128)(2,1)}, u32[]{:S(2)}) %copy-start.2) | copy-done | bytes 2097176
  98.2 1.6 %copy-done.4 = bf16[1,512,2048]{2,1,0:T(8,128)(2,1)S(1)} copy-done((bf16[1,512,2048]{2,1,0:T(8,128)(2,1)S(1)}, bf16[1,512,2048]{2,1,0:T(8,128)(2,1)}, u32[]{:S(2)}) %copy-start.4) | copy-done | bytes 2097176
  99.8 1.2 copy-done.8
  101.0 4.1 %shard_map.163 = bf16[256,2048]{1,0:T(8,128)(2,1)S(1)} custom-call(bf16[256,2048]{1,0:T(8,128)(2,1)S(1)} %bitcast.29, bf16[2048,512]{1,0:T(8,128)(2,1)S(1)} %bitcast.20, bf16[2048,512]{1,0:T(8,128)(2,1)S(1)} %bitcast.22, bf16[512,2048]{1,0:T(8,128)(2,1)S(1)} %bitcast.24), custom_call_target="tpu_custom_call" | custom-call | flops 1610612736 | bytes 6291456 | tf_op jit(solution)/shard_map/pallas_call | solution.py:521
  105.1 1.0 copy-done.6
  106.1 6.6 %all-to-all-done.3 = bf16[16,16,2048]{2,1,0:T(8,128)(2,1)S(1)} async-done(((bf16[16,16,2048]{2,1,0:T(8,128)(2,1)}), bf16[16,16,2048]{2,1,0:T(8,128)(2,1)S(1)}, u32[]{:S(2)}, u32[]{:S(2)}) %all-to-all-start.3) | async-done | bytes 1048608 | tf_op jit(solution)/shard_map/all_to_all | solution.py:647
  112.7 3.8 %all-to-all-start.1 = ((bf16[16,16,2048]{2,1,0:T(8,128)(2,1)}), bf16[16,16,2048]{2,1,0:T(8,128)(2,1)S(1)}, u32[]{:S(2)}, u32[]{:S(2)}) async-start(bf16[16,16,2048]{2,1,0:T(8,128)(2,1)} %bitcast.28), calls=%async_computation.1 | async-start | bytes 2097152 | tf_op jit(solution)/shard_map/all_to_all | solution.py:647
  116.6 2.0 %shard_map.166 = bf16[128,2048]{1,0:T(8,128)(2,1)} custom-call(s32[1]{0:T(128)} %bitcast.first_ref, f32[4,128]{1,0:T(4,128)S(1)} %collective-permute-done.2.meta_ref, bf16[256,2048]{1,0:T(8,128)(2,1)S(1)} %bitcast.26), custom_call_target="tpu_custom_call" | custom-call | flops 268435456 | bytes 1048576 | tf_op jit(solution)/shard_map/pallas_call | solution.py:580
  118.6 2.6 %collective-permute-start.4 = (bf16[128,2048]{1,0:T(8,128)(2,1)}, bf16[128,2048]{1,0:T(8,128)(2,1)S(1)}, u32[]{:S(2)}, u32[]{:S(2)}) collective-permute-start(bf16[128,2048]{1,0:T(8,128)(2,1)} %shard_map.166), channel_id=1, source_target_pairs={{0,16},{16,0},{1,17},{17,1},{2,18},{18,2},{3,19},{19,3},{4,20},{20... | collective-permute-start | bytes 1572872 | tf_op jit(solution)/shard_map/ppermute | solution.py:37
  121.2 1.6 %copy-done.11 = bf16[2048,512]{1,0:T(8,128)(2,1)S(1)} copy-done((bf16[2048,512]{1,0:T(8,128)(2,1)S(1)}, bf16[2048,512]{1,0:T(8,128)(2,1)}, u32[]{:S(2)}) %copy-start.11) | copy-done | bytes 2097176
  122.8 1.6 %copy-done.12 = bf16[2048,512]{1,0:T(8,128)(2,1)S(1)} copy-done((bf16[2048,512]{1,0:T(8,128)(2,1)S(1)}, bf16[2048,512]{1,0:T(8,128)(2,1)}, u32[]{:S(2)}) %copy-start.12) | copy-done | bytes 2097176
  124.4 1.6 %copy-done.13 = bf16[512,2048]{1,0:T(8,128)(2,1)S(1)} copy-done((bf16[512,2048]{1,0:T(8,128)(2,1)S(1)}, bf16[512,2048]{1,0:T(8,128)(2,1)}, u32[]{:S(2)}) %copy-start.13) | copy-done | bytes 2097176
  126.0 1.0 copy-done.17
  127.0 1.0 copy-done.19
  128.1 3.2 %shard_map.164.rest_0_ = f32[128,2048]{1,0:T(8,128)S(1)} custom-call(bf16[128,2048]{1,0:T(8,128)(2,1)S(1)} %copy-done.19, bf16[2048,512]{1,0:T(8,128)(2,1)S(1)} %copy-done.11, bf16[2048,512]{1,0:T(8,128)(2,1)S(1)} %copy-done.12, bf16[512,2048]{1,0:T(8,128)(2,1)S(1)} %copy-done.13, bf16[128,2048]{1,0:T(8,128)(2,1)S(1)} %copy-done.17), custom_call_target="tpu_custom_call" | custom-call | flops 805306368 | bytes 6291456 | tf_op jit(solution)/shard_map/pallas_call | solution.py:521
  131.3 11.2 %all-to-all-done.1 = bf16[16,16,2048]{2,1,0:T(8,128)(2,1)S(1)} async-done(((bf16[16,16,2048]{2,1,0:T(8,128)(2,1)}), bf16[16,16,2048]{2,1,0:T(8,128)(2,1)S(1)}, u32[]{:S(2)}, u32[]{:S(2)}) %all-to-all-start.1) | async-done | bytes 1048608 | tf_op jit(solution)/shard_map/all_to_all | solution.py:647
  142.5 2.5 %collective-permute-done.4.rest_1_ = bf16[128,2048]{1,0:T(8,128)(2,1)S(1)} collective-permute-done((bf16[128,2048]{1,0:T(8,128)(2,1)}, bf16[128,2048]{1,0:T(8,128)(2,1)S(1)}, u32[]{:S(2)}, u32[]{:S(2)}) %collective-permute-start.4) | collective-permute-done | bytes 524320 | tf_op jit(solution)/shard_map/ppermute | solution.py:37
  145.0 2.2 %shard_map.167 = bf16[128,2048]{1,0:T(8,128)(2,1)} custom-call(s32[1]{0:T(128)} %bitcast.first_ref, f32[4,128]{1,0:T(4,128)S(1)} %get-tuple-element.14.meta_ref, bf16[256,2048]{1,0:T(8,128)(2,1)S(1)} %bitcast.25, f32[128,2048]{1,0:T(8,128)S(1)} %shard_map.164.rest_0_, bf16[128,2048]{1,0:T(8,128)(2,1)S(1)} %collective-permute-done.4.rest_1_), custom_call_target="tpu_custom_call" | custom-call | flops 268435456 | bytes 1048576 | tf_op jit(solution)/shard_map/pallas_call | solution.py:580
  (51 shorter events, 0.6 us)
Async XLA Ops:
  0.0 0.9 copy-start.20
  1.0 0.9 copy-start.22
  1.9 0.7 copy-start.25
  2.6 0.7 copy-start.26
  3.3 0.7 copy-start.27
  4.0 13.0 %collective-permute-start = (bf16[32,640]{1,0:T(8,128)(2,1)S(1)}, bf16[32,640]{1,0:T(8,128)(2,1)S(1)}, u32[]{:S(2)}, u32[]{:S(2)}) collective-permute-start(bf16[32,640]{1,0:T(8,128)(2,1)S(1)} %get-tuple-element.15), channel_id=1, source_target_pairs={{0,2},{2,4},{4,6},{6,8},{8,10},{10,12},{12,14},{14,16},{16,18},{18... | collective-permute-start | bytes 122888 | tf_op jit(solution)/shard_map/ppermute | solution.py:33
  8.9 1.0 copy-start.21
  9.9 0.9 copy-start.23
  10.8 0.7 copy-start.28
  11.5 0.8 copy-start.30
  12.2 0.7 copy-start.32
  12.9 0.7 copy-start.34
  13.6 3.4 %copy-start.29 = (s32[256]{0:T(256)S(1)}, s32[256]{0:T(256)}, u32[]{:S(2)}) copy-start(s32[256]{0:T(256)} %param.20) | copy-start | bytes 3076
  13.6 3.4 %copy-start.31 = (bf16[31,512]{1,0:T(8,128)(2,1)S(1)}, bf16[31,512]{1,0:T(8,128)(2,1)}, u32[]{:S(2)}) copy-start(bf16[31,512]{1,0:T(8,128)(2,1)} %taps_ref.3) | copy-start | bytes 95236
  13.6 3.4 %copy-start.33 = (f32[512]{0:T(512)S(1)}, f32[512]{0:T(512)}, u32[]{:S(2)}) copy-start(f32[512]{0:T(512)} %param.21) | copy-start | bytes 6148
  13.6 3.4 %copy-start.35 = (f32[512]{0:T(512)S(1)}, f32[512]{0:T(512)}, u32[]{:S(2)}) copy-start(f32[512]{0:T(512)} %param.22) | copy-start | bytes 6148
  17.0 2.2 %copy-start.15 = (bf16[128,2048]{1,0:T(8,128)(2,1)S(1)}, bf16[128,2048]{1,0:T(8,128)(2,1)}, u32[]{:S(2)}) copy-start(bf16[128,2048]{1,0:T(8,128)(2,1)} %residual_hbm.1) | copy-start | bytes 1572868
  17.0 2.2 %copy-start.24 = (f32[2048]{0:T(1024)S(1)}, f32[2048]{0:T(1024)}, u32[]{:S(2)}) copy-start(f32[2048]{0:T(1024)} %param.25) | copy-start | bytes 24580
  17.7 1.4 collective-permute-start.1
  19.1 2.2 %copy-start.5 = (bf16[1024,2048]{1,0:T(8,128)(2,1)S(1)}, bf16[1024,2048]{1,0:T(8,128)(2,1)}, u32[]{:S(2)}) copy-start(bf16[1024,2048]{1,0:T(8,128)(2,1)} %weight_hbm.1) | copy-start | bytes 12582916
  24.5 47.6 %copy-start.16 = (bf16[128,2048]{1,0:T(8,128)(2,1)}, bf16[128,2048]{1,0:T(8,128)(2,1)S(1)}, u32[]{:S(2)}) copy-start(bf16[128,2048]{1,0:T(8,128)(2,1)S(1)} %get-tuple-element.22.rest_0_) | copy-start | bytes 1572868
  24.6 47.6 %copy-start.14 = (bf16[256,2048]{1,0:T(8,128)(2,1)}, bf16[256,2048]{1,0:T(8,128)(2,1)S(1)}, u32[]{:S(2)}) copy-start(bf16[256,2048]{1,0:T(8,128)(2,1)S(1)} %get-tuple-element.20) | copy-start | bytes 3145732
  24.6 47.6 %copy-start.18 = (bf16[128,2048]{1,0:T(8,128)(2,1)}, bf16[128,2048]{1,0:T(8,128)(2,1)S(1)}, u32[]{:S(2)}) copy-start(bf16[128,2048]{1,0:T(8,128)(2,1)S(1)} %get-tuple-element.21.rows_hbm) | copy-start | bytes 1572868
  24.6 26.3 %collective-permute-start.3 = (bf16[128,2048]{1,0:T(8,128)(2,1)S(1)}, bf16[128,2048]{1,0:T(8,128)(2,1)S(1)}, u32[]{:S(2)}, u32[]{:S(2)}) collective-permute-start(bf16[128,2048]{1,0:T(8,128)(2,1)S(1)} %get-tuple-element.21.rows_hbm), channel_id=1, source_target_pairs={{0,16},{16,0},{1,17},{17,1},{2,18},{18,2},{3,19},{19,3},{4,20},{20... | collective-permute-start | bytes 1572872 | tf_op jit(solution)/shard_map/ppermute | solution.py:37
  27.2 23.6 %collective-permute-start.2 = (f32[4,128]{1,0:T(4,128)S(1)}, f32[4,128]{1,0:T(4,128)S(1)}, u32[]{:S(2)}, u32[]{:S(2)}) collective-permute-start(f32[4,128]{1,0:T(4,128)S(1)} %get-tuple-element.14.meta_ref), channel_id=1, source_target_pairs={{0,16},{16,0},{1,17},{17,1},{2,18},{18,2},{3,19},{19,3},{4,20},{20... | collective-permute-start | bytes 6152 | tf_op jit(solution)/shard_map/ppermute | solution.py:37
  52.2 23.7 %copy-start = (bf16[1,2048,512]{2,1,0:T(8,128)(2,1)S(1)}, bf16[1,2048,512]{2,1,0:T(8,128)(2,1)}, u32[]{:S(2)}) copy-start(bf16[1,2048,512]{2,1,0:T(8,128)(2,1)} %param.28) | copy-start | bytes 6291460
  72.2 19.8 %all-to-all-start = ((bf16[16,16,2048]{2,1,0:T(8,128)(2,1)}), bf16[16,16,2048]{2,1,0:T(8,128)(2,1)S(1)}, u32[]{:S(2)}, u32[]{:S(2)}) async-start(bf16[16,16,2048]{2,1,0:T(8,128)(2,1)} %bitcast.32), calls=%async_computation | async-start | bytes 2097152 | tf_op jit(solution)/shard_map/all_to_all | solution.py:647
  75.9 1.6 %copy-start.1 = (bf16[1,2048,512]{2,1,0:T(8,128)(2,1)S(1)}, bf16[1,2048,512]{2,1,0:T(8,128)(2,1)}, u32[]{:S(2)}) copy-start(bf16[1,2048,512]{2,1,0:T(8,128)(2,1)} %param.29) | copy-start | bytes 6291460
  77.5 1.6 %copy-start.3 = (bf16[1,512,2048]{2,1,0:T(8,128)(2,1)S(1)}, bf16[1,512,2048]{2,1,0:T(8,128)(2,1)}, u32[]{:S(2)}) copy-start(bf16[1,512,2048]{2,1,0:T(8,128)(2,1)} %param.30) | copy-start | bytes 6291460
  79.1 1.2 copy-start.10
  84.4 1.0 copy-start.9
  92.0 1.0 copy-start.7
  93.0 19.8 %all-to-all-start.3 = ((bf16[16,16,2048]{2,1,0:T(8,128)(2,1)}), bf16[16,16,2048]{2,1,0:T(8,128)(2,1)S(1)}, u32[]{:S(2)}, u32[]{:S(2)}) async-start(bf16[16,16,2048]{2,1,0:T(8,128)(2,1)} %bitcast.30), calls=%async_computation.3 | async-start | bytes 2097152 | tf_op jit(solution)/shard_map/all_to_all | solution.py:647
  96.6 1.6 %copy-start.2 = (bf16[1,2048,512]{2,1,0:T(8,128)(2,1)S(1)}, bf16[1,2048,512]{2,1,0:T(8,128)(2,1)}, u32[]{:S(2)}) copy-start(bf16[1,2048,512]{2,1,0:T(8,128)(2,1)} %param.29) | copy-start | bytes 6291460
  98.2 1.6 %copy-start.4 = (bf16[1,512,2048]{2,1,0:T(8,128)(2,1)S(1)}, bf16[1,512,2048]{2,1,0:T(8,128)(2,1)}, u32[]{:S(2)}) copy-start(bf16[1,512,2048]{2,1,0:T(8,128)(2,1)} %param.30) | copy-start | bytes 6291460
  99.8 1.2 copy-start.8
  105.1 1.0 copy-start.6
  112.7 29.8 %all-to-all-start.1 = ((bf16[16,16,2048]{2,1,0:T(8,128)(2,1)}), bf16[16,16,2048]{2,1,0:T(8,128)(2,1)S(1)}, u32[]{:S(2)}, u32[]{:S(2)}) async-start(bf16[16,16,2048]{2,1,0:T(8,128)(2,1)} %bitcast.28), calls=%async_computation.1 | async-start | bytes 2097152 | tf_op jit(solution)/shard_map/all_to_all | solution.py:647
  118.6 26.4 %collective-permute-start.4 = (bf16[128,2048]{1,0:T(8,128)(2,1)}, bf16[128,2048]{1,0:T(8,128)(2,1)S(1)}, u32[]{:S(2)}, u32[]{:S(2)}) collective-permute-start(bf16[128,2048]{1,0:T(8,128)(2,1)} %shard_map.166), channel_id=1, source_target_pairs={{0,16},{16,0},{1,17},{17,1},{2,18},{18,2},{3,19},{19,3},{4,20},{20... | collective-permute-start | bytes 1572872 | tf_op jit(solution)/shard_map/ppermute | solution.py:37
  121.2 1.6 %copy-start.11 = (bf16[2048,512]{1,0:T(8,128)(2,1)S(1)}, bf16[2048,512]{1,0:T(8,128)(2,1)}, u32[]{:S(2)}) copy-start(bf16[2048,512]{1,0:T(8,128)(2,1)} %gate_hbm.1) | copy-start | bytes 6291460
  122.8 1.6 %copy-start.12 = (bf16[2048,512]{1,0:T(8,128)(2,1)S(1)}, bf16[2048,512]{1,0:T(8,128)(2,1)}, u32[]{:S(2)}) copy-start(bf16[2048,512]{1,0:T(8,128)(2,1)} %up_hbm.1) | copy-start | bytes 6291460
  124.4 1.6 %copy-start.13 = (bf16[512,2048]{1,0:T(8,128)(2,1)S(1)}, bf16[512,2048]{1,0:T(8,128)(2,1)}, u32[]{:S(2)}) copy-start(bf16[512,2048]{1,0:T(8,128)(2,1)} %down_hbm.1) | copy-start | bytes 6291460
  126.0 1.0 copy-start.17
  127.0 1.0 copy-start.19

commit v4 on v3

v4 whole, which is shorter than its diff:
```python
import functools

import jax
import jax.numpy as jnp
from jax import lax
from jax.experimental import pallas as pl
from jax.experimental.pallas import tpu as pltpu
from jax.sharding import Mesh
from jax.sharding import PartitionSpec as P

LANES = 128


epsilon = 1e-06

HALF = ("sp", "tp")
LINE = ("half", "sp")

F32, BF16, I32 = jnp.float32, jnp.bfloat16, jnp.int32

ROWS = 32
STEPS = 4

VMEM = pl.BlockSpec(memory_space=pltpu.VMEM)
ANY = pl.BlockSpec(memory_space=pl.ANY)
HBM = pl.BlockSpec(memory_space=pltpu.HBM)
PARAMS = pltpu.CompilerParams(vmem_limit_bytes=24 * 2**20)


def from_behind(x, axis, by):
    peers = lax.axis_size(axis)
    pairs = [(i, i + by) for i in range(peers) if 0 <= i + by < peers]
    return lax.ppermute(x, axis, pairs)


def to_mirror(x):
    return lax.ppermute(x, "half", [(0, 1), (1, 0)])


def kept(*arrays):
    return [pltpu.with_memory_space_constraint(x, pltpu.HBM) for x in arrays]


def glu_of(value, gate):
    return (value.astype(F32) * jax.nn.sigmoid(gate.astype(F32))).astype(BF16)


def cost(flops, moved):
    return pl.CostEstimate(
        flops=int(flops), bytes_accessed=int(moved), transcendentals=0
    )


def column_of(row, count, start):
    across = lax.broadcasted_iota(I32, (count, LANES), 1)
    down = lax.broadcasted_iota(I32, (count, LANES), 0)
    picked = jnp.where(across == down + start, row, 0.0)
    return jnp.broadcast_to(jnp.sum(picked, axis=1, keepdims=True), (count, LANES))


def start_copies(pairs, sems, first=0):
    copies = []
    for index, (source, target) in enumerate(pairs):
        copies.append(pltpu.make_async_copy(source, target, sems.at[first + index]))
        copies[-1].start()
    return copies


def edge_body(
    value_hbm,
    gate_hbm,
    ids_hbm,
    routes_hbm,
    weight_hbm,
    edge_ref,
    meta_ref,
    value,
    gate,
    ids,
    routes,
    sems,
):
    rim, channels = value.shape
    positions = value_hbm.shape[0]
    top = routes_hbm.shape[0]
    tail = pl.ds(positions - rim, rim)
    copies = start_copies(
        (
            (value_hbm.at[tail, :], value),
            (gate_hbm.at[tail, :], gate),
            (ids_hbm.at[:, pl.ds(positions - LANES, LANES)], ids),
            (routes_hbm, routes),
            (weight_hbm, meta_ref.at[pl.ds(top, top), :]),
        ),
        sems,
    )
    for copy in copies:
        copy.wait()
    edge_ref[:, pl.ds(0, channels)] = glu_of(value[...], gate[...])
    edge_ref[:, pl.ds(channels, LANES)] = column_of(
        ids[...].astype(F32), rim, LANES - rim
    ).astype(BF16)
    meta_ref[pl.ds(0, top), :] = routes[...].astype(F32)


def edge_of(value, gate, ids, routes, weight, rim):
    channels = value.shape[1]
    top, tokens = routes.shape
    return pl.pallas_call(
        edge_body,
        out_shape=(
            jax.ShapeDtypeStruct((rim, channels + LANES), BF16),
            jax.ShapeDtypeStruct((2 * top, tokens), F32),
        ),
        in_specs=[HBM] * 5,
        out_specs=(VMEM, VMEM),
        scratch_shapes=[
            pltpu.VMEM((rim, channels), BF16),
            pltpu.VMEM((rim, channels), BF16),
            pltpu.VMEM((1, LANES), I32),
            pltpu.VMEM((top, tokens), I32),
            pltpu.SemaphoreType.DMA((5,)),
        ],
        cost_estimate=cost(1e6, 1e5),
        compiler_params=PARAMS,
        name="edge",
    )(*kept(value, gate, ids, routes, weight))


def conv_rows(row, count, rim, width, blocks, glu, ids, weights, gain_ref, shift_ref, store):
    here = ids[pl.ds(row + rim, count), :]
    total = [jnp.zeros((count, LANES), F32) for _ in range(blocks)]
    for tap in range(width):
        past = row + (rim - width + 1 + tap)
        same = ids[pl.ds(past, count), :] == here
        for c in range(blocks):
            weight = weights[pl.ds(tap, 1), pl.ds(c * LANES, LANES)]
            term = weight * glu[c, pl.ds(past, count), :]
            total[c] = total[c] + jnp.where(same, term, 0.0)
    for c in range(blocks):
        lanes = pl.ds(c * LANES, LANES)
        centered = total[c] - jnp.mean(total[c], axis=-1, keepdims=True)
        spread = jnp.mean(centered * centered, axis=-1, keepdims=True)
        scaled = centered * lax.rsqrt(spread + epsilon)
        store(
            lanes,
            jax.nn.silu(scaled * gain_ref[:, lanes] + shift_ref[:, lanes]).astype(BF16),
        )


def conv_body(
    value_hbm,
    gate_hbm,
    ids_hbm,
    taps_hbm,
    gain_hbm,
    shift_hbm,
    keep_ref,
    send_ref,
    head_ref,
    head_ids_ref,
    weights,
    gain_ref,
    shift_ref,
    value,
    gate,
    ids_row,
    taps,
    glu,
    ids,
    sems,
):
    positions, channels = value_hbm.shape
    width = taps_hbm.shape[0]
    blocks = channels // LANES
    rows = ROWS
    tokens = keep_ref.shape[0]
    small = start_copies(
        (
            (ids_hbm, ids_row),
            (taps_hbm, taps),
            (gain_hbm, gain_ref),
            (shift_hbm, shift_ref),
        ),
        sems,
    )
    tiles = []
    for c in range(blocks):
        lanes = pl.ds(c * LANES, LANES)
        tiles.append(
            start_copies(
                (
                    (value_hbm.at[:, lanes], value.at[:, lanes]),
                    (gate_hbm.at[:, lanes], gate.at[:, lanes]),
                ),
                sems,
                4 + 2 * c,
            )
        )
    for copy in small:
        copy.wait()
    weights[pl.ds(0, width), :] = taps[...].astype(F32)
    for start in range(0, positions, LANES):
        row = ids_row[:, pl.ds(start, LANES)].astype(F32)
        ids[pl.ds(start, LANES), :] = column_of(row, LANES, 0)
    for c, pair in enumerate(tiles):
        lanes = pl.ds(c * LANES, LANES)
        for copy in pair:
            copy.wait()
        glu[c] = glu_of(value[:, lanes], gate[:, lanes]).astype(F32)
        head_ref[c] = glu[c, pl.ds(0, rows), :]
    head_ids_ref[...] = ids[pl.ds(0, rows), :]

    core = lax.axis_index("tp")
    parts = positions // tokens
    for out_ref, part in ((send_ref, parts - 1 - core), (keep_ref, core)):

        def step(index, carry, out_ref=out_ref, part=part):
            inside = pl.multiple_of(index * rows, rows)
            row = pl.multiple_of(part * tokens + inside - rows, rows)

            def store(lanes, act):
                out_ref[pl.ds(inside, rows), lanes] = act

            conv_rows(
                row, rows, rows, width, blocks, glu, ids, weights, gain_ref, shift_ref, store
            )
            return carry

        lax.fori_loop((part == 0).astype(I32), tokens // rows, step, 0)


def convolve(value, gate, ids, taps, gain, shift, tokens):
    positions, channels = value.shape
    blocks = channels // LANES
    half = jax.ShapeDtypeStruct((tokens, channels), BF16)
    taps_rows = -(-taps.shape[0] // 8) * 8

    def same(x):
        return jax.ShapeDtypeStruct(x.shape, x.dtype)

    return pl.pallas_call(
        conv_body,
        out_shape=(
            half,
            half,
            jax.ShapeDtypeStruct((blocks, ROWS, LANES), F32),
            jax.ShapeDtypeStruct((ROWS, LANES), F32),
            jax.ShapeDtypeStruct((taps_rows, channels), F32),
            same(gain),
            same(shift),
        ),
        in_specs=[HBM] * 6,
        out_specs=[VMEM] * 7,
        scratch_shapes=[
            pltpu.VMEM((positions, channels), BF16),
            pltpu.VMEM((positions, channels), BF16),
            pltpu.VMEM((1, positions), I32),
            pltpu.VMEM(taps.shape, BF16),
            pltpu.VMEM((blocks, positions, LANES), F32),
            pltpu.VMEM((positions, LANES), F32),
            pltpu.SemaphoreType.DMA((4 + 2 * blocks,)),
        ],
        cost_estimate=cost(6e9, 6 * value.size),
        compiler_params=PARAMS,
        name="conv",
    )(*kept(value, gate, ids, taps, gain, shift))


def rim_body(
    width,
    edge_ref,
    head_ref,
    head_ids_ref,
    weights,
    gain_ref,
    shift_ref,
    keep_in,
    send_in,
    keep_any,
    send_any,
    glu,
    ids,
    act,
    sem,
):
    blocks, rows, _ = head_ref.shape
    channels = blocks * LANES
    ids[pl.ds(0, rows), :] = edge_ref[:, pl.ds(channels, LANES)].astype(F32)
    ids[pl.ds(rows, rows), :] = head_ids_ref[...]
    for c in range(blocks):
        glu[c, pl.ds(0, rows), :] = edge_ref[:, pl.ds(c * LANES, LANES)].astype(F32)
        glu[c, pl.ds(rows, rows), :] = head_ref[c]

    def store(lanes, value):
        act[:, lanes] = value

    conv_rows(0, rows, rows, width, blocks, glu, ids, weights, gain_ref, shift_ref, store)

    core = lax.axis_index("tp")
    for mine, out_any in ((core == 0, keep_any), (core != 0, send_any)):

        @pl.when(mine)
        def _(out_any=out_any):
            copy = pltpu.make_async_copy(act, out_any.at[pl.ds(0, rows), :], sem)
            copy.start()
            copy.wait()


def convolve_rim(edge, head, head_ids, weights, gain, shift, keep, send, width):
    blocks = head.shape[0]
    return pl.pallas_call(
        functools.partial(rim_body, width),
        out_shape=(
            jax.ShapeDtypeStruct(keep.shape, BF16),
            jax.ShapeDtypeStruct(send.shape, BF16),
        ),
        in_specs=[VMEM] * 6 + [ANY] * 2,
        out_specs=(ANY, ANY),
        input_output_aliases={6: 0, 7: 1},
        scratch_shapes=[
            pltpu.VMEM((blocks, 2 * ROWS, LANES), F32),
            pltpu.VMEM((2 * ROWS, LANES), F32),
            pltpu.VMEM((ROWS, blocks * LANES), BF16),
            pltpu.SemaphoreType.DMA,
        ],
        cost_estimate=cost(1e9, 4e5),
        compiler_params=PARAMS,
        name="rim",
    )(edge, head, head_ids, weights, gain, shift, keep, send)


def selection(routes, first, experts, capacity, rows):
    top, tokens = routes.shape
    routes = routes.astype(I32)
    names = lax.broadcasted_iota(I32, (experts, tokens), 0)
    earlier = lax.broadcasted_iota(I32, (tokens, tokens), 0) < lax.broadcasted_iota(
        I32, (tokens, tokens), 1
    )
    earlier = earlier.astype(F32).astype(BF16)
    index = lax.broadcasted_iota(I32, (rows, tokens), 0)
    used = jnp.zeros((experts, 1), F32)
    picks = []
    for k in range(top):
        route = routes[k : k + 1, :]
        chosen = (names == route).astype(F32)
        before = jnp.dot(chosen.astype(BF16), earlier, preferred_element_type=F32) + used
        slot = jnp.sum(chosen * before, axis=0, keepdims=True).astype(I32)
        picks.append(index == (route - first) * capacity + slot)
        used = used + jnp.sum(chosen, axis=1, keepdims=True)
    return picks


def first_expert(experts):
    return lax.axis_index("half") * (experts // lax.axis_size("half"))


def chosen_of(picks):
    return functools.reduce(jnp.logical_or, picks).astype(F32).astype(BF16)


def project_body(
    shape_of,
    meta_ref,
    gain_ref,
    keep_ref,
    got_ref,
    weight_ref,
    residual_ref,
    parcel_hbm,
    stream_ref,
    normed_ref,
    parcel,
    sems,
):
    experts, capacity, top = shape_of
    depth = keep_ref.shape[1]
    width = residual_ref.shape[1]
    core = lax.axis_index("tp")
    mine = pl.multiple_of(core * depth, depth)
    theirs = pl.multiple_of((1 - core) * depth, depth)
    picks = selection(
        meta_ref[pl.ds(0, top), :], first_expert(experts), experts, capacity, parcel.shape[0]
    )
    chosen = chosen_of(picks)
    tile = width // STEPS
    square = 0.0
    for n in range(STEPS):
        cols = pl.ds(n * tile, tile)
        total = jnp.dot(
            keep_ref[...], weight_ref[pl.ds(mine, depth), cols], preferred_element_type=F32
        )
        total = total + jnp.dot(
            got_ref[...], weight_ref[pl.ds(theirs, depth), cols], preferred_element_type=F32
        )
        stream = (residual_ref[:, cols].astype(F32) + total).astype(BF16)
        stream_ref[:, cols] = stream
        wide = stream.astype(F32)
        square = square + jnp.sum(wide * wide, axis=-1, keepdims=True)
    scale = lax.rsqrt(square / width + epsilon)
    back = []
    for n in range(STEPS):
        cols = pl.ds(n * tile, tile)
        normed = (stream_ref[:, cols].astype(F32) * scale * gain_ref[:, cols]).astype(BF16)
        normed_ref[:, cols] = normed
        parcel[:, cols] = jnp.dot(chosen, normed, preferred_element_type=F32).astype(BF16)
        back += start_copies(((parcel.at[:, cols], parcel_hbm.at[:, cols]),), sems, n)
    for copy in back:
        copy.wait()


def project(keep, got, weight, residual, gain, meta, sizes, rows):
    tokens, width = residual.shape
    out = jax.ShapeDtypeStruct((tokens, width), BF16)
    return pl.pallas_call(
        functools.partial(project_body, sizes),
        out_shape=(pltpu.HBM((rows, width), BF16), out, out),
        in_specs=[VMEM] * 6,
        out_specs=[HBM, VMEM, VMEM],
        scratch_shapes=[
            pltpu.VMEM((rows, width), BF16),
            pltpu.SemaphoreType.DMA((STEPS,)),
        ],
        cost_estimate=cost(2 * tokens * weight.size, 2 * weight.size),
        compiler_params=PARAMS,
        name="project",
    )(meta, gain, keep, got, weight, residual)


def gather_body(shape_of, meta_ref, rows_ref, parcel_ref):
    experts, capacity, top = shape_of
    picks = selection(
        meta_ref[pl.ds(0, top), :], first_expert(experts), experts, capacity, parcel_ref.shape[0]
    )
    chosen = chosen_of(picks)
    tile = rows_ref.shape[1] // STEPS
    for n in range(STEPS):
        cols = pl.ds(n * tile, tile)
        parcel_ref[:, cols] = jnp.dot(
            chosen, rows_ref[:, cols], preferred_element_type=F32
        ).astype(BF16)


def gather(meta, rows, sizes, count):
    tokens, width = rows.shape
    return pl.pallas_call(
        functools.partial(gather_body, sizes),
        out_shape=jax.ShapeDtypeStruct((count, width), BF16),
        in_specs=[VMEM, VMEM],
        out_specs=VMEM,
        cost_estimate=cost(2 * count * tokens * width, 2 * (count + tokens) * width),
        compiler_params=PARAMS,
        name="gather",
    )(meta, rows)


def expert_body(
    rows_ref, gate_ref, up_hbm, down_hbm, out_hbm, up, down, hidden, out, up_sems, sems, out_sems
):
    inner = gate_ref.shape[1]
    width = out.shape[1]
    half = inner // 2
    halves = [pl.ds(n * half, half) for n in range(2)]
    first = start_copies([(up_hbm.at[:, cols], up.at[:, cols]) for cols in halves], up_sems)
    second = stream_in(down_hbm, down, sems)
    rows = rows_ref[...]
    for cols, copy in zip(halves, first):
        gate = jnp.dot(rows, gate_ref[:, cols], preferred_element_type=F32)
        copy.wait()
        raised = jnp.dot(rows, up[:, cols], preferred_element_type=F32)
        hidden[:, cols] = (jax.nn.silu(gate) * raised).astype(BF16)
    tile = width // STEPS
    back = []
    for n, copy in enumerate(second):
        cols = pl.ds(n * tile, tile)
        copy.wait()
        out[:, cols] = jnp.dot(hidden[...], down[:, cols], preferred_element_type=F32).astype(BF16)
        back += start_copies(((out.at[:, cols], out_hbm.at[:, cols]),), out_sems, n)
    for copy in back:
        copy.wait()


def expert(rows, gate, up, down):
    count, width = rows.shape
    inner = gate.shape[1]
    return pl.pallas_call(
        expert_body,
        out_shape=pltpu.HBM((count, width), BF16),
        in_specs=[VMEM] * 2 + [HBM] * 2,
        out_specs=HBM,
        scratch_shapes=[
            pltpu.VMEM(up.shape, BF16),
            pltpu.VMEM(down.shape, BF16),
            pltpu.VMEM((count, inner), BF16),
            pltpu.VMEM((count, width), BF16),
            pltpu.SemaphoreType.DMA((2,)),
            pltpu.SemaphoreType.DMA((STEPS,)),
            pltpu.SemaphoreType.DMA((STEPS,)),
        ],
        cost_estimate=cost(6 * count * width * inner, 6 * width * inner),
        compiler_params=PARAMS,
        name="expert",
    )(rows, gate, *kept(up, down))


def mlp_body(
    steps,
    rows_hbm,
    gate_hbm,
    up_hbm,
    down_hbm,
    *rest,
):
    extra = rest[:-11]
    (out_hbm, rows, gate, up, down, total_gate, total_up, hidden, out, in_sems, out_sems) = rest[
        -11:
    ]
    depth = gate.shape[0] // steps
    tile = down.shape[1] // steps
    rows_copy = pltpu.make_async_copy(rows_hbm, rows, in_sems.at[0])
    rows_copy.start()
    wide, narrow = [], []
    for n in range(steps):
        part = pl.ds(n * depth, depth)
        pair = (
            pltpu.make_async_copy(gate_hbm.at[part, :], gate.at[part, :], in_sems.at[1 + 3 * n]),
            pltpu.make_async_copy(up_hbm.at[part, :], up.at[part, :], in_sems.at[2 + 3 * n]),
        )
        for copy in pair:
            copy.start()
        wide.append(pair)
    for n in range(steps):
        cols = pl.ds(n * tile, tile)
        copy = pltpu.make_async_copy(down_hbm.at[:, cols], down.at[:, cols], in_sems.at[3 + 3 * n])
        copy.start()
        narrow.append(copy)
    rows_copy.wait()
    for n, pair in enumerate(wide):
        part = pl.ds(n * depth, depth)
        for copy, weight, total in zip(pair, (gate, up), (total_gate, total_up)):
            copy.wait()
            product = jnp.dot(rows[:, part], weight[part, :], preferred_element_type=F32)
            total[...] = product if n == 0 else total[...] + product
    hidden[...] = (jax.nn.silu(total_gate[...]) * total_up[...]).astype(BF16)
    back = []
    for n, copy in enumerate(narrow):
        cols = pl.ds(n * tile, tile)
        copy.wait()
        result = jnp.dot(hidden[...], down[:, cols], preferred_element_type=F32)
        for ref in extra:
            result = result + ref[:, cols].astype(F32)
        out[:, cols] = result.astype(out.dtype)
        copy = pltpu.make_async_copy(out.at[:, cols], out_hbm.at[:, cols], out_sems.at[n])
        copy.start()
        back.append(copy)
    for copy in back:
        copy.wait()


def gated_mlp(rows, gate, up, down, extra, dtype):
    count, width = rows.shape
    inner = gate.shape[-1]
    steps = STEPS
    return pl.pallas_call(
        functools.partial(mlp_body, steps),
        out_shape=pltpu.HBM((count, width), dtype),
        in_specs=[ANY] + [HBM] * 3 + [VMEM] * len(extra),
        out_specs=ANY,
        scratch_shapes=[
            pltpu.VMEM((count, width), rows.dtype),
            pltpu.VMEM((width, inner), gate.dtype),
            pltpu.VMEM((width, inner), up.dtype),
            pltpu.VMEM((inner, width), down.dtype),
            pltpu.VMEM((count, inner), F32),
            pltpu.VMEM((count, inner), F32),
            pltpu.VMEM((count, inner), BF16),
            pltpu.VMEM((count, width), dtype),
            pltpu.SemaphoreType.DMA((1 + 3 * steps,)),
            pltpu.SemaphoreType.DMA((steps,)),
        ],
        cost_estimate=cost(6 * count * width * inner, 6 * width * inner),
        compiler_params=PARAMS,
    )(rows, *kept(gate, up, down), *extra)


def stream_in(source, target, sems):
    tile = target.shape[1] // STEPS
    tiles = [pl.ds(n * tile, tile) for n in range(STEPS)]
    return start_copies([(source.at[:, cols], target.at[:, cols]) for cols in tiles], sems)


def weigh(shape_of, meta_ref, rows):
    experts, capacity, top = shape_of
    picks = selection(meta_ref[pl.ds(0, top), :], first_expert(experts), experts, capacity, rows)
    table = jnp.zeros((rows, meta_ref.shape[1]), F32)
    for k, pick in enumerate(picks):
        table = table + jnp.where(pick, meta_ref[pl.ds(top + k, 1), :], 0.0)
    table = table.T
    high = table.astype(BF16)
    return high, (table - high.astype(F32)).astype(BF16)


def partial_body(shape_of, meta_ref, back_ref, out_ref):
    high, low = weigh(shape_of, meta_ref, back_ref.shape[0])
    tile = back_ref.shape[1] // STEPS
    for n in range(STEPS):
        cols = pl.ds(n * tile, tile)
        total = jnp.dot(high, back_ref[:, cols], preferred_element_type=F32)
        total = total + jnp.dot(low, back_ref[:, cols], preferred_element_type=F32)
        out_ref[:, cols] = total.astype(BF16)


def partial_sum(meta, back, sizes):
    rows, width = back.shape
    tokens = meta.shape[1]
    return pl.pallas_call(
        functools.partial(partial_body, sizes),
        out_shape=jax.ShapeDtypeStruct((tokens, width), BF16),
        in_specs=[VMEM, VMEM],
        out_specs=VMEM,
        cost_estimate=cost(4 * tokens * rows * width, 2 * rows * width),
        compiler_params=PARAMS,
        name="partial",
    )(meta, back)


def final_body(
    shape_of, meta_ref, back_ref, other_ref, base_any, out_hbm, base, out, in_sems, sems
):
    arrivals = stream_in(base_any, base, in_sems)
    high, low = weigh(shape_of, meta_ref, back_ref.shape[0])
    tile = back_ref.shape[1] // STEPS
    done = []
    for n in range(STEPS):
        cols = pl.ds(n * tile, tile)
        total = jnp.dot(high, back_ref[:, cols], preferred_element_type=F32)
        total = total + jnp.dot(low, back_ref[:, cols], preferred_element_type=F32)
        arrivals[n].wait()
        total = total + other_ref[:, cols].astype(F32) + base[:, cols]
        out[:, cols] = total.astype(BF16)
        done += start_copies(((out.at[:, cols], out_hbm.at[:, cols]),), sems, n)
    for copy in done:
        copy.wait()


def final_sum(meta, back, other, base, sizes):
    rows, width = back.shape
    tokens = meta.shape[1]
    return pl.pallas_call(
        functools.partial(final_body, sizes),
        out_shape=jax.ShapeDtypeStruct((tokens, width), BF16),
        in_specs=[VMEM] * 3 + [HBM],
        out_specs=HBM,
        scratch_shapes=[
            pltpu.VMEM((tokens, width), F32),
            pltpu.VMEM((tokens, width), BF16),
            pltpu.SemaphoreType.DMA((STEPS,)),
            pltpu.SemaphoreType.DMA((STEPS,)),
        ],
        cost_estimate=cost(4 * tokens * rows * width, 2 * rows * width),
        compiler_params=PARAMS,
        name="final",
    )(meta, back, other, *kept(base))


def per_device(
    conv_value,
    conv_gate,
    taps,
    doc_ids,
    gn_gain,
    gn_shift,
    conv_out,
    residual,
    norm_gain,
    routes,
    route_weight,
    expert_gate,
    expert_up,
    expert_down,
    shared_gate,
    shared_up,
    shared_down,
):
    model_width = residual.shape[1]
    token_count, top_count = routes.shape
    half_devices = lax.axis_size("sp") * lax.axis_size("tp")
    local_experts = expert_gate.shape[0]
    half_experts = local_experts * half_devices
    experts = half_experts * lax.axis_size("half")
    capacity = 2 * token_count * top_count // experts
    half_rows = half_experts * capacity
    sizes = (experts, capacity, top_count)

    ids = doc_ids[None, :]
    gain, shift = gn_gain[None, :], gn_shift[None, :]
    own_edge, own_meta = edge_of(conv_value, conv_gate, ids, routes.T, route_weight.T, ROWS)
    edge = from_behind(own_edge, LINE, 1)
    keep, send, head, head_ids, weights, gain, shift = convolve(
        conv_value, conv_gate, ids, taps, gain, shift, token_count
    )
    keep, send = convolve_rim(
        edge, head, head_ids, weights, gain, shift, keep, send, taps.shape[0]
    )
    got = lax.ppermute(send, "tp", [(0, 1), (1, 0)])
    mirror_meta = to_mirror(own_meta)
    parcel, stream, normed = project(
        keep, got, conv_out, residual, norm_gain[None, :], own_meta, sizes, half_rows
    )
    mirror_normed = to_mirror(normed)

    def exchange(rows):
        parcel = rows.reshape(half_devices, local_experts * capacity, model_width)
        arrived = lax.all_to_all(parcel, HALF, split_axis=0, concat_axis=0, tiled=True)
        return arrived.reshape(half_rows, model_width)

    def experts_on(rows):
        split = rows.reshape(half_devices, local_experts, capacity, model_width)
        results = []
        for e in range(local_experts):
            mine = split[:, e].reshape(half_devices * capacity, model_width)
            results.append(
                expert(mine, expert_gate[e], expert_up[e], expert_down[e]).reshape(half_devices, capacity, model_width)
            )
        return jnp.stack(results, axis=1)

    own_arrived = exchange(parcel)
    base = gated_mlp(normed, shared_gate, shared_up, shared_down, (stream,), F32)
    mirror_parcel = gather(mirror_meta, mirror_normed, sizes, half_rows)
    mirror_arrived = exchange(mirror_parcel)
    mirror_result = experts_on(mirror_arrived)
    mirror_back = exchange(mirror_result)
    own_result = experts_on(own_arrived)
    partial = partial_sum(mirror_meta, mirror_back, sizes)
    other_part = to_mirror(partial)
    own_back = exchange(own_result)
    return final_sum(own_meta, own_back, other_part, base, sizes)


def solution(mesh):
    sequence_split, core_split = mesh.devices.shape
    folded = Mesh(
        mesh.devices.reshape(2, sequence_split // 2, core_split), ("half", "sp", "tp")
    )
    line, everyone = LINE, LINE + ("tp",)
    return jax.shard_map(
        per_device,
        mesh=folded,
        in_specs=(
            P(line, "tp"),
            P(line, "tp"),
            P(None, "tp"),
            P(line),
            P("tp"),
            P("tp"),
            P(),
            P(everyone, None),
            P(),
            P(everyone, None),
            P(everyone, None),
            P(everyone, None, None),
            P(everyone, None, None),
            P(everyone, None, None),
            P(),
            P(),
            P(),
        ),
        out_specs=P(everyone, None),
        check_vma=False,
    )
```

time: 149 us -> 138 us (0.926)
  local copies, waits for them, and re-layouts: 29.5 us -> 5.05 us
  waiting for transfers between devices: 51.5 us -> 63.8 us
  Pallas kernels: 24.3 us -> 26.6 us
    unnamed x72 -> x22, local copies, waits for them, and re-layouts: 29.5 us -> 5.05 us
    all_to_all x3, waiting for transfers between devices: 24.4 us -> 38.8 us  [exchange(): lax.all_to_all(parcel, HALF, split_axis=0, concat_axis=0, tiled=True)]
    pallas_call x9, Pallas kernels: 23 us -> 26 us  [the longest x2 9.38 us: expert(): pl.pallas_call(expert_body, out_shape=pltpu.HBM((count, width), BF16), in...]
    ppermute x3, waiting for transfers between devices: 25.7 us -> 23.6 us  [to_mirror(): return lax.ppermute(x, 'half', [(0, 1), (1, 0)])]
  transfers between devices with their start and end apart: 8 -> 8, of which waited for: 6 -> 6; matrix products, arithmetic and copies ran while one was open for 0% -> 0% of each run, Pallas kernels for 11% -> 14%
where the time goes in v4:
time: 138 us; the launch traced here: 137 us
  waiting for transfers between devices  63.8 us (46%)
  Pallas kernels  26.6 us (19%)
  starting transfers between devices  21.4 us (16%)
  blocking collectives  20 us (14%)
  local copies, waits for them, and re-layouts  5.05 us (4%)
    all_to_all x3, waiting for transfers between devices, exchange(): lax.all_to_all(parcel, HALF, split_axis=0, concat_axis=0, tiled=True)  38.8 us
    ppermute x3, waiting for transfers between devices, to_mirror(): return lax.ppermute(x, 'half', [(0, 1), (1, 0)])  23.6 us
    all_to_all x1, blocking collectives, exchange(): lax.all_to_all(parcel, HALF, split_axis=0, concat_axis=0, tiled=True)  20 us
    all_to_all x3, starting transfers between devices, exchange(): lax.all_to_all(parcel, HALF, split_axis=0, concat_axis=0, tiled=True)  11 us
    pallas_call x2, Pallas kernels, expert(): pl.pallas_call(expert_body, out_shape=pltpu.HBM((count, width), BF16), in...  9.38 us
    ppermute x3, starting transfers between devices, to_mirror(): return lax.ppermute(x, 'half', [(0, 1), (1, 0)])  5.49 us
    unnamed x22, local copies, waits for them, and re-layouts  5.05 us
    ppermute x1, starting transfers between devices, from_behind(): return lax.ppermute(x, axis, pairs)  4.87 us
  transfers between devices with their start and end apart: 8, of which 6 were waited for; matrix products, arithmetic and copies ran while one was open for 0% of the time, Pallas kernels for 14%

profile of v4, /device:TPU:0, one launch (start us, length us, event | category | flops | bytes accessed | tf_op | source)
XLA Modules:
  0.0 137.0 jit_solution(78235497787750720)
XLA Ops:
  0.0 0.9 edge.1
  0.9 4.9 %collective-permute-start = (bf16[32,640]{1,0:T(8,128)(2,1)S(1)}, bf16[32,640]{1,0:T(8,128)(2,1)S(1)}, u32[]{:S(2)}, u32[]{:S(2)}) collective-permute-start(bf16[32,640]{1,0:T(8,128)(2,1)S(1)} %get-tuple-element.20), channel_id=1, source_target_pairs={{0,2},{2,4},{4,6},{6,8},{8,10},{10,12},{12,14},{14,16},{16,18},{18... | collective-permute-start | bytes 122888 | tf_op jit(solution)/shard_map/ppermute | solution.py:33
  5.8 0.0 copy-start.1
  5.8 4.7 %conv.1 = (bf16[128,512]{1,0:T(8,128)(2,1)S(1)}, bf16[128,512]{1,0:T(8,128)(2,1)S(1)}, f32[4,32,128]{2,1,0:T(8,128)S(1)}, f32[32,128]{1,0:T(8,128)S(1)}, f32[32,...) custom-call(bf16[256,512]{1,0:T(8,128)(2,1)} %value_hbm.3, bf16[256,512]{1,0:T(8,128)(2,1)} %gate_hbm.4, ...), custom_call_target="tpu_custom_call" | custom-call | flops 6000000000 | bytes 786432 | tf_op jit(solution)/shard_map/conv/pallas_call | solution.py:242
  10.5 0.0 copy-start.5
  10.5 0.0 copy-start.10
  10.5 0.0 collective-permute-done.edge_ref
  10.5 0.5 rim.1
  11.1 0.1 collective-permute-start.1
  11.1 1.3 collective-permute-done.1.got_ref
  12.5 0.0 copy-done.1
  12.5 0.0 copy-done.5
  12.5 0.0 copy-done.10
  12.5 2.2 %project.1 = (bf16[256,2048]{1,0:T(8,128)(2,1)}, bf16[128,2048]{1,0:T(8,128)(2,1)S(1)}, bf16[128,2048]{1,0:T(8,128)(2,1)S(1)}) custom-call(f32[4,128]{1,0:T(4,128)S(1)} %get-tuple-element.19.meta_ref, f32[1,2048]{1,0:T(1,128)S(1)} %bitcast.24, bf16[128,512]{1,0:T(8,128)(2,1)S(1)} %get-tuple-element.28.keep_ref, ...), custom_call_target="tpu_custom_call" | custom-call | flops 536870912 | bytes 4194304 | tf_op jit(solution)/shard_map/project/pallas_call | solution.py:415
  14.7 0.0 copy-start.6
  14.7 0.8 copy-done.6
  15.5 2.6 %collective-permute-start.3 = (bf16[128,2048]{1,0:T(8,128)(2,1)S(1)}, bf16[128,2048]{1,0:T(8,128)(2,1)S(1)}, u32[]{:S(2)}, u32[]{:S(2)}) collective-permute-start(bf16[128,2048]{1,0:T(8,128)(2,1)S(1)} %get-tuple-element.31.rows_hbm), channel_id=1, source_target_pairs={{0,16},{16,0},{1,17},{17,1},{2,18},{18,2},{3,19},{19,3},{4,20},{20... | collective-permute-start | bytes 1572872 | tf_op jit(solution)/shard_map/ppermute | solution.py:37
  18.1 0.0 copy-start.8
  18.1 0.8 copy-done.8
  18.8 0.3 collective-permute-start.2
  19.2 22.5 %collective-permute-done.2.meta_ref = f32[4,128]{1,0:T(4,128)S(1)} collective-permute-done((f32[4,128]{1,0:T(4,128)S(1)}, f32[4,128]{1,0:T(4,128)S(1)}, u32[]{:S(2)}, u32[]{:S(2)}) %collective-permute-start.2) | collective-permute-done | bytes 2080 | tf_op jit(solution)/shard_map/ppermute | solution.py:37
  41.7 0.0 collective-permute-done.3.rows_ref
  41.7 0.6 gather.1
  42.2 0.0 copy-start
  42.2 20.0 %all_to_all.20 = bf16[16,16,2048]{2,1,0:T(8,128)(2,1)} all-to-all(bf16[16,16,2048]{2,1,0:T(8,128)(2,1)S(1)} %bitcast.20), channel_id=1, replica_groups=mesh['half'=2,'sp'=8,'tp'=2] {'sp','tp'}, dimensions={0} | all-to-all | bytes 2097152 | tf_op jit(solution)/shard_map/all_to_all | solution.py:714
  62.2 3.7 %all-to-all-start = ((bf16[16,16,2048]{2,1,0:T(8,128)(2,1)}), bf16[16,16,2048]{2,1,0:T(8,128)(2,1)S(1)}, u32[]{:S(2)}, u32[]{:S(2)}) async-start(bf16[16,16,2048]{2,1,0:T(8,128)(2,1)} %bitcast.31), calls=%async_computation | async-start | bytes 2097152 | tf_op jit(solution)/shard_map/all_to_all | solution.py:714
  65.9 0.0 copy-done
  65.9 0.0 copy-start.4
  65.9 1.2 copy-done.4
  67.1 4.7 %expert.3 = bf16[256,2048]{1,0:T(8,128)(2,1)} custom-call(bf16[256,2048]{1,0:T(8,128)(2,1)S(1)} %bitcast.23, bf16[2048,512]{1,0:T(8,128)(2,1)S(1)} %bitcast.17, bf16[2048,512]{1,0:T(8,128)(2,1)} %bitcast.25, bf16[512,2048]{1,0:T(8,128)(2,1)} %bitcast.27), custom_call_target="tpu_custom_call" | custom-call | flops 1610612736 | bytes 6291456 | tf_op jit(solution)/shard_map/expert/pallas_call | solution.py:486
  71.9 10.2 %all-to-all-done = bf16[16,16,2048]{2,1,0:T(8,128)(2,1)S(1)} async-done(((bf16[16,16,2048]{2,1,0:T(8,128)(2,1)}), bf16[16,16,2048]{2,1,0:T(8,128)(2,1)S(1)}, u32[]{:S(2)}, u32[]{:S(2)}) %all-to-all-start) | async-done | bytes 1048608 | tf_op jit(solution)/shard_map/all_to_all | solution.py:714
  82.0 1.0 copy-done.2
  83.0 3.7 %all-to-all-start.3 = ((bf16[16,16,2048]{2,1,0:T(8,128)(2,1)}), bf16[16,16,2048]{2,1,0:T(8,128)(2,1)S(1)}, u32[]{:S(2)}, u32[]{:S(2)}) async-start(bf16[16,16,2048]{2,1,0:T(8,128)(2,1)} %bitcast.30), calls=%async_computation.3 | async-start | bytes 2097152 | tf_op jit(solution)/shard_map/all_to_all | solution.py:714
  86.7 0.0 copy-start.3
  86.7 1.2 copy-done.3
  87.9 4.7 %expert.2 = bf16[256,2048]{1,0:T(8,128)(2,1)} custom-call(bf16[256,2048]{1,0:T(8,128)(2,1)S(1)} %bitcast.22, bf16[2048,512]{1,0:T(8,128)(2,1)S(1)} %bitcast.18, bf16[2048,512]{1,0:T(8,128)(2,1)} %bitcast.26, bf16[512,2048]{1,0:T(8,128)(2,1)} %bitcast.28), custom_call_target="tpu_custom_call" | custom-call | flops 1610612736 | bytes 6291456 | tf_op jit(solution)/shard_map/expert/pallas_call | solution.py:486
  92.6 0.0 copy-start.7
  92.6 0.0 copy-start.9
  92.6 10.2 %all-to-all-done.3 = bf16[16,16,2048]{2,1,0:T(8,128)(2,1)S(1)} async-done(((bf16[16,16,2048]{2,1,0:T(8,128)(2,1)}), bf16[16,16,2048]{2,1,0:T(8,128)(2,1)S(1)}, u32[]{:S(2)}, u32[]{:S(2)}) %all-to-all-start.3) | async-done | bytes 1048608 | tf_op jit(solution)/shard_map/all_to_all | solution.py:714
  102.8 3.7 %all-to-all-start.1 = ((bf16[16,16,2048]{2,1,0:T(8,128)(2,1)}), bf16[16,16,2048]{2,1,0:T(8,128)(2,1)S(1)}, u32[]{:S(2)}, u32[]{:S(2)}) async-start(bf16[16,16,2048]{2,1,0:T(8,128)(2,1)} %bitcast.29), calls=%async_computation.1 | async-start | bytes 2097152 | tf_op jit(solution)/shard_map/all_to_all | solution.py:714
  106.4 1.4 %partial.1 = bf16[128,2048]{1,0:T(8,128)(2,1)} custom-call(f32[4,128]{1,0:T(4,128)S(1)} %collective-permute-done.2.meta_ref, bf16[256,2048]{1,0:T(8,128)(2,1)S(1)} %bitcast.19), custom_call_target="tpu_custom_call" | custom-call | flops 268435456 | bytes 1048576 | tf_op jit(solution)/shard_map/partial/pallas_call | solution.py:616
  107.9 2.6 %collective-permute-start.4 = (bf16[128,2048]{1,0:T(8,128)(2,1)}, bf16[128,2048]{1,0:T(8,128)(2,1)S(1)}, u32[]{:S(2)}, u32[]{:S(2)}) collective-permute-start(bf16[128,2048]{1,0:T(8,128)(2,1)} %partial.1), channel_id=1, source_target_pairs={{0,16},{16,0},{1,17},{17,1},{2,18},{18,2},{3,19},{19,3},{4,20},{20... | collective-permute-start | bytes 1572872 | tf_op jit(solution)/shard_map/ppermute | solution.py:37
  110.4 0.0 copy-done.7
  110.4 0.0 copy-done.9
  110.4 4.3 %shard_map.163.base_any = f32[128,2048]{1,0:T(8,128)} custom-call(bf16[128,2048]{1,0:T(8,128)(2,1)S(1)} %copy-done.9, bf16[2048,512]{1,0:T(8,128)(2,1)} %gate_hbm.5, bf16[2048,512]{1,0:T(8,128)(2,1)} %up_hbm.1, bf16[512,2048]{1,0:T(8,128)(2,1)} %down_hbm.1, bf16[128,2048]{1,0:T(8,128)(2,1)S(1)} %copy-done.7), custom_call_target="tpu_custom_call" | custom-call | flops 805306368 | bytes 6291456 | tf_op jit(solution)/shard_map/pallas_call | solution.py:564
  114.8 18.5 %all-to-all-done.1 = bf16[16,16,2048]{2,1,0:T(8,128)(2,1)S(1)} async-done(((bf16[16,16,2048]{2,1,0:T(8,128)(2,1)}), bf16[16,16,2048]{2,1,0:T(8,128)(2,1)S(1)}, u32[]{:S(2)}, u32[]{:S(2)}) %all-to-all-start.1) | async-done | bytes 1048608 | tf_op jit(solution)/shard_map/all_to_all | solution.py:714
  133.2 1.1 collective-permute-done.4.other_ref
  134.4 2.6 %final.1 = bf16[128,2048]{1,0:T(8,128)(2,1)} custom-call(f32[4,128]{1,0:T(4,128)S(1)} %get-tuple-element.19.meta_ref, bf16[256,2048]{1,0:T(8,128)(2,1)S(1)} %bitcast.21, bf16[128,2048]{1,0:T(8,128)(2,1)S(1)} %collective-permute-done.4.other_ref, f32[128,2048]{1,0:T(8,128)} %shard_map.163.base_any), custom_call_target="tpu_custom_call" | custom-call | flops 268435456 | bytes 1048576 | tf_op jit(solution)/shard_map/final/pallas_call | solution.py:649
  (1 shorter events, 0.0 us)
Async XLA Ops:
  0.9 9.6 %collective-permute-start = (bf16[32,640]{1,0:T(8,128)(2,1)S(1)}, bf16[32,640]{1,0:T(8,128)(2,1)S(1)}, u32[]{:S(2)}, u32[]{:S(2)}) collective-permute-start(bf16[32,640]{1,0:T(8,128)(2,1)S(1)} %get-tuple-element.20), channel_id=1, source_target_pairs={{0,2},{2,4},{4,6},{6,8},{8,10},{10,12},{12,14},{14,16},{16,18},{18... | collective-permute-start | bytes 122888 | tf_op jit(solution)/shard_map/ppermute | solution.py:33
  5.8 6.7 %copy-start.1 = (bf16[1024,2048]{1,0:T(8,128)(2,1)S(1)}, bf16[1024,2048]{1,0:T(8,128)(2,1)}, u32[]{:S(2)}) copy-start(bf16[1024,2048]{1,0:T(8,128)(2,1)} %weight_ref.1) | copy-start | bytes 12582916
  10.5 2.0 %copy-start.5 = (bf16[128,2048]{1,0:T(8,128)(2,1)S(1)}, bf16[128,2048]{1,0:T(8,128)(2,1)}, u32[]{:S(2)}) copy-start(bf16[128,2048]{1,0:T(8,128)(2,1)} %residual_ref.1) | copy-start | bytes 1572868
  10.5 2.0 %copy-start.10 = (f32[2048]{0:T(1024)S(1)}, f32[2048]{0:T(1024)}, u32[]{:S(2)}) copy-start(f32[2048]{0:T(1024)} %param.25) | copy-start | bytes 24580
  11.1 1.4 %collective-permute-start.1 = (bf16[128,512]{1,0:T(8,128)(2,1)S(1)}, bf16[128,512]{1,0:T(8,128)(2,1)S(1)}, u32[]{:S(2)}, u32[]{:S(2)}) collective-permute-start(bf16[128,512]{1,0:T(8,128)(2,1)S(1)} %get-tuple-element.29), channel_id=1, source_target_pairs={{0,1},{1,0},{2,3},{3,2},{4,5},{5,4},{6,7},{7,6},{8,9},{9,8},{10,11... | collective-permute-start | bytes 393224 | tf_op jit(solution)/shard_map/ppermute | solution.py:705
  14.7 0.8 copy-start.6
  15.5 26.2 %collective-permute-start.3 = (bf16[128,2048]{1,0:T(8,128)(2,1)S(1)}, bf16[128,2048]{1,0:T(8,128)(2,1)S(1)}, u32[]{:S(2)}, u32[]{:S(2)}) collective-permute-start(bf16[128,2048]{1,0:T(8,128)(2,1)S(1)} %get-tuple-element.31.rows_hbm), channel_id=1, source_target_pairs={{0,16},{16,0},{1,17},{17,1},{2,18},{18,2},{3,19},{19,3},{4,20},{20... | collective-permute-start | bytes 1572872 | tf_op jit(solution)/shard_map/ppermute | solution.py:37
  18.1 0.8 copy-start.8
  18.8 22.8 %collective-permute-start.2 = (f32[4,128]{1,0:T(4,128)S(1)}, f32[4,128]{1,0:T(4,128)S(1)}, u32[]{:S(2)}, u32[]{:S(2)}) collective-permute-start(f32[4,128]{1,0:T(4,128)S(1)} %get-tuple-element.19.meta_ref), channel_id=1, source_target_pairs={{0,16},{16,0},{1,17},{17,1},{2,18},{18,2},{3,19},{19,3},{4,20},{20... | collective-permute-start | bytes 6152 | tf_op jit(solution)/shard_map/ppermute | solution.py:37
  42.2 23.7 %copy-start = (bf16[1,2048,512]{2,1,0:T(8,128)(2,1)S(1)}, bf16[1,2048,512]{2,1,0:T(8,128)(2,1)}, u32[]{:S(2)}) copy-start(bf16[1,2048,512]{2,1,0:T(8,128)(2,1)} %param.28) | copy-start | bytes 6291460
  62.2 19.8 %all-to-all-start = ((bf16[16,16,2048]{2,1,0:T(8,128)(2,1)}), bf16[16,16,2048]{2,1,0:T(8,128)(2,1)S(1)}, u32[]{:S(2)}, u32[]{:S(2)}) async-start(bf16[16,16,2048]{2,1,0:T(8,128)(2,1)} %bitcast.31), calls=%async_computation | async-start | bytes 2097152 | tf_op jit(solution)/shard_map/all_to_all | solution.py:714
  65.9 1.2 copy-start.4
  82.0 1.0 copy-start.2
  83.0 19.8 %all-to-all-start.3 = ((bf16[16,16,2048]{2,1,0:T(8,128)(2,1)}), bf16[16,16,2048]{2,1,0:T(8,128)(2,1)S(1)}, u32[]{:S(2)}, u32[]{:S(2)}) async-start(bf16[16,16,2048]{2,1,0:T(8,128)(2,1)} %bitcast.30), calls=%async_computation.3 | async-start | bytes 2097152 | tf_op jit(solution)/shard_map/all_to_all | solution.py:714
  86.7 1.2 copy-start.3
  92.6 17.9 %copy-start.7 = (bf16[128,2048]{1,0:T(8,128)(2,1)S(1)}, bf16[128,2048]{1,0:T(8,128)(2,1)}, u32[]{:S(2)}) copy-start(bf16[128,2048]{1,0:T(8,128)(2,1)} %copy-done.6) | copy-start | bytes 1572868
  92.6 17.9 %copy-start.9 = (bf16[128,2048]{1,0:T(8,128)(2,1)S(1)}, bf16[128,2048]{1,0:T(8,128)(2,1)}, u32[]{:S(2)}) copy-start(bf16[128,2048]{1,0:T(8,128)(2,1)} %copy-done.8) | copy-start | bytes 1572868
  102.8 30.5 %all-to-all-start.1 = ((bf16[16,16,2048]{2,1,0:T(8,128)(2,1)}), bf16[16,16,2048]{2,1,0:T(8,128)(2,1)S(1)}, u32[]{:S(2)}, u32[]{:S(2)}) async-start(bf16[16,16,2048]{2,1,0:T(8,128)(2,1)} %bitcast.29), calls=%async_computation.1 | async-start | bytes 2097152 | tf_op jit(solution)/shard_map/all_to_all | solution.py:714
  107.9 26.5 %collective-permute-start.4 = (bf16[128,2048]{1,0:T(8,128)(2,1)}, bf16[128,2048]{1,0:T(8,128)(2,1)S(1)}, u32[]{:S(2)}, u32[]{:S(2)}) collective-permute-start(bf16[128,2048]{1,0:T(8,128)(2,1)} %partial.1), channel_id=1, source_target_pairs={{0,16},{16,0},{1,17},{17,1},{2,18},{18,2},{3,19},{19,3},{4,20},{20... | collective-permute-start | bytes 1572872 | tf_op jit(solution)/shard_map/ppermute | solution.py:37
